TPU v7x, 128 devices: a whole 4x4x4 slice. The times are simulated.
128 devices in a mesh: ep: 64 (over z, y, x), tp: 2 (over core).
Axes of the slice: x: 4, y: 4, z: 4, core: 2. Of those that a mesh axis runs over, the one named last changes fastest.
Arguments:
- tokens: bfloat16 [16384, 2048], P('ep'), may hold values from -16 to 16
- expert_ids: int32 [16384, 4], P('ep'), may hold values from 0 to 63, all different within a row; in each aligned block of 256 rows (0 to 255, 256 to 511, ...) at most 24 rows name the same one
- gates: float32 [16384, 4], P('ep'), may hold values from 0.05 to 0.6
- cotangent: bfloat16 [16384, 2048], P('ep'), may hold values from -16 to 16
- w_gate: bfloat16 [64, 2048, 512], P('ep', None, 'tp'), may hold values from -0.125 to 0.125
- w_up: bfloat16 [64, 2048, 512], P('ep', None, 'tp'), may hold values from -0.125 to 0.125
- w_down: bfloat16 [64, 512, 2048], P('ep', 'tp'), may hold values from -0.25 to 0.25
- sh_gate: bfloat16 [2048, 512], P(None, 'tp'), may hold values from -0.125 to 0.125
- sh_up: bfloat16 [2048, 512], P(None, 'tp'), may hold values from -0.125 to 0.125
- sh_down: bfloat16 [512, 2048], P('tp'), may hold values from -0.25 to 0.25
Outputs:
- token_grad: bfloat16 [16384, 2048], P('ep', 'tp')
- gate_grad: float32 [16384, 4], P('ep')
- expert_gate_grad: float32 [64, 2048, 512], P('ep', None, 'tp')
- expert_up_grad: float32 [64, 2048, 512], P('ep', None, 'tp')
- expert_down_grad: float32 [64, 512, 2048], P('ep', 'tp')
- shared_gate_grad: float32 [2048, 512], P('ep', 'tp')
- shared_up_grad: float32 [2048, 512], P('ep', 'tp')
- shared_down_grad: float32 [512, 2048], P('tp', 'ep')
- expert_gate_rows: float32 [64, 2048], P('ep')
- expert_up_rows: float32 [64, 2048], P('ep')
- expert_down_rows: float32 [64, 512], P('ep', 'tp')
- shared_gate_rows: float32 [2048], P('ep')
- shared_up_rows: float32 [2048], P('ep')
- shared_down_rows: float32 [512], P('tp')
Inputs may be any that keep to these rules, and one draw needn't show every extreme that they name: `expert_ids`: each row names 4 different experts. Within each aligned block of 256 tokens no expert is named by more than 24 assignments, a bound that is reached in some blocks.
All inputs are finite; a program needn't handle non-finite values.
Results may differ from a plain program's by a relative error of at most 0.0085.
Values may be sent and summed in bfloat16 or wider, within the bound.
No kernel may reach another device: no remote copies, remote signals or barrier semaphores. Data moves between devices by JAX's collectives and lax.ppermute only.
A program may use at most 128 MiB of HBM per device.

v0:
```python
import jax
import jax.numpy as jnp
from jax import lax
from jax.sharding import PartitionSpec as P


F32 = jnp.float32
BF16 = jnp.bfloat16
ROWS = (((0,), (0,)), ((), ()))
COLS = (((1,), (1,)), ((), ()))
PLAIN = (((1,), (0,)), ((), ()))


def mm(a, b, contract=PLAIN):
    return lax.dot_general(a, b, contract, preferred_element_type=F32)


def swap(x):
    return lax.ppermute(x, "tp", [(0, 1), (1, 0)])


def to_each(x):
    return lax.all_to_all(x, "ep", 0, 0, tiled=True)


def silu_parts(pre):
    sigmoid = jax.nn.sigmoid(pre)
    return (pre * sigmoid, sigmoid * (1.0 + pre * (1.0 - sigmoid)))


def to_hidden(inputs, cots, w_g, w_u, w_d):
    gate_pre = mm(inputs, w_g)
    up_pre = mm(inputs, w_u)
    active, slope = silu_parts(gate_pre)
    hidden = (active * up_pre).astype(BF16)
    hidden_cot = mm(cots, w_d, COLS)
    gate_part = jnp.sum(hidden.astype(F32) * hidden_cot, axis=1)
    d_gate = (hidden_cot * up_pre * slope).astype(BF16)
    d_up = (hidden_cot * active).astype(BF16)
    return hidden, d_gate, d_up, gate_part


def input_rows(d_both, w_both, first, width):
    return mm(d_both, lax.dynamic_slice_in_dim(w_both, first, width, 0), COLS).astype(BF16)


def layer(tokens, expert_ids, gates, cotangent, w_gate, w_up, w_down, sh_gate, sh_up, sh_down):
    experts = lax.axis_size("ep")
    tok_rows, width = tokens.shape
    top = expert_ids.shape[1]
    cap = 3 * tok_rows * top // (2 * experts)
    slots = experts * cap
    half = width // 2
    tp = lax.axis_index("tp")
    own, other = tp * half, (1 - tp) * half
    w_g, w_u, w_d = w_gate[0], w_up[0], w_down[0]

    ids_t = expert_ids.T
    names = [ids_t[k][None, :] == jnp.arange(experts, dtype=jnp.int32)[:, None] for k in range(top)]
    hit = names[0]
    for name in names[1:]:
        hit = hit | name
    order = jnp.arange(tok_rows)
    before = (order[:, None] < order[None, :]).astype(BF16)
    rank = mm(hit.astype(BF16), before)
    place = jnp.where(hit, rank, -1.0)
    pick = place[:, None, :] == jnp.arange(cap, dtype=F32)[None, :, None]
    select = pick.astype(BF16).reshape(slots, tok_rows)
    gates_t = gates.T
    gate_of = sum(jnp.where(names[k], gates_t[k][None, :], 0.0) for k in range(top))
    slot_gate = jnp.sum(jnp.where(pick, gate_of[:, None, :], 0.0), axis=2).reshape(slots)

    both = jnp.concatenate(
        [
            lax.dynamic_slice_in_dim(tokens, own, half, 1),
            lax.dynamic_slice_in_dim(cotangent, own, half, 1),
        ],
        axis=1,
    )
    is_cot = jnp.arange(width) >= half
    scale = jnp.where(is_cot[None, :], slot_gate[:, None], 1.0)
    sent = (mm(select, both) * scale).astype(BF16)
    got = to_each(sent.reshape(experts, cap, width)).reshape(slots, width)

    s_hidden, s_gate, s_up, _ = to_hidden(tokens, cotangent, sh_gate, sh_up, sh_down)
    hid = s_hidden.shape[1]
    s_both = jnp.concatenate([sh_gate, sh_up], axis=1)
    s_d = jnp.concatenate([s_gate, s_up], axis=1)
    s_other = input_rows(s_d, s_both, other, half)
    s_own = input_rows(s_d, s_both, own, half)
    shared = jnp.concatenate([mm(tokens, s_d, ROWS), mm(cotangent, s_hidden, ROWS)], axis=1).astype(BF16)
    shared_got = to_each(shared.reshape(experts, width // experts, 3 * hid))
    s_peer = swap(s_other)
    w_gu = jnp.concatenate([w_g, w_u], axis=1)
    w_gu_own = lax.dynamic_slice_in_dim(w_gu, own, half, 0)
    w_gu_other = lax.dynamic_slice_in_dim(w_gu, other, half, 0)
    w_d_own = lax.dynamic_slice_in_dim(w_d, own, half, 1)
    w_d_other = lax.dynamic_slice_in_dim(w_d, other, half, 1)

    peer = swap(got)
    pre = mm(got[:, :half], w_gu_own) + mm(peer[:, :half], w_gu_other)
    hidden_cot = mm(got[:, half:], w_d_own, COLS) + mm(peer[:, half:], w_d_other, COLS)
    gate_pre, up_pre = pre[:, :hid], pre[:, hid:]
    active, slope = silu_parts(gate_pre)
    hidden = (active * up_pre).astype(BF16)
    gate_part = jnp.sum(hidden.astype(F32) * hidden_cot, axis=1)
    d_both = jnp.concatenate([hidden_cot * up_pre * slope, hidden_cot * active], axis=1).astype(BF16)
    rows_other = mm(d_both, w_gu_other, COLS).astype(BF16)
    rows_own = mm(d_both, w_gu_own, COLS).astype(BF16)
    from_peer = swap(rows_other)
    gate_peer = swap(gate_part)
    slot_rows = (from_peer.astype(F32) + rows_own.astype(F32)).astype(BF16)
    back_rows = to_each(slot_rows.reshape(experts, cap, half)).reshape(slots, half)

    low = tp == 0
    inputs = jnp.concatenate(
        [jnp.where(low, got[:, :half], peer[:, :half]), jnp.where(low, peer[:, :half], got[:, :half])],
        axis=1,
    )
    cots = jnp.concatenate(
        [jnp.where(low, got[:, half:], peer[:, half:]), jnp.where(low, peer[:, half:], got[:, half:])],
        axis=1,
    )
    grad_g = mm(inputs, d_both[:, :hid], ROWS)
    grad_u = mm(inputs, d_both[:, hid:], ROWS)
    grad_d = mm(hidden, cots, ROWS)

    shared_sum = jnp.sum(shared_got.astype(F32), axis=0)
    shared_g, shared_u = shared_sum[:, :hid], shared_sum[:, hid : 2 * hid]
    shared_d = shared_sum[:, 2 * hid :].T
    down_part = jnp.sum(shared_d * shared_d, axis=1)
    s_rows = s_peer.astype(F32) + s_own.astype(F32)
    gate_sum = gate_part + gate_peer
    small = jnp.concatenate(
        [gate_sum.reshape(experts, cap), jnp.broadcast_to(down_part[None], (experts, hid))], axis=1
    )
    small = to_each(small)
    back_gate = small[:, :cap]
    down_norms = jnp.sum(small[:, cap:], axis=0)

    norms = jnp.concatenate(
        [
            jnp.sum(grad_g * grad_g, axis=1),
            jnp.sum(grad_u * grad_u, axis=1),
            jnp.sum(shared_g * shared_g, axis=1),
            jnp.sum(shared_u * shared_u, axis=1),
        ]
    )
    norms = norms + swap(norms)
    step = width // experts
    gate_norms, up_norms = norms[:width], norms[width : 2 * width]
    shared_gate_norms, shared_up_norms = norms[2 * width : 2 * width + step], norms[2 * width + step :]

    routed = mm(select, back_rows, ROWS)
    token_grad = (routed + s_rows).astype(BF16)
    gate_at = jnp.sum(jnp.where(pick, back_gate[:, :, None], 0.0), axis=1)
    gate_grad = (
        jnp.stack([jnp.sum(jnp.where(name, gate_at, 0.0), axis=0) for name in names], axis=1) / gates
    )
    return (
        token_grad,
        gate_grad,
        grad_g[None],
        grad_u[None],
        grad_d[None],
        shared_g,
        shared_u,
        shared_d,
        gate_norms[None],
        up_norms[None],
        jnp.sum(grad_d * grad_d, axis=1)[None],
        shared_gate_norms,
        shared_up_norms,
        down_norms,
    )


def solution(mesh):
    placed = (
        P("ep", None),
        P("ep", None),
        P("ep", None),
        P("ep", None),
        P("ep", None, "tp"),
        P("ep", None, "tp"),
        P("ep", "tp", None),
        P(None, "tp"),
        P(None, "tp"),
        P("tp", None),
    )
    return jax.shard_map(
        layer,
        mesh=mesh,
        in_specs=placed,
        out_specs=(
            P("ep", "tp"),
            P("ep", None),
            P("ep", None, "tp"),
            P("ep", None, "tp"),
            P("ep", "tp", None),
            P("ep", "tp"),
            P("ep", "tp"),
            P("tp", "ep"),
            P("ep", None),
            P("ep", None),
            P("ep", "tp"),
            P("ep"),
            P("ep"),
            P("tp"),
        ),
        check_vma=False,
    )
```

profile of v0, /device:TPU:0, one launch (start us, length us, event | category | flops | bytes accessed | tf_op | source)
XLA Modules:
  0.0 228.8 jit_solution(18437642324484138321)
XLA Ops:
  0.8 0.8 fusion.61
  1.6 0.8 fusion.60
  3.3 1.1 constant_dynamic-slice_fusion
  4.4 1.1 constant_dynamic-slice_fusion.1
  5.5 2.1 multiply_convert_fusion
  7.6 86.7 %all_to_all.27 = bf16[64,24,2048]{2,1,0:T(8,128)(2,1)} all-to-all(bf16[64,24,2048]{2,1,0:T(8,128)(2,1)S(1)} %bitcast.65), channel_id=1, replica_groups=mesh['ep'=64,'tp'=2] {'ep'}, dimensions={0} | all-to-all | bytes 12582912 | tf_op jit(solution)/shard_map/all_to_all | solution.py:23
  96.7 1.3 copy.34
  98.0 2.0 fusion.6
  100.0 2.9 %copy.33 = bf16[2048,512]{1,0:T(8,128)(2,1)S(1)} copy(bf16[2048,512]{0,1:T(8,128)(2,1)} %fusion.6) | data formatting | bytes 4194304 | tf_op jit(solution)/shard_map/dot_general | solution.py:15
  102.9 3.1 %pad_maximum_fusion.3 = bf16[64,32,768]{2,1,0:T(8,128)(2,1)} fusion(bf16[64,32,256]{2,1,0:T(8,128)(2,1)} %bitcast.66, bf16[64,32,512]{2,1,0:T(8,128)(2,1)S(1)} %bitcast.64), kind=kLoop, calls=%fused_computation.13 | loop fusion | flops 6291456 | bytes 6291456 | tf_op jit(solution)/shard_map/concatenate | solution.py:91
  106.0 6.4 %all-to-all-start.2 = ((bf16[64,32,768]{2,1,0:T(8,128)(2,1)}), bf16[64,32,768]{2,1,0:T(8,128)(2,1)}, u32[]{:S(2)}, u32[]{:S(2)}) async-start(bf16[64,32,768]{2,1,0:T(8,128)(2,1)} %pad_maximum_fusion.3), calls=%async_computation.2 | async-start | bytes 6291456 | tf_op jit(solution)/shard_map/all_to_all | solution.py:23
  112.5 3.1 %fusion.12 = f32[1536,256]{0,1:T(8,128)S(1)} fusion(bf16[1536,2048]{1,0:T(8,128)(2,1)} %bitcast.12, bf16[1,256,2048]{2,1,0:T(8,128)(2,1)S(1)} %copy-done, s32[]{:T(128)S(6)} %select_n.90), kind=kOutput, calls=%fused_computation.27 | convolution fusion | flops 805306368 | bytes 5242884 | tf_op jit(solution)/shard_map/dot_general | solution.py:15
  115.6 3.8 %fusion.9 = f32[1536,512]{0,1:T(8,128)S(1)} fusion(bf16[1536,2048]{1,0:T(8,128)(2,1)} %bitcast.12, s32[]{:T(128)S(6)} %select_n.90, bf16[2048,256]{1,0:T(8,128)(2,1)S(1)} %bitcast.96, bf16[2048,256]{1,0:T(8,128)(2,1)S(1)} %bitcast.100), kind=kOutput, calls=%fused_computation.24 | convolution fusion | flops 1612709888 | bytes 8388612 | tf_op jit(solution)/shard_map/dot_general | solution.py:15
  119.4 3.8 %convolution_add_fusion = f32[1536,512]{0,1:T(8,128)S(1)} fusion(f32[1536,512]{0,1:T(8,128)S(1)} %fusion.9, bf16[1536,2048]{1,0:T(8,128)(2,1)} %collective-permute-done, s32[]{:T(128)S(6)} %select_n.97, bf16[2048,256]{1,0:T(8,128)(2,1)S(1)} %bitcast.97, bf16[2048,256]{1,0:T(8,128)(2,1)S(1)} %bitcast.101), kind=kOutput, calls=%fused_computation.12 | convolution fusion | flops 1613496320 | bytes 11534340 | tf_op jit(solution)/shard_map/dot_general | solution.py:15
  123.2 4.5 %multiply_reduce_fusion.3 = (f32[1536]{0:T(1024)S(1)}, bf16[1536,256]{0,1:T(8,128)(2,1)}, bf16[1536,256]{0,1:T(8,128)(2,1)S(1)}, bf16[1536,256]{0,1:T(8,128)(2,1)S(1)}) fusion(f32[1536,512]{0,1:T(8,128)S(1)} %convolution_add_fusion, f32[1536,256]{0,1:T(8,128)S(1)} %fusion.12, bf16[1,256,2048]{2,1,0:T(8,128)(2,1)S(1)} %copy-done, s32[]{:T(128)S(6)} %select_n.97, ...), kind=kOutput, calls=%fused_computation.39 | convolution fusion | flops 812775936 | bytes 10754052 | tf_op jit(solution)/shard_map/dot_general | solution.py:15
  127.8 3.5 %convolution_convert_fusion.1 = bf16[1536,1024]{1,0:T(8,128)(2,1)} fusion(bf16[1536,256]{0,1:T(8,128)(2,1)S(1)} %get-tuple-element.72, bf16[1536,256]{0,1:T(8,128)(2,1)S(1)} %get-tuple-element.73, s32[]{:T(128)S(6)} %select_n.97, bf16[2048,256]{1,0:T(8,128)(2,1)S(1)} %bitcast.98, bf16[2048,256]{1,0:T(8,128)(2,1)S(1)} %bitcast.102), kind=kOutput, calls=%fused_computation.11 | convolution fusion | flops 1617428480 | bytes 6815748 | tf_op jit(solution)/shard_map/dot_general | solution.py:15
  131.5 1.3 convolution_convert_fusion.5
  133.3 1.6 fusion.17
  134.8 19.8 %all-to-all-done.2 = bf16[64,32,768]{2,1,0:T(8,128)(2,1)} async-done(((bf16[64,32,768]{2,1,0:T(8,128)(2,1)}), bf16[64,32,768]{2,1,0:T(8,128)(2,1)}, u32[]{:S(2)}, u32[]{:S(2)}) %all-to-all-start.2) | async-done | bytes 3145760 | tf_op jit(solution)/shard_map/all_to_all | solution.py:23
  154.6 2.3 %convert_reduce_fusion = f32[32,768]{1,0:T(8,128)S(1)} fusion(bf16[64,32,768]{2,1,0:T(8,128)(2,1)} %all-to-all-done.2), kind=kLoop, calls=%fused_computation.6 | loop fusion | flops 3121152 | bytes 3244032 | tf_op jit(solution)/shard_map/reduce_sum | solution.py:128
  159.7 7.8 %all-to-all-start.3 = ((f32[64,1,280]{2,1,0:T(1,128)}), f32[64,1,280]{2,1,0:T(1,128)S(1)}, u32[]{:S(2)}, u32[]{:S(2)}) async-start(f32[64,1,280]{2,1,0:T(1,128)} %all_to_all.20), calls=%async_computation.3 | async-start | bytes 196608 | tf_op jit(solution)/shard_map/all_to_all | solution.py:23
  167.5 5.7 %add_convert_fusion = bf16[1536,1024]{1,0:T(8,128)(2,1)} fusion(bf16[1536,1024]{1,0:T(8,128)(2,1)} %collective-permute-done.1, bf16[1536,256]{0,1:T(8,128)(2,1)S(1)} %copy-done.16, bf16[1536,256]{0,1:T(8,128)(2,1)} %copy-done.17, s32[]{:T(128)S(6)} %select_n.90, bf16[2048,256]{1,0:T(8,128)(2,1)S(1)} %bitcast.99, bf16[2048,256]{1,0:T(8,128)(2,1)S(1)} %bitcast.103), kind=kOutput, calls=%fused_computation.7 | convolution fusion | flops 1623719936 | bytes 9961476 | tf_op jit(solution)/shard_map/dot_general | solution.py:15
  173.2 3.8 %all-to-all-done.3 = f32[64,1,280]{2,1,0:T(1,128)S(1)} async-done(((f32[64,1,280]{2,1,0:T(1,128)}), f32[64,1,280]{2,1,0:T(1,128)S(1)}, u32[]{:S(2)}, u32[]{:S(2)}) %all-to-all-start.3) | async-done | bytes 71712 | tf_op jit(solution)/shard_map/all_to_all | solution.py:23
  177.0 6.6 %all-to-all-start.1 = ((bf16[64,24,1024]{2,1,0:T(8,128)(2,1)}), bf16[64,24,1024]{2,1,0:T(8,128)(2,1)}, u32[]{:S(2)}, u32[]{:S(2)}) async-start(bf16[64,24,1024]{2,1,0:T(8,128)(2,1)} %bitcast.67), calls=%async_computation.1 | async-start | bytes 6291456 | tf_op jit(solution)/shard_map/all_to_all | solution.py:23
  183.6 7.8 %broadcast_select_fusion.1 = (bf16[1536,1024]{1,0:T(8,128)(2,1)}, bf16[1536,1024]{1,0:T(8,128)(2,1)S(1)}, bf16[1536,1024]{1,0:T(8,128)(2,1)}, bf16[1536,1024]{1,0:T(8,128)(2,1)S(1)}) fusion(pred[]{:T(512)S(6)} %eq.127, bf16[1536,2048]{1,0:T(8,128)(2,1)} %collective-permute-done, bf16[1536,2048]{1,0:T(8,128)(2,1)} %bitcast.12), kind=kLoop, calls=%fused_computation.15 | loop fusion | flops 6291456 | bytes 25165824 | tf_op jit(solution)/shard_map/jit(_where)/select_n | solution.py:121
  191.4 1.8 multiply_reduce_fusion.2
  193.2 4.4 %multiply_reduce_fusion.1 = (f32[2048]{0:T(1024)S(1)}, f32[2048,256]{0,1:T(8,128)}) fusion(bf16[1536,256]{0,1:T(8,128)(2,1)S(1)} %copy-done.16, bf16[1536,1024]{1,0:T(8,128)(2,1)S(1)} %get-tuple-element.69, bf16[1536,1024]{1,0:T(8,128)(2,1)S(1)} %get-tuple-element.71), kind=kOutput, calls=%fused_computation.34 | convolution fusion | flops 1624242176 | bytes 9183232 | tf_op jit(solution)/shard_map/dot_general | solution.py:15
  197.6 6.8 %multiply_reduce_fusion = (f32[256]{0:T(256)}, f32[256,2048]{1,0:T(8,128)}) fusion(bf16[1536,256]{0,1:T(8,128)(2,1)} %get-tuple-element.67, bf16[1536,1024]{1,0:T(8,128)(2,1)} %get-tuple-element.70, bf16[1536,1024]{1,0:T(8,128)(2,1)} %get-tuple-element.68), kind=kOutput, calls=%fused_computation.33 | convolution fusion | flops 1624243968 | bytes 9176064 | tf_op jit(solution)/shard_map/dot_general | solution.py:15
  204.4 1.8 copy.35
  206.2 3.0 %copy.36 = f32[1,2048,256]{2,1,0:T(8,128)} copy(f32[1,2048,256]{1,2,0:T(8,128)} %bitcast.69) | data formatting | bytes 4194304
  212.1 12.8 %all-to-all-done.1 = bf16[64,24,1024]{2,1,0:T(8,128)(2,1)} async-done(((bf16[64,24,1024]{2,1,0:T(8,128)(2,1)}), bf16[64,24,1024]{2,1,0:T(8,128)(2,1)}, u32[]{:S(2)}, u32[]{:S(2)}) %all-to-all-start.1) | async-done | bytes 3145760 | tf_op jit(solution)/shard_map/all_to_all | solution.py:23
  225.0 3.8 %add_convert_fusion.1 = bf16[256,1024]{1,0:T(8,128)(2,1)} fusion(f32[256,1024]{1,0:T(8,128)S(1)} %copy-done.6, bf16[256,1024]{1,0:T(8,128)(2,1)} %collective-permute-done.2, bf16[64,24,1024]{2,1,0:T(8,128)(2,1)} %all-to-all-done.1, f32[64,256]{1,0:T(8,128)S(1)} %convolution_select_fusion), kind=kOutput, calls=%fused_computation.58 | convolution fusion | flops 806748160 | bytes 5308416 | tf_op jit(solution)/shard_map/dot_general | solution.py:15
  (79 shorter events, 9.7 us)
Async XLA Ops:
  0.6 111.8 %copy-start = (bf16[1,256,2048]{2,1,0:T(8,128)(2,1)S(1)}, bf16[1,256,2048]{2,1,0:T(8,128)(2,1)}, u32[]{:S(2)}) copy-start(bf16[1,256,2048]{2,1,0:T(8,128)(2,1)} %param.16) | copy-start | bytes 3145732
  7.6 86.8 %copy-start.2 = (bf16[256,2048]{1,0:T(8,128)(2,1)S(1)}, bf16[256,2048]{1,0:T(8,128)(2,1)}, u32[]{:S(2)}) copy-start(bf16[256,2048]{1,0:T(8,128)(2,1)} %param.13) | copy-start | bytes 3145732
  7.6 86.8 %copy-start.7 = (bf16[256,2048]{1,0:T(8,128)(2,1)S(1)}, bf16[256,2048]{1,0:T(8,128)(2,1)}, u32[]{:S(2)}) copy-start(bf16[256,2048]{1,0:T(8,128)(2,1)} %param.19) | copy-start | bytes 3145732
  7.6 87.3 %copy-start.3 = (bf16[256,2048]{1,0:T(8,128)(2,1)S(1)}, bf16[256,2048]{1,0:T(8,128)(2,1)}, u32[]{:S(2)}) copy-start(bf16[256,2048]{1,0:T(8,128)(2,1)} %param.10) | copy-start | bytes 3145732
  7.6 87.3 %copy-start.4 = (bf16[2048,256]{1,0:T(8,128)(2,1)S(1)}, bf16[2048,256]{1,0:T(8,128)(2,1)}, u32[]{:S(2)}) copy-start(bf16[2048,256]{1,0:T(8,128)(2,1)} %param.18) | copy-start | bytes 3145732
  94.4 1.2 copy-start.8
  94.4 25.0 %collective-permute-start = (bf16[1536,2048]{1,0:T(8,128)(2,1)}, bf16[1536,2048]{1,0:T(8,128)(2,1)}, u32[]{:S(2)}, u32[]{:S(2)}) collective-permute-start(bf16[1536,2048]{1,0:T(8,128)(2,1)} %bitcast.12), channel_id=1, source_target_pairs={{0,1},{1,0},{2,3},{3,2},{4,5},{5,4},{6,7},{7,6},{8,9},{9,8},{10,11... | collective-permute-start | bytes 18874376 | tf_op jit(solution)/shard_map/ppermute | solution.py:19
  106.0 48.6 %all-to-all-start.2 = ((bf16[64,32,768]{2,1,0:T(8,128)(2,1)}), bf16[64,32,768]{2,1,0:T(8,128)(2,1)}, u32[]{:S(2)}, u32[]{:S(2)}) async-start(bf16[64,32,768]{2,1,0:T(8,128)(2,1)} %pad_maximum_fusion.3), calls=%async_computation.2 | async-start | bytes 6291456 | tf_op jit(solution)/shard_map/all_to_all | solution.py:23
  112.5 3.1 %copy-start.11 = (bf16[1,2048,256]{2,1,0:T(8,128)(2,1)S(1)}, bf16[1,2048,256]{2,1,0:T(8,128)(2,1)}, u32[]{:S(2)}) copy-start(bf16[1,2048,256]{2,1,0:T(8,128)(2,1)} %param.14) | copy-start | bytes 3145732
  112.5 3.1 %copy-start.13 = (bf16[1,2048,256]{2,1,0:T(8,128)(2,1)S(1)}, bf16[1,2048,256]{2,1,0:T(8,128)(2,1)}, u32[]{:S(2)}) copy-start(bf16[1,2048,256]{2,1,0:T(8,128)(2,1)} %param.15) | copy-start | bytes 3145732
  127.7 3.5 %copy-start.15 = (bf16[1536,256]{0,1:T(8,128)(2,1)}, bf16[1536,256]{0,1:T(8,128)(2,1)S(1)}, u32[]{:S(2)}) copy-start(bf16[1536,256]{0,1:T(8,128)(2,1)S(1)} %get-tuple-element.72) | copy-start | bytes 2359300
  127.7 3.5 %copy-start.17 = (bf16[1536,256]{0,1:T(8,128)(2,1)}, bf16[1536,256]{0,1:T(8,128)(2,1)S(1)}, u32[]{:S(2)}) copy-start(bf16[1536,256]{0,1:T(8,128)(2,1)S(1)} %get-tuple-element.73) | copy-start | bytes 2359300
  127.7 3.6 %copy-start.9 = (bf16[2048,256]{1,0:T(8,128)(2,1)S(1)}, bf16[2048,256]{1,0:T(8,128)(2,1)}, u32[]{:S(2)}) copy-start(bf16[2048,256]{1,0:T(8,128)(2,1)} %param.17) | copy-start | bytes 3145732
  127.7 3.7 %copy-start.5 = (bf16[2048,256]{1,0:T(8,128)(2,1)S(1)}, bf16[2048,256]{1,0:T(8,128)(2,1)}, u32[]{:S(2)}) copy-start(bf16[2048,256]{1,0:T(8,128)(2,1)} %param.18) | copy-start | bytes 3145732
  131.3 36.2 %collective-permute-start.1 = (bf16[1536,1024]{1,0:T(8,128)(2,1)}, bf16[1536,1024]{1,0:T(8,128)(2,1)}, u32[]{:S(2)}, u32[]{:S(2)}) collective-permute-start(bf16[1536,1024]{1,0:T(8,128)(2,1)} %convolution_convert_fusion.1), channel_id=1, source_target_pairs={{0,1},{1,0},{2,3},{3,2},{4,5},{5,4},{6,7},{7,6},{8,9},{9,8},{10,11... | collective-permute-start | bytes 9437192 | tf_op jit(solution)/shard_map/ppermute | solution.py:19
  132.8 79.3 %collective-permute-start.2 = (bf16[256,1024]{1,0:T(8,128)(2,1)}, bf16[256,1024]{1,0:T(8,128)(2,1)}, u32[]{:S(2)}, u32[]{:S(2)}) collective-permute-start(bf16[256,1024]{1,0:T(8,128)(2,1)} %convolution_convert_fusion.5), channel_id=1, source_target_pairs={{0,1},{1,0},{2,3},{3,2},{4,5},{5,4},{6,7},{7,6},{8,9},{9,8},{10,11... | collective-permute-start | bytes 1572872 | tf_op jit(solution)/shard_map/ppermute | solution.py:19
  133.3 34.3 %copy-start.16 = (bf16[1536,256]{0,1:T(8,128)(2,1)S(1)}, bf16[1536,256]{0,1:T(8,128)(2,1)}, u32[]{:S(2)}) copy-start(bf16[1536,256]{0,1:T(8,128)(2,1)} %copy-done.15) | copy-start | bytes 2359300
  134.8 32.7 %copy-start.12 = (bf16[1,2048,256]{2,1,0:T(8,128)(2,1)S(1)}, bf16[1,2048,256]{2,1,0:T(8,128)(2,1)}, u32[]{:S(2)}) copy-start(bf16[1,2048,256]{2,1,0:T(8,128)(2,1)} %param.14) | copy-start | bytes 3145732
  134.8 32.7 %copy-start.14 = (bf16[1,2048,256]{2,1,0:T(8,128)(2,1)S(1)}, bf16[1,2048,256]{2,1,0:T(8,128)(2,1)}, u32[]{:S(2)}) copy-start(bf16[1,2048,256]{2,1,0:T(8,128)(2,1)} %param.15) | copy-start | bytes 3145732
  157.7 1.2 collective-permute-start.3
  159.7 17.3 %all-to-all-start.3 = ((f32[64,1,280]{2,1,0:T(1,128)}), f32[64,1,280]{2,1,0:T(1,128)S(1)}, u32[]{:S(2)}, u32[]{:S(2)}) async-start(f32[64,1,280]{2,1,0:T(1,128)} %all_to_all.20), calls=%async_computation.3 | async-start | bytes 196608 | tf_op jit(solution)/shard_map/all_to_all | solution.py:23
  177.0 47.9 %all-to-all-start.1 = ((bf16[64,24,1024]{2,1,0:T(8,128)(2,1)}), bf16[64,24,1024]{2,1,0:T(8,128)(2,1)}, u32[]{:S(2)}, u32[]{:S(2)}) async-start(bf16[64,24,1024]{2,1,0:T(8,128)(2,1)} %bitcast.67), calls=%async_computation.1 | async-start | bytes 6291456 | tf_op jit(solution)/shard_map/all_to_all | solution.py:23
  183.6 7.8 %copy-start.18 = (bf16[1536,256]{0,1:T(8,128)(2,1)S(1)}, bf16[1536,256]{0,1:T(8,128)(2,1)}, u32[]{:S(2)}) copy-start(bf16[1536,256]{0,1:T(8,128)(2,1)} %copy-done.17) | copy-start | bytes 2359300
  197.6 11.6 %collective-permute-start.4 = (f32[4160]{0:T(1024)S(1)}, f32[4160]{0:T(1024)S(1)}, u32[]{:S(2)}, u32[]{:S(2)}) collective-permute-start(f32[4160]{0:T(1024)S(1)} %concatenate.48), channel_id=1, source_target_pairs={{0,1},{1,0},{2,3},{3,2},{4,5},{5,4},{6,7},{7,6},{8,9},{9,8},{10,11... | collective-permute-start | bytes 49928 | tf_op jit(solution)/shard_map/ppermute | solution.py:19
  206.2 5.3 %copy-start.10 = (f32[256,4]{0,1:T(4,128)S(1)}, f32[256,4]{0,1:T(4,128)}, u32[]{:S(2)}) copy-start(f32[256,4]{0,1:T(4,128)} %param.12) | copy-start | bytes 12292
  206.2 18.7 %copy-start.6 = (f32[256,1024]{1,0:T(8,128)S(1)}, f32[256,1024]{1,0:T(8,128)}, u32[]{:S(2)}) copy-start(f32[256,1024]{1,0:T(8,128)} %fusion.17) | copy-start | bytes 3145732
  211.5 17.3 %copy-start.1 = (bf16[1,256,2048]{2,1,0:T(8,128)(2,1)S(1)}, bf16[1,256,2048]{2,1,0:T(8,128)(2,1)}, u32[]{:S(2)}) copy-start(bf16[1,256,2048]{2,1,0:T(8,128)(2,1)} %param.16) | copy-start | bytes 3145732
where the time goes:
time: 230 us; the launch traced here: 229 us
  blocking collectives  86.7 us (38%)
  matrix products  50.3 us (22%)
  waiting for transfers between devices  36.9 us (16%)
  starting transfers between devices  21.3 us (9%)
  other arithmetic  17 us (7%)
  local copies, waits for them, and re-layouts  15.5 us (7%)
    all_to_all x1, blocking collectives, to_each(): return lax.all_to_all(x, 'ep', 0, 0, tiled=True)  86.7 us
    dot_general x19, matrix products, mm(): return lax.dot_general(a, b, contract, preferred_element_type=F32)  50.3 us
    all_to_all x3, waiting for transfers between devices, to_each(): return lax.all_to_all(x, 'ep', 0, 0, tiled=True)  36.4 us
    all_to_all x3, starting transfers between devices, to_each(): return lax.all_to_all(x, 'ep', 0, 0, tiled=True)  20.7 us
    select_n x1, other arithmetic, layer(): jnp.where(low, got[:, half:], peer[:, half:])  7.79 us
    unnamed x42, local copies, waits for them, and re-layouts  5.11 us
  transfers between devices with their start and end apart: 8, of which 4 were waited for; matrix products, arithmetic and copies ran while one was open for 31% of the time, Pallas kernels for 0%

commit v1 on v0

--- a/solution.py
+++ b/solution.py
@@ -1,6 +1,8 @@
 import jax
 import jax.numpy as jnp
 from jax import lax
+from jax.experimental import pallas as pl
+from jax.experimental.pallas import tpu as pltpu
 from jax.sharding import PartitionSpec as P
 
 
@@ -21,6 +23,221 @@
 
 def to_each(x):
     return lax.all_to_all(x, "ep", 0, 0, tiled=True)
+
+
+def routing_kernel(tp_ref, ids_ref, gates_ref, tok_ref, cot_ref, sent_ref, place_ref, place_at, gate_at):
+    experts, tok_rows = place_at.shape
+    rows, width = sent_ref.shape
+    half = width // 2
+    steps = pl.num_programs(0)
+    block = experts // steps
+    cap = rows // block
+    step = pl.program_id(0)
+
+    @pl.when(step == 0)
+    def _():
+        e = lax.broadcasted_iota(jnp.int32, (experts, tok_rows), 0)
+        hit = jnp.zeros((experts, tok_rows), F32)
+        gate_of = jnp.zeros((experts, tok_rows), F32)
+        for k in range(ids_ref.shape[0]):
+            name = ids_ref[k : k + 1, :] == e
+            hit = jnp.where(name, 1.0, hit)
+            gate_of = jnp.where(name, gates_ref[k : k + 1, :], gate_of)
+        earlier = lax.broadcasted_iota(jnp.int32, (tok_rows, tok_rows), 0)
+        later = lax.broadcasted_iota(jnp.int32, (tok_rows, tok_rows), 1)
+        before = jnp.where(earlier < later, 1.0, 0.0).astype(BF16)
+        rank = mm(hit.astype(BF16), before)
+        place = jnp.where(hit > 0.0, rank, -1.0)
+        place_at[...] = place
+        gate_at[...] = gate_of
+        place_ref[...] = place
+
+    r = lax.broadcasted_iota(jnp.int32, (cap, tok_rows), 0).astype(F32)
+    picks, scales = [], []
+    for j in range(block):
+        at = pl.ds(step * block + j, 1)
+        pick = jnp.broadcast_to(place_at[at, :], (cap, tok_rows)) == r
+        picks.append(jnp.where(pick, 1.0, 0.0))
+        scales.append(jnp.sum(jnp.where(pick, gate_at[at, :], 0.0), axis=1, keepdims=True))
+    select = jnp.concatenate(picks, axis=0).astype(BF16)
+    scale = jnp.concatenate(scales, axis=0)
+    sent_ref[:, :half] = mm(select, tok_ref[...]).astype(BF16)
+    sent_ref[:, half:] = (mm(select, cot_ref[...]) * scale).astype(BF16)
+
+
+def routing(tp, ids_t, gates_t, tokens, cotangent, experts, cap):
+    tok_rows, width = tokens.shape
+    half = width // 2
+    top = ids_t.shape[0]
+    steps = 8
+    rows = experts * cap // steps
+    return pl.pallas_call(
+        routing_kernel,
+        grid_spec=pltpu.PrefetchScalarGridSpec(
+            num_scalar_prefetch=1,
+            grid=(steps,),
+            in_specs=[
+                pl.BlockSpec((top, tok_rows), lambda i, tp: (0, 0)),
+                pl.BlockSpec((top, tok_rows), lambda i, tp: (0, 0)),
+                pl.BlockSpec((tok_rows, half), lambda i, tp: (0, tp[0])),
+                pl.BlockSpec((tok_rows, half), lambda i, tp: (0, tp[0])),
+            ],
+            out_specs=[
+                pl.BlockSpec((rows, width), lambda i, tp: (i, 0)),
+                pl.BlockSpec((experts, tok_rows), lambda i, tp: (0, 0)),
+            ],
+            scratch_shapes=[pltpu.VMEM((experts, tok_rows), F32), pltpu.VMEM((experts, tok_rows), F32)],
+        ),
+        out_shape=[
+            jax.ShapeDtypeStruct((experts * cap, width), BF16),
+            jax.ShapeDtypeStruct((experts, tok_rows), F32),
+        ],
+        name="routing",
+    )(tp.reshape(1), ids_t, gates_t, tokens, cotangent)
+
+
+def payload_kernel(own_ref, peer_ref, out_ref):
+    block, lines, lanes = out_ref.shape
+    cap = own_ref.shape[0] // block
+    for e in range(block):
+        at = slice(e * cap, (e + 1) * cap)
+        for c in range(lines // cap):
+            cols = slice(c * lanes, (c + 1) * lanes)
+            both = own_ref[at, cols].astype(F32) + peer_ref[at, cols].astype(F32)
+            out_ref[e, c * cap : (c + 1) * cap, :] = both.astype(BF16)
+
+
+def payload_of(own, peer, experts, extra):
+    slots, half = own.shape
+    steps = 8
+    cap = slots // experts
+    lines = cap * half // 128
+    return pl.pallas_call(
+        payload_kernel,
+        grid=(steps,),
+        in_specs=[pl.BlockSpec((slots // steps, half), lambda i: (i, 0))] * 2,
+        out_specs=pl.BlockSpec((experts // steps, lines, 128), lambda i: (i, 0, 0)),
+        out_shape=jax.ShapeDtypeStruct((experts, lines + extra, 128), BF16),
+        name="payload",
+    )(own, peer)
+
+
+def total_kernel(got_ref, notes_ref, payload_ref, sums_ref, out_ref, acc):
+    step = pl.program_id(0)
+    part = jnp.sum(got_ref[...].astype(F32), axis=0)
+
+    @pl.when(step == 0)
+    def _():
+        acc[...] = part
+
+    @pl.when(step > 0)
+    def _():
+        acc[...] = acc[...] + part
+
+    @pl.when(step == pl.num_programs(0) - 1)
+    def _():
+        total = acc[...]
+        sums_ref[...] = total
+        down = total[:, 2 * (total.shape[1] // 3) :]
+        norms = jnp.sum(down * down, axis=0, keepdims=True)
+        high = norms.astype(BF16).astype(F32)
+        low = norms - high
+        lines = out_ref.shape[1:]
+        row = lax.broadcasted_iota(jnp.int32, lines, 0)
+        marks = jnp.zeros(lines, F32)
+        pieces = norms.shape[1] // lines[1]
+        for at, value in enumerate((high, low)):
+            for c in range(pieces):
+                line = value[:, c * lines[1] : (c + 1) * lines[1]]
+                marks = jnp.where(row == at * pieces + c, line, marks)
+        out_ref[...] = (notes_ref[...] + marks[None]).astype(BF16)
+
+
+def totals(got, notes, payload):
+    size, rows, cols = got.shape
+    steps = 4
+    experts, extra, lanes = notes.shape
+    last = payload.shape[1] // extra - 1
+    return pl.pallas_call(
+        total_kernel,
+        grid=(steps,),
+        in_specs=[
+            pl.BlockSpec((size // steps, rows, cols), lambda i: (i, 0, 0)),
+            pl.BlockSpec((experts, extra, lanes), lambda i: (0, 0, 0)),
+            pl.BlockSpec(memory_space=pl.ANY),
+        ],
+        out_specs=[
+            pl.BlockSpec((rows, cols), lambda i: (0, 0)),
+            pl.BlockSpec((experts, extra, lanes), lambda i: (0, last, 0)),
+        ],
+        out_shape=[
+            jax.ShapeDtypeStruct((rows, cols), F32),
+            jax.ShapeDtypeStruct(payload.shape, BF16),
+        ],
+        input_output_aliases={2: 1},
+        scratch_shapes=[pltpu.VMEM((rows, cols), F32)],
+        name="totals",
+    )(got, notes, payload)
+
+
+def final_kernel(rows_ref, notes_ref, select_ref, own_ref, peer_ref, place_ref, ids_ref, gates_ref, tok_ref, gate_ref, down_ref):
+    experts, lines, lanes = rows_ref.shape
+    cap = lines // 2
+    left = rows_ref[:, :cap, :].reshape(experts * cap, lanes)
+    right = rows_ref[:, cap:, :].reshape(experts * cap, lanes)
+    back = jnp.concatenate([left, right], axis=1)
+    routed = mm(select_ref[...], back)
+    tok_ref[...] = (routed + (own_ref[...].astype(F32) + peer_ref[...].astype(F32))).astype(BF16)
+
+    @pl.when(pl.program_id(0) == 0)
+    def _():
+        notes = notes_ref[...].astype(F32)
+        whole = jnp.sum(notes, axis=0)
+        down_ref[...] = whole
+        row = lax.broadcasted_iota(jnp.int32, notes.shape, 1)
+        gate = jnp.sum(jnp.where((row == 4) | (row == 5), notes, 0.0), axis=1)
+        place = place_ref[...]
+        at = jnp.zeros(place.shape, F32)
+        for r in range(cap):
+            at = jnp.where(place == r, gate[:, r : r + 1], at)
+        e = lax.broadcasted_iota(jnp.int32, place.shape, 0)
+        for k in range(ids_ref.shape[0]):
+            mine = jnp.sum(jnp.where(ids_ref[k : k + 1, :] == e, at, 0.0), axis=0, keepdims=True)
+            gate_ref[k : k + 1, :] = mine / gates_ref[k : k + 1, :]
+
+
+def finished(payload, select_t, s_own, s_peer, place, ids_t, gates_t):
+    experts, lines, lanes = payload.shape
+    tok_rows, half = s_own.shape
+    slots = select_t.shape[1]
+    cap = slots // experts
+    steps = half // (2 * lanes)
+    extra = lines - cap * half // lanes
+    return pl.pallas_call(
+        final_kernel,
+        grid=(steps,),
+        in_specs=[
+            pl.BlockSpec((experts, 2 * cap, lanes), lambda i: (0, i, 0)),
+            pl.BlockSpec((experts, extra, lanes), lambda i: (0, lines // extra - 1, 0)),
+            pl.BlockSpec((tok_rows, slots), lambda i: (0, 0)),
+            pl.BlockSpec((tok_rows, 2 * lanes), lambda i: (0, i)),
+            pl.BlockSpec((tok_rows, 2 * lanes), lambda i: (0, i)),
+            pl.BlockSpec(place.shape, lambda i: (0, 0)),
+            pl.BlockSpec(ids_t.shape, lambda i: (0, 0)),
+            pl.BlockSpec(gates_t.shape, lambda i: (0, 0)),
+        ],
+        out_specs=[
+            pl.BlockSpec((tok_rows, 2 * lanes), lambda i: (0, i)),
+            pl.BlockSpec(gates_t.shape, lambda i: (0, 0)),
+            pl.BlockSpec((extra, lanes), lambda i: (0, 0)),
+        ],
+        out_shape=[
+            jax.ShapeDtypeStruct((tok_rows, half), BF16),
+            jax.ShapeDtypeStruct(gates_t.shape, F32),
+            jax.ShapeDtypeStruct((extra, lanes), F32),
+        ],
+        name="final",
+    )(payload, payload, select_t, s_own, s_peer, place, ids_t, gates_t)
 
 
 def silu_parts(pre):
@@ -56,30 +273,8 @@
     w_g, w_u, w_d = w_gate[0], w_up[0], w_down[0]
 
     ids_t = expert_ids.T
-    names = [ids_t[k][None, :] == jnp.arange(experts, dtype=jnp.int32)[:, None] for k in range(top)]
-    hit = names[0]
-    for name in names[1:]:
-        hit = hit | name
-    order = jnp.arange(tok_rows)
-    before = (order[:, None] < order[None, :]).astype(BF16)
-    rank = mm(hit.astype(BF16), before)
-    place = jnp.where(hit, rank, -1.0)
-    pick = place[:, None, :] == jnp.arange(cap, dtype=F32)[None, :, None]
-    select = pick.astype(BF16).reshape(slots, tok_rows)
     gates_t = gates.T
-    gate_of = sum(jnp.where(names[k], gates_t[k][None, :], 0.0) for k in range(top))
-    slot_gate = jnp.sum(jnp.where(pick, gate_of[:, None, :], 0.0), axis=2).reshape(slots)
-
-    both = jnp.concatenate(
-        [
-            lax.dynamic_slice_in_dim(tokens, own, half, 1),
-            lax.dynamic_slice_in_dim(cotangent, own, half, 1),
-        ],
-        axis=1,
-    )
-    is_cot = jnp.arange(width) >= half
-    scale = jnp.where(is_cot[None, :], slot_gate[:, None], 1.0)
-    sent = (mm(select, both) * scale).astype(BF16)
+    sent, place = routing(tp, ids_t, gates_t, tokens, cotangent, experts, cap)
     got = to_each(sent.reshape(experts, cap, width)).reshape(slots, width)
 
     s_hidden, s_gate, s_up, _ = to_hidden(tokens, cotangent, sh_gate, sh_up, sh_down)
@@ -97,6 +292,9 @@
     w_d_own = lax.dynamic_slice_in_dim(w_d, own, half, 1)
     w_d_other = lax.dynamic_slice_in_dim(w_d, other, half, 1)
 
+    slot = jnp.arange(slots, dtype=jnp.int32)
+    pick = place.T[:, :, None] == (slot[:cap].astype(F32))[None, None, :]
+    select_t = pick.astype(BF16).reshape(tok_rows, slots)
     peer = swap(got)
     pre = mm(got[:, :half], w_gu_own) + mm(peer[:, :half], w_gu_other)
     hidden_cot = mm(got[:, half:], w_d_own, COLS) + mm(peer[:, half:], w_d_other, COLS)
@@ -109,8 +307,16 @@
     rows_own = mm(d_both, w_gu_own, COLS).astype(BF16)
     from_peer = swap(rows_other)
     gate_peer = swap(gate_part)
-    slot_rows = (from_peer.astype(F32) + rows_own.astype(F32)).astype(BF16)
-    back_rows = to_each(slot_rows.reshape(experts, cap, half)).reshape(slots, half)
+    extra = 8
+    payload = payload_of(rows_own, from_peer, experts, extra)
+    gate_sum = jnp.pad((gate_part + gate_peer).reshape(experts, 1, cap), ((0, 0), (0, 0), (0, 128 - cap)))
+    high = lax.reduce_precision(gate_sum, 8, 7)
+    line = jnp.arange(extra)[None, :, None]
+    notes = jnp.where(line == 4, high, jnp.where(line == 5, gate_sum - high, 0.0))
+    shared_sum, payload = totals(shared_got, notes, payload)
+    back = to_each(payload)
+    shared_g, shared_u = shared_sum[:, :hid], shared_sum[:, hid : 2 * hid]
+    shared_d = shared_sum[:, 2 * hid :].T
 
     low = tp == 0
     inputs = jnp.concatenate(
@@ -124,19 +330,6 @@
     grad_g = mm(inputs, d_both[:, :hid], ROWS)
     grad_u = mm(inputs, d_both[:, hid:], ROWS)
     grad_d = mm(hidden, cots, ROWS)
-
-    shared_sum = jnp.sum(shared_got.astype(F32), axis=0)
-    shared_g, shared_u = shared_sum[:, :hid], shared_sum[:, hid : 2 * hid]
-    shared_d = shared_sum[:, 2 * hid :].T
-    down_part = jnp.sum(shared_d * shared_d, axis=1)
-    s_rows = s_peer.astype(F32) + s_own.astype(F32)
-    gate_sum = gate_part + gate_peer
-    small = jnp.concatenate(
-        [gate_sum.reshape(experts, cap), jnp.broadcast_to(down_part[None], (experts, hid))], axis=1
-    )
-    small = to_each(small)
-    back_gate = small[:, :cap]
-    down_norms = jnp.sum(small[:, cap:], axis=0)
 
     norms = jnp.concatenate(
         [
@@ -151,12 +344,10 @@
     gate_norms, up_norms = norms[:width], norms[width : 2 * width]
     shared_gate_norms, shared_up_norms = norms[2 * width : 2 * width + step], norms[2 * width + step :]
 
-    routed = mm(select, back_rows, ROWS)
-    token_grad = (routed + s_rows).astype(BF16)
-    gate_at = jnp.sum(jnp.where(pick, back_gate[:, :, None], 0.0), axis=1)
-    gate_grad = (
-        jnp.stack([jnp.sum(jnp.where(name, gate_at, 0.0), axis=0) for name in names], axis=1) / gates
-    )
+    token_grad, gate_grad, whole = finished(back, select_t, s_own, s_peer, place, ids_t, gates_t)
+    gate_grad = gate_grad.T
+    lines = hid // 128
+    down_norms = (whole[:lines] + whole[lines : 2 * lines]).reshape(hid)
     return (
         token_grad,
         gate_grad,

time: 230 us -> 239 us (1.039)
  Pallas kernels: 0 us -> 24.4 us
  starting transfers between devices: 21.3 us -> 14.3 us
  waiting for transfers between devices: 36.9 us -> 33.5 us
  other arithmetic: 17 us -> 13.7 us
    pallas_call x0 -> x4, Pallas kernels: none -> 24.4 us  [the longest x1 7.11 us: routing(): pl.pallas_call(routing_kernel, grid_spec=pltpu.PrefetchScalarGridSpec(num...]
    all_to_all x3 -> x2, starting transfers between devices: 20.7 us -> 13.1 us  [to_each(): return lax.all_to_all(x, 'ep', 0, 0, tiled=True)]
    reduce_sum x6 -> x0, other arithmetic: 4.35 us -> none  [the longest x1 2.35 us: layer(): shared_sum = jnp.sum(shared_got.astype(F32), axis=0)]
    eq x2 -> x4, local copies, waits for them, and re-layouts: 0.09 us -> 3.28 us  [layer(): pick = place.T[:, :, None] == slot[:cap].astype(F32)[None, None, :]]
    all_to_all x3 -> x2, waiting for transfers between devices: 36.4 us -> 33.5 us  [to_each(): return lax.all_to_all(x, 'ep', 0, 0, tiled=True)]
    dot_general x19 -> x16, matrix products: 50.3 us -> 48.9 us  [mm(): return lax.dot_general(a, b, contract, preferred_element_type=F32)]
    unnamed x42 -> x39, local copies, waits for them, and re-layouts: 5.11 us -> 6.16 us
  transfers between devices with their start and end apart: 8 -> 7, of which waited for: 4 -> 2; matrix products, arithmetic and copies ran while one was open for 31% -> 27% of each run, Pallas kernels for 0% -> 4%
where the time goes in v1:
time: 239 us; the launch traced here: 238 us
  blocking collectives  86.8 us (36%)
  matrix products  48.9 us (20%)
  waiting for transfers between devices  33.5 us (14%)
  Pallas kernels  24.4 us (10%)
  local copies, waits for them, and re-layouts  15.3 us (6%)
  starting transfers between devices  14.3 us (6%)
  other arithmetic  13.7 us (6%)
    all_to_all x1, blocking collectives, to_each(): return lax.all_to_all(x, 'ep', 0, 0, tiled=True)  86.8 us
    dot_general x16, matrix products, mm(): return lax.dot_general(a, b, contract, preferred_element_type=F32)  48.9 us
    all_to_all x2, waiting for transfers between devices, to_each(): return lax.all_to_all(x, 'ep', 0, 0, tiled=True)  33.5 us
    all_to_all x2, starting transfers between devices, to_each(): return lax.all_to_all(x, 'ep', 0, 0, tiled=True)  13.1 us
    select_n x1, other arithmetic, layer(): jnp.where(low, got[:, half:], peer[:, half:])  7.83 us
    pallas_call x1, Pallas kernels, routing(): pl.pallas_call(routing_kernel, grid_spec=pltpu.PrefetchScalarGridSpec(num...  7.11 us
    pallas_call x1, Pallas kernels, payload_of(): pl.pallas_call(payload_kernel, grid=(steps,), in_specs=[pl.BlockSpec((slo...  6.95 us
    pallas_call x1, Pallas kernels, finished(): pl.pallas_call(final_kernel, grid=(steps,), in_specs=[pl.BlockSpec((exper...  6.63 us
  transfers between devices with their start and end apart: 7, of which 2 were waited for; matrix products, arithmetic and copies ran while one was open for 27% of the time, Pallas kernels for 4%

profile of v1, /device:TPU:0, one launch (start us, length us, event | category | flops | bytes accessed | tf_op | source)
XLA Modules:
  0.0 237.9 jit_solution(3204651888801023310)
XLA Ops:
  0.7 7.1 %routing.1 = (bf16[1536,2048]{1,0:T(8,128)(2,1)}, f32[64,256]{1,0:T(8,128)}) custom-call(s32[1]{0:T(128)} %bitcast.4.tp_ref, s32[4,256]{1,0:T(4,128)} %bitcast.56, f32[4,256]{1,0:T(4,128)} %bitcast.58, bf16[256,2048]{1,0:T(8,128)(2,1)} %tok_ref.1, bf16[256,2048]{1,0:T(8,128)(2,1)} %cot_ref.1), custom_call_target="tpu_custom_call" | custom-call | tf_op jit(solution)/shard_map/routing/pallas_call | solution.py:74
  7.8 86.8 %all_to_all.15 = bf16[64,24,2048]{2,1,0:T(8,128)(2,1)} all-to-all(bf16[64,24,2048]{2,1,0:T(8,128)(2,1)} %bitcast.50), channel_id=1, replica_groups=mesh['ep'=64,'tp'=2] {'ep'}, dimensions={0} | all-to-all | bytes 12582912 | tf_op jit(solution)/shard_map/all_to_all | solution.py:25
  94.6 1.8 fusion.46
  96.5 1.8 fusion.45
  99.6 2.0 fusion.6
  101.6 3.9 %copy.30 = bf16[2048,512]{1,0:T(8,128)(2,1)} copy(bf16[2048,512]{0,1:T(8,128)(2,1)} %fusion.6) | data formatting | bytes 4194304 | tf_op jit(solution)/shard_map/dot_general | solution.py:17
  105.5 1.5 fusion.7
  107.6 3.0 %fusion.9 = f32[1536,256]{0,1:T(8,128)S(1)} fusion(bf16[1536,2048]{1,0:T(8,128)(2,1)} %bitcast.8, bf16[1,256,2048]{2,1,0:T(8,128)(2,1)S(1)} %copy-done, s32[]{:T(128)S(6)} %select_n.38), kind=kOutput, calls=%fused_computation.21 | convolution fusion | flops 805306368 | bytes 5242884 | tf_op jit(solution)/shard_map/dot_general | solution.py:17
  110.6 3.8 %fusion.12 = f32[1536,512]{0,1:T(8,128)S(1)} fusion(bf16[1536,2048]{1,0:T(8,128)(2,1)} %bitcast.8, s32[]{:T(128)S(6)} %select_n.38, bf16[2048,256]{1,0:T(8,128)(2,1)S(1)} %bitcast.63, bf16[2048,256]{1,0:T(8,128)(2,1)S(1)} %bitcast.67), kind=kOutput, calls=%fused_computation.24 | convolution fusion | flops 1612709888 | bytes 8388612 | tf_op jit(solution)/shard_map/dot_general | solution.py:17
  114.5 3.8 %convolution_add_fusion = f32[1536,512]{0,1:T(8,128)S(1)} fusion(f32[1536,512]{0,1:T(8,128)S(1)} %fusion.12, bf16[1536,2048]{1,0:T(8,128)(2,1)} %collective-permute-done, s32[]{:T(128)S(6)} %select_n.39, bf16[2048,256]{1,0:T(8,128)(2,1)S(1)} %bitcast.64, bf16[2048,256]{1,0:T(8,128)(2,1)S(1)} %bitcast.68), kind=kOutput, calls=%fused_computation.9 | convolution fusion | flops 1613496320 | bytes 11534340 | tf_op jit(solution)/shard_map/dot_general | solution.py:17
  118.3 4.5 %multiply_convert_fusion.1 = (bf16[1536,256]{0,1:T(8,128)(2,1)S(1)}, bf16[1536,256]{0,1:T(8,128)(2,1)S(1)}, f32[1536]{0:T(1024)S(1)}, bf16[1536,256]{0,1:T(8,128)(2,1)}) fusion(f32[1536,512]{0,1:T(8,128)S(1)} %convolution_add_fusion, f32[1536,256]{0,1:T(8,128)S(1)} %fusion.9, bf16[1,256,2048]{2,1,0:T(8,128)(2,1)S(1)} %copy-done, s32[]{:T(128)S(6)} %select_n.39, ...), kind=kOutput, calls=%fused_computation.35 | convolution fusion | flops 812775936 | bytes 10754052 | tf_op jit(solution)/shard_map/dot_general | solution.py:17
  122.8 3.5 %convolution_convert_fusion = bf16[1536,1024]{1,0:T(8,128)(2,1)} fusion(bf16[1536,256]{0,1:T(8,128)(2,1)S(1)} %get-tuple-element.67, bf16[1536,256]{0,1:T(8,128)(2,1)S(1)} %get-tuple-element.66, s32[]{:T(128)S(6)} %select_n.39, bf16[2048,256]{1,0:T(8,128)(2,1)S(1)} %bitcast.65, bf16[2048,256]{1,0:T(8,128)(2,1)S(1)} %bitcast.69), kind=kOutput, calls=%fused_computation.7 | convolution fusion | flops 1617428480 | bytes 6815748 | tf_op jit(solution)/shard_map/dot_general | solution.py:17
  126.8 1.9 pad_maximum_fusion.3
  128.8 6.4 %all-to-all-start = ((bf16[64,32,768]{2,1,0:T(8,128)(2,1)}), bf16[64,32,768]{2,1,0:T(8,128)(2,1)}, u32[]{:S(2)}, u32[]{:S(2)}) async-start(bf16[64,32,768]{2,1,0:T(8,128)(2,1)} %pad_maximum_fusion.3), calls=%async_computation | async-start | bytes 6291456 | tf_op jit(solution)/shard_map/all_to_all | solution.py:25
  135.4 1.3 copy-done.5
  136.7 1.3 convolution_convert_fusion.4
  139.2 1.9 copy.32
  141.3 2.5 %convolution_convert_fusion.5.own_ref = bf16[256,1024]{1,0:T(8,128)(2,1)} fusion(bf16[2048,512]{1,0:T(8,128)(2,1)} %copy-done.5, s32[]{:T(128)S(6)} %select_n.38, bf16[256,256]{0,1:T(8,128)(2,1)S(1)} %get-tuple-element.71, bf16[256,256]{0,1:T(8,128)(2,1)S(1)} %get-tuple-element.70), kind=kOutput, calls=%fused_computation.42 | convolution fusion | flops 269221888 | bytes 1835012 | tf_op jit(solution)/shard_map/dot_general | solution.py:17
  145.3 5.0 %convolution_convert_fusion.1.own_ref = bf16[1536,1024]{1,0:T(8,128)(2,1)} fusion(bf16[1536,256]{0,1:T(8,128)(2,1)} %copy-done.16, bf16[1536,256]{0,1:T(8,128)(2,1)S(1)} %copy-done.15, s32[]{:T(128)S(6)} %select_n.38, bf16[2048,256]{1,0:T(8,128)(2,1)} %bitcast.62, bf16[2048,256]{1,0:T(8,128)(2,1)} %bitcast.66), kind=kOutput, calls=%fused_computation.8 | convolution fusion | flops 1617428480 | bytes 6815748 | tf_op jit(solution)/shard_map/dot_general | solution.py:17
  151.3 6.9 %payload.1.payload_ref = bf16[64,200,128]{2,1,0:T(8,128)(2,1)} custom-call(bf16[1536,1024]{1,0:T(8,128)(2,1)} %convolution_convert_fusion.1.own_ref, bf16[1536,1024]{1,0:T(8,128)(2,1)} %collective-permute-done.2.peer_ref), custom_call_target="tpu_custom_call" | custom-call | tf_op jit(solution)/shard_map/payload/pallas_call | solution.py:115
  158.2 18.5 %all-to-all-done.got_ref = bf16[64,32,768]{2,1,0:T(8,128)(2,1)} async-done(((bf16[64,32,768]{2,1,0:T(8,128)(2,1)}), bf16[64,32,768]{2,1,0:T(8,128)(2,1)}, u32[]{:S(2)}, u32[]{:S(2)}) %all-to-all-start) | async-done | bytes 3145760 | tf_op jit(solution)/shard_map/all_to_all | solution.py:25
  176.8 3.7 %totals.1 = (f32[32,768]{1,0:T(8,128)}, bf16[64,200,128]{2,1,0:T(8,128)(2,1)}) custom-call(bf16[64,32,768]{2,1,0:T(8,128)(2,1)} %all-to-all-done.got_ref, f32[64,8,128]{2,1,0:T(8,128)} %select_select_fusion.notes_ref, bf16[64,200,128]{2,1,0:T(8,128)(2,1)} %payload.1.payload_ref), custom_call_target="tpu_custom_call", output_to_operand_aliasing={{1}: (2, {})} | custom-call | tf_op jit(solution)/shard_map/totals/pallas_call | solution.py:161
  180.5 6.7 %all-to-all-start.2 = ((bf16[64,200,128]{2,1,0:T(8,128)(2,1)}), bf16[64,200,128]{2,1,0:T(8,128)(2,1)}, u32[]{:S(2)}, u32[]{:S(2)}) async-start(bf16[64,200,128]{2,1,0:T(8,128)(2,1)} %get-tuple-element.22), calls=%async_computation.2 | async-start | bytes 6553600 | tf_op jit(solution)/shard_map/all_to_all | solution.py:25
  187.2 7.8 %broadcast_select_fusion.1 = (bf16[1536,1024]{1,0:T(8,128)(2,1)}, bf16[1536,1024]{1,0:T(8,128)(2,1)S(1)}, bf16[1536,1024]{1,0:T(8,128)(2,1)}, bf16[1536,1024]{1,0:T(8,128)(2,1)S(1)}) fusion(pred[]{:T(512)S(6)} %eq.47, bf16[1536,2048]{1,0:T(8,128)(2,1)} %collective-permute-done, bf16[1536,2048]{1,0:T(8,128)(2,1)} %bitcast.8), kind=kLoop, calls=%fused_computation.12 | loop fusion | flops 6291456 | bytes 25165824 | tf_op jit(solution)/shard_map/jit(_where)/select_n | solution.py:327
  195.1 1.8 multiply_reduce_fusion.1
  196.9 4.4 %multiply_reduce_fusion.2 = (f32[2048]{0:T(1024)S(1)}, f32[2048,256]{0,1:T(8,128)}) fusion(bf16[1536,256]{0,1:T(8,128)(2,1)S(1)} %copy-done.15, bf16[1536,1024]{1,0:T(8,128)(2,1)S(1)} %get-tuple-element.63, bf16[1536,1024]{1,0:T(8,128)(2,1)S(1)} %get-tuple-element.65), kind=kOutput, calls=%fused_computation.32 | convolution fusion | flops 1624242176 | bytes 9183232 | tf_op jit(solution)/shard_map/dot_general | solution.py:17
  202.4 6.8 %multiply_reduce_fusion = (f32[256]{0:T(256)}, f32[256,2048]{1,0:T(8,128)}) fusion(bf16[1536,256]{0,1:T(8,128)(2,1)} %get-tuple-element.69, bf16[1536,1024]{1,0:T(8,128)(2,1)} %get-tuple-element.64, bf16[1536,1024]{1,0:T(8,128)(2,1)} %get-tuple-element.62), kind=kOutput, calls=%fused_computation.30 | convolution fusion | flops 1624243968 | bytes 9176064 | tf_op jit(solution)/shard_map/dot_general | solution.py:17
  209.1 1.8 copy.34
  210.9 2.9 %copy.33 = f32[1,2048,256]{2,1,0:T(8,128)} copy(f32[1,2048,256]{1,2,0:T(8,128)} %bitcast.54) | data formatting | bytes 4194304
  215.0 15.0 %all-to-all-done.2.rows_ref.notes_ref = bf16[64,200,128]{2,1,0:T(8,128)(2,1)} async-done(((bf16[64,200,128]{2,1,0:T(8,128)(2,1)}), bf16[64,200,128]{2,1,0:T(8,128)(2,1)}, u32[]{:S(2)}, u32[]{:S(2)}) %all-to-all-start.2) | async-done | bytes 3276832 | tf_op jit(solution)/shard_map/all_to_all | solution.py:25
  230.0 6.6 %final.1 = (bf16[256,1024]{1,0:T(8,128)(2,1)}, f32[4,256]{1,0:T(4,128)}, f32[8,128]{1,0:T(8,128)}) custom-call(bf16[64,200,128]{2,1,0:T(8,128)(2,1)} %all-to-all-done.2.rows_ref.notes_ref, bf16[64,200,128]{2,1,0:T(8,128)(2,1)} %all-to-all-done.2.rows_ref.notes_ref, bf16[256,1536]{1,0:T(8,128)(2,1)} %compare_convert_fusion.select_ref, ...), custom_call_target="tpu_custom_call" | custom-call | tf_op jit(solution)/shard_map/final/pallas_call | solution.py:216
  236.6 1.3 add_bitcast_fusion
  (64 shorter events, 8.6 us)
Async XLA Ops:
  0.6 106.9 %copy-start = (bf16[1,256,2048]{2,1,0:T(8,128)(2,1)S(1)}, bf16[1,256,2048]{2,1,0:T(8,128)(2,1)}, u32[]{:S(2)}) copy-start(bf16[1,256,2048]{2,1,0:T(8,128)(2,1)} %param.16) | copy-start | bytes 3145732
  7.8 86.8 %copy-start.2 = (bf16[256,2048]{1,0:T(8,128)(2,1)S(1)}, bf16[256,2048]{1,0:T(8,128)(2,1)}, u32[]{:S(2)}) copy-start(bf16[256,2048]{1,0:T(8,128)(2,1)} %tok_ref.1) | copy-start | bytes 3145732
  7.8 88.7 %copy-start.3 = (bf16[256,2048]{1,0:T(8,128)(2,1)S(1)}, bf16[256,2048]{1,0:T(8,128)(2,1)}, u32[]{:S(2)}) copy-start(bf16[256,2048]{1,0:T(8,128)(2,1)} %cot_ref.1) | copy-start | bytes 3145732
  94.6 19.9 %collective-permute-start = (bf16[1536,2048]{1,0:T(8,128)(2,1)}, bf16[1536,2048]{1,0:T(8,128)(2,1)}, u32[]{:S(2)}, u32[]{:S(2)}) collective-permute-start(bf16[1536,2048]{1,0:T(8,128)(2,1)} %bitcast.8), channel_id=1, source_target_pairs={{0,1},{1,0},{2,3},{3,2},{4,5},{5,4},{6,7},{7,6},{8,9},{9,8},{10,11... | collective-permute-start | bytes 18874376 | tf_op jit(solution)/shard_map/ppermute | solution.py:21
  94.6 3.7 %copy-start.8 = (bf16[2048,256]{1,0:T(8,128)(2,1)S(1)}, bf16[2048,256]{1,0:T(8,128)(2,1)}, u32[]{:S(2)}) copy-start(bf16[2048,256]{1,0:T(8,128)(2,1)} %param.17) | copy-start | bytes 3145732
  96.4 1.8 copy-start.7
  107.5 3.1 %copy-start.12 = (bf16[1,2048,256]{2,1,0:T(8,128)(2,1)S(1)}, bf16[1,2048,256]{2,1,0:T(8,128)(2,1)}, u32[]{:S(2)}) copy-start(bf16[1,2048,256]{2,1,0:T(8,128)(2,1)} %param.14) | copy-start | bytes 3145732
  107.5 3.1 %copy-start.13 = (bf16[1,2048,256]{2,1,0:T(8,128)(2,1)S(1)}, bf16[1,2048,256]{2,1,0:T(8,128)(2,1)}, u32[]{:S(2)}) copy-start(bf16[1,2048,256]{2,1,0:T(8,128)(2,1)} %param.15) | copy-start | bytes 3145732
  122.8 3.5 %copy-start.14 = (bf16[1536,256]{0,1:T(8,128)(2,1)}, bf16[1536,256]{0,1:T(8,128)(2,1)S(1)}, u32[]{:S(2)}) copy-start(bf16[1536,256]{0,1:T(8,128)(2,1)S(1)} %get-tuple-element.66) | copy-start | bytes 2359300
  122.8 3.5 %copy-start.16 = (bf16[1536,256]{0,1:T(8,128)(2,1)}, bf16[1536,256]{0,1:T(8,128)(2,1)S(1)}, u32[]{:S(2)}) copy-start(bf16[1536,256]{0,1:T(8,128)(2,1)S(1)} %get-tuple-element.67) | copy-start | bytes 2359300
  122.8 4.0 %copy-start.4 = (bf16[2048,512]{1,0:T(8,128)(2,1)S(1)}, bf16[2048,512]{1,0:T(8,128)(2,1)}, u32[]{:S(2)}) copy-start(bf16[2048,512]{1,0:T(8,128)(2,1)} %copy.30) | copy-start | bytes 6291460
  126.3 24.9 %collective-permute-start.2 = (bf16[1536,1024]{1,0:T(8,128)(2,1)}, bf16[1536,1024]{1,0:T(8,128)(2,1)}, u32[]{:S(2)}, u32[]{:S(2)}) collective-permute-start(bf16[1536,1024]{1,0:T(8,128)(2,1)} %convolution_convert_fusion), channel_id=1, source_target_pairs={{0,1},{1,0},{2,3},{3,2},{4,5},{5,4},{6,7},{7,6},{8,9},{9,8},{10,11... | collective-permute-start | bytes 9437192 | tf_op jit(solution)/shard_map/ppermute | solution.py:21
  128.8 6.4 %copy-start.9 = (bf16[2048,256]{1,0:T(8,128)(2,1)S(1)}, bf16[2048,256]{1,0:T(8,128)(2,1)}, u32[]{:S(2)}) copy-start(bf16[2048,256]{1,0:T(8,128)(2,1)} %param.17) | copy-start | bytes 3145732
  128.8 6.5 %copy-start.6 = (bf16[2048,256]{1,0:T(8,128)(2,1)S(1)}, bf16[2048,256]{1,0:T(8,128)(2,1)}, u32[]{:S(2)}) copy-start(bf16[2048,256]{1,0:T(8,128)(2,1)} %param.18) | copy-start | bytes 3145732
  128.8 48.0 %all-to-all-start = ((bf16[64,32,768]{2,1,0:T(8,128)(2,1)}), bf16[64,32,768]{2,1,0:T(8,128)(2,1)}, u32[]{:S(2)}, u32[]{:S(2)}) async-start(bf16[64,32,768]{2,1,0:T(8,128)(2,1)} %pad_maximum_fusion.3), calls=%async_computation | async-start | bytes 6291456 | tf_op jit(solution)/shard_map/all_to_all | solution.py:25
  135.2 2.8 %copy-start.10 = (f32[64,256]{1,0:T(8,128)S(1)}, f32[64,256]{1,0:T(8,128)}, u32[]{:S(2)}) copy-start(f32[64,256]{1,0:T(8,128)} %get-tuple-element.23.place_ref) | copy-start | bytes 196612
  135.3 1.3 copy-start.5
  137.9 77.1 %collective-permute-start.3 = (bf16[256,1024]{1,0:T(8,128)(2,1)}, bf16[256,1024]{1,0:T(8,128)(2,1)}, u32[]{:S(2)}, u32[]{:S(2)}) collective-permute-start(bf16[256,1024]{1,0:T(8,128)(2,1)} %convolution_convert_fusion.4), channel_id=1, source_target_pairs={{0,1},{1,0},{2,3},{3,2},{4,5},{5,4},{6,7},{7,6},{8,9},{9,8},{10,11... | collective-permute-start | bytes 1572872 | tf_op jit(solution)/shard_map/ppermute | solution.py:21
  139.2 6.1 %copy-start.15 = (bf16[1536,256]{0,1:T(8,128)(2,1)S(1)}, bf16[1536,256]{0,1:T(8,128)(2,1)}, u32[]{:S(2)}) copy-start(bf16[1536,256]{0,1:T(8,128)(2,1)} %copy-done.14) | copy-start | bytes 2359300
  144.8 5.5 %collective-permute-start.1 = (f32[1536]{0:T(1024)S(1)}, f32[1536]{0:T(1024)S(1)}, u32[]{:S(2)}, u32[]{:S(2)}) collective-permute-start(f32[1536]{0:T(1024)S(1)} %get-tuple-element.68), channel_id=1, source_target_pairs={{0,1},{1,0},{2,3},{3,2},{4,5},{5,4},{6,7},{7,6},{8,9},{9,8},{10,11... | collective-permute-start | bytes 18440 | tf_op jit(solution)/shard_map/ppermute | solution.py:21
  180.5 49.5 %all-to-all-start.2 = ((bf16[64,200,128]{2,1,0:T(8,128)(2,1)}), bf16[64,200,128]{2,1,0:T(8,128)(2,1)}, u32[]{:S(2)}, u32[]{:S(2)}) async-start(bf16[64,200,128]{2,1,0:T(8,128)(2,1)} %get-tuple-element.22), calls=%async_computation.2 | async-start | bytes 6553600 | tf_op jit(solution)/shard_map/all_to_all | solution.py:25
  187.2 7.8 %copy-start.17 = (bf16[1536,256]{0,1:T(8,128)(2,1)S(1)}, bf16[1536,256]{0,1:T(8,128)(2,1)}, u32[]{:S(2)}) copy-start(bf16[1536,256]{0,1:T(8,128)(2,1)} %copy-done.16) | copy-start | bytes 2359300
  196.9 4.4 %copy-start.11 = (f32[32,768]{1,0:T(8,128)S(1)}, f32[32,768]{1,0:T(8,128)}, u32[]{:S(2)}) copy-start(f32[32,768]{1,0:T(8,128)} %get-tuple-element.26) | copy-start | bytes 294916
  202.1 11.7 %collective-permute-start.4 = (f32[4160]{0:T(1024)S(1)}, f32[4160]{0:T(1024)S(1)}, u32[]{:S(2)}, u32[]{:S(2)}) collective-permute-start(f32[4160]{0:T(1024)S(1)} %concatenate.40), channel_id=1, source_target_pairs={{0,1},{1,0},{2,3},{3,2},{4,5},{5,4},{6,7},{7,6},{8,9},{9,8},{10,11... | collective-permute-start | bytes 49928 | tf_op jit(solution)/shard_map/ppermute | solution.py:21
  214.4 23.5 %copy-start.1 = (bf16[1,256,2048]{2,1,0:T(8,128)(2,1)S(1)}, bf16[1,256,2048]{2,1,0:T(8,128)(2,1)}, u32[]{:S(2)}) copy-start(bf16[1,256,2048]{2,1,0:T(8,128)(2,1)} %param.16) | copy-start | bytes 3145732

commit v2 on v1

--- a/solution.py
+++ b/solution.py
@@ -11,6 +11,7 @@
 ROWS = (((0,), (0,)), ((), ()))
 COLS = (((1,), (1,)), ((), ()))
 PLAIN = (((1,), (0,)), ((), ()))
+SIDE = 4
 
 
 def mm(a, b, contract=PLAIN):
@@ -69,7 +70,7 @@
     tok_rows, width = tokens.shape
     half = width // 2
     top = ids_t.shape[0]
-    steps = 8
+    steps = 4
     rows = experts * cap // steps
     return pl.pallas_call(
         routing_kernel,
@@ -155,7 +156,7 @@
 
 def totals(got, notes, payload):
     size, rows, cols = got.shape
-    steps = 4
+    steps = 2
     experts, extra, lanes = notes.shape
     last = payload.shape[1] // extra - 1
     return pl.pallas_call(
@@ -193,7 +194,7 @@
     def _():
         notes = notes_ref[...].astype(F32)
         whole = jnp.sum(notes, axis=0)
-        down_ref[...] = whole
+        down_ref[...] = jnp.concatenate([whole[0:1] + whole[2:3], whole[1:2] + whole[3:4]], axis=1)
         row = lax.broadcasted_iota(jnp.int32, notes.shape, 1)
         gate = jnp.sum(jnp.where((row == 4) | (row == 5), notes, 0.0), axis=1)
         place = place_ref[...]
@@ -229,15 +230,20 @@
         out_specs=[
             pl.BlockSpec((tok_rows, 2 * lanes), lambda i: (0, i)),
             pl.BlockSpec(gates_t.shape, lambda i: (0, 0)),
-            pl.BlockSpec((extra, lanes), lambda i: (0, 0)),
+            pl.BlockSpec((1, 2 * lanes), lambda i: (0, 0)),
         ],
         out_shape=[
             jax.ShapeDtypeStruct((tok_rows, half), BF16),
             jax.ShapeDtypeStruct(gates_t.shape, F32),
-            jax.ShapeDtypeStruct((extra, lanes), F32),
+            jax.ShapeDtypeStruct((1, 2 * lanes), F32),
         ],
         name="final",
     )(payload, payload, select_t, s_own, s_peer, place, ids_t, gates_t)
+
+
+def next_along(x, by):
+    size = lax.axis_size("ep")
+    return lax.ppermute(x, "ep", [(i, (i + by * (size // SIDE)) % size) for i in range(size)])
 
 
 def silu_parts(pre):
@@ -284,7 +290,19 @@
     s_other = input_rows(s_d, s_both, other, half)
     s_own = input_rows(s_d, s_both, own, half)
     shared = jnp.concatenate([mm(tokens, s_d, ROWS), mm(cotangent, s_hidden, ROWS)], axis=1).astype(BF16)
-    shared_got = to_each(shared.reshape(experts, width // experts, 3 * hid))
+    plane = experts // SIDE
+    z = lax.div(lax.axis_index("ep"), plane)
+    part = width // SIDE
+    pieces = [
+        lax.dynamic_slice_in_dim(shared, lax.rem(z + by, SIDE) * part, part, 0) for by in range(SIDE)
+    ]
+    arrived = [next_along(pieces[by], by) for by in range(1, SIDE)]
+    terms = pieces[0].astype(F32)
+    for piece in arrived:
+        terms = terms + piece.astype(F32)
+    terms = terms.astype(BF16).reshape(plane, width // experts, 3 * hid)
+    groups = [list(range(i, i + plane)) for i in range(0, experts, plane)]
+    shared_got = lax.all_to_all(terms, "ep", 0, 0, tiled=True, axis_index_groups=groups)
     s_peer = swap(s_other)
     w_gu = jnp.concatenate([w_g, w_u], axis=1)
     w_gu_own = lax.dynamic_slice_in_dim(w_gu, own, half, 0)
@@ -344,10 +362,9 @@
     gate_norms, up_norms = norms[:width], norms[width : 2 * width]
     shared_gate_norms, shared_up_norms = norms[2 * width : 2 * width + step], norms[2 * width + step :]
 
-    token_grad, gate_grad, whole = finished(back, select_t, s_own, s_peer, place, ids_t, gates_t)
+    token_grad, gate_grad, down_norms = finished(back, select_t, s_own, s_peer, place, ids_t, gates_t)
     gate_grad = gate_grad.T
-    lines = hid // 128
-    down_norms = (whole[:lines] + whole[lines : 2 * lines]).reshape(hid)
+    down_norms = down_norms.reshape(hid)
     return (
         token_grad,
         gate_grad,

time: 239 us -> 246 us (1.029)
  waiting for transfers between devices: 33.5 us -> 43.8 us
  matrix products: 48.9 us -> 43.7 us
  Pallas kernels: 24.4 us -> 21.5 us
  other arithmetic: 13.7 us -> 16.4 us
    ppermute x0 -> x3, waiting for transfers between devices: none -> 26.8 us  [next_along(): lax.ppermute(x, 'ep', [(i, (i + by * (size // SIDE)) % size) for i in ran...]
    all_to_all x2 -> x1, waiting for transfers between devices: 33.5 us -> 16.2 us  [to_each(): return lax.all_to_all(x, 'ep', 0, 0, tiled=True)]
    dot_general x16, matrix products: 48.9 us -> 43.7 us  [mm(): return lax.dot_general(a, b, contract, preferred_element_type=F32)]
    dot_general x2 -> x0, local copies, waits for them, and re-layouts: 4.44 us -> none  [mm(): return lax.dot_general(a, b, contract, preferred_element_type=F32)]
    all_to_all x2 -> x1, starting transfers between devices: 13.1 us -> 8.69 us  [to_each(): return lax.all_to_all(x, 'ep', 0, 0, tiled=True)]
    ppermute x0 -> x3, starting transfers between devices: none -> 3.78 us  [next_along(): lax.ppermute(x, 'ep', [(i, (i + by * (size // SIDE)) % size) for i in ran...]
    all_to_all x0 -> x1, starting transfers between devices: none -> 3.61 us  [layer(): lax.all_to_all(terms, 'ep', 0, 0, tiled=True, axis_index_groups=groups)]
    convert_element_type x0 -> x1, other arithmetic: none -> 2.99 us  [layer(): terms = terms.astype(BF16).reshape(plane, width // experts, 3 * hid)]
  transfers between devices with their start and end apart: 7 -> 10, of which waited for: 2 -> 5; matrix products, arithmetic and copies ran while one was open for 27% -> 25% of each run, Pallas kernels for 4% -> 4%
where the time goes in v2:
time: 246 us
  blocking collectives  86.8 us (35%)
  waiting for transfers between devices  43.8 us (18%)
  matrix products  43.7 us (18%)
  Pallas kernels  21.5 us (9%)
  starting transfers between devices  16.5 us (7%)
  other arithmetic  16.4 us (7%)
  local copies, waits for them, and re-layouts  15.9 us (6%)
    all_to_all x1, blocking collectives, to_each(): return lax.all_to_all(x, 'ep', 0, 0, tiled=True)  86.8 us
    dot_general x16, matrix products, mm(): return lax.dot_general(a, b, contract, preferred_element_type=F32)  43.7 us
    ppermute x3, waiting for transfers between devices, next_along(): lax.ppermute(x, 'ep', [(i, (i + by * (size // SIDE)) % size) for i in ran...  26.8 us
    all_to_all x1, waiting for transfers between devices, to_each(): return lax.all_to_all(x, 'ep', 0, 0, tiled=True)  16.2 us
    all_to_all x1, starting transfers between devices, to_each(): return lax.all_to_all(x, 'ep', 0, 0, tiled=True)  8.69 us
    select_n x1, other arithmetic, layer(): jnp.where(low, got[:, half:], peer[:, half:])  7.89 us
    unnamed x39, local copies, waits for them, and re-layouts  7.64 us
    pallas_call x1, Pallas kernels, payload_of(): pl.pallas_call(payload_kernel, grid=(steps,), in_specs=[pl.BlockSpec((slo...  6.95 us
  transfers between devices with their start and end apart: 10, of which 5 were waited for; matrix products, arithmetic and copies ran while one was open for 25% of the time, Pallas kernels for 4%

profile of v2, /device:TPU:0, one launch (start us, length us, event | category | flops | bytes accessed | tf_op | source)
XLA Modules:
  0.0 245.5 jit_solution(17448975703480562610)
XLA Ops:
  0.7 5.8 %routing.1 = (bf16[1536,2048]{1,0:T(8,128)(2,1)}, f32[64,256]{1,0:T(8,128)}) custom-call(s32[1]{0:T(128)} %bitcast.3.tp_ref, s32[4,256]{1,0:T(4,128)} %bitcast.52, f32[4,256]{1,0:T(4,128)} %bitcast.54, bf16[256,2048]{1,0:T(8,128)(2,1)} %tok_ref.1, bf16[256,2048]{1,0:T(8,128)(2,1)} %cot_ref.1), custom_call_target="tpu_custom_call" | custom-call | tf_op jit(solution)/shard_map/routing/pallas_call | solution.py:75
  6.4 86.8 %all_to_all.15 = bf16[64,24,2048]{2,1,0:T(8,128)(2,1)} all-to-all(bf16[64,24,2048]{2,1,0:T(8,128)(2,1)} %bitcast.47), channel_id=1, replica_groups=mesh['ep'=64,'tp'=2] {'ep'}, dimensions={0} | all-to-all | bytes 12582912 | tf_op jit(solution)/shard_map/all_to_all | solution.py:26
  93.3 1.9 fusion.49
  96.3 3.1 %fusion.9 = f32[1536,256]{0,1:T(8,128)S(1)} fusion(bf16[1536,2048]{1,0:T(8,128)(2,1)} %bitcast.7, bf16[1,256,2048]{2,1,0:T(8,128)(2,1)S(1)} %copy-done, s32[]{:T(128)S(6)} %select_n.54), kind=kOutput, calls=%fused_computation.28 | convolution fusion | flops 805306368 | bytes 5242884 | tf_op jit(solution)/shard_map/dot_general | solution.py:18
  99.4 3.8 %fusion.12 = f32[1536,512]{0,1:T(8,128)S(1)} fusion(bf16[1536,2048]{1,0:T(8,128)(2,1)} %bitcast.7, s32[]{:T(128)S(6)} %select_n.54, bf16[2048,256]{1,0:T(8,128)(2,1)S(1)} %bitcast.59, bf16[2048,256]{1,0:T(8,128)(2,1)S(1)} %bitcast.63), kind=kOutput, calls=%fused_computation.31 | convolution fusion | flops 1612709888 | bytes 8388612 | tf_op jit(solution)/shard_map/dot_general | solution.py:18
  103.7 3.8 %convolution_add_fusion = f32[1536,512]{0,1:T(8,128)S(1)} fusion(f32[1536,512]{0,1:T(8,128)S(1)} %fusion.12, bf16[1536,2048]{1,0:T(8,128)(2,1)} %collective-permute-done.3, s32[]{:T(128)S(6)} %select_n.55, bf16[2048,256]{1,0:T(8,128)(2,1)S(1)} %bitcast.60, bf16[2048,256]{1,0:T(8,128)(2,1)S(1)} %bitcast.64), kind=kOutput, calls=%fused_computation.17 | convolution fusion | flops 1613496320 | bytes 11534340 | tf_op jit(solution)/shard_map/dot_general | solution.py:18
  107.5 4.6 %multiply_convert_fusion.1 = (bf16[1536,256]{0,1:T(8,128)(2,1)S(1)}, bf16[1536,256]{0,1:T(8,128)(2,1)S(1)}, f32[1536]{0:T(1024)S(1)}, bf16[1536,256]{0,1:T(8,128)(2,1)}) fusion(f32[1536,512]{0,1:T(8,128)S(1)} %convolution_add_fusion, f32[1536,256]{0,1:T(8,128)S(1)} %fusion.9, bf16[1,256,2048]{2,1,0:T(8,128)(2,1)S(1)} %copy-done, s32[]{:T(128)S(6)} %select_n.55, ...), kind=kOutput, calls=%fused_computation.42 | convolution fusion | flops 812775936 | bytes 10754052 | tf_op jit(solution)/shard_map/dot_general | solution.py:18
  112.1 3.5 %convolution_convert_fusion = bf16[1536,1024]{1,0:T(8,128)(2,1)} fusion(bf16[1536,256]{0,1:T(8,128)(2,1)S(1)} %get-tuple-element.67, bf16[1536,256]{0,1:T(8,128)(2,1)S(1)} %get-tuple-element.66, s32[]{:T(128)S(6)} %select_n.55, bf16[2048,256]{1,0:T(8,128)(2,1)S(1)} %bitcast.61, bf16[2048,256]{1,0:T(8,128)(2,1)S(1)} %bitcast.65), kind=kOutput, calls=%fused_computation.11 | convolution fusion | flops 1617428480 | bytes 6815748 | tf_op jit(solution)/shard_map/dot_general | solution.py:18
  117.6 1.5 fusion.21
  119.0 2.2 collective-permute-start.2
  123.0 1.3 copy-done.5
  124.3 1.3 convolution_convert_fusion.4
  126.9 3.0 %copy.30 = f32[256,1536]{1,0:T(8,128)} copy(f32[256,1536]{0,1:T(8,128)} %bitcast.48) | data formatting | bytes 3145728 | tf_op jit(solution)/shard_map/eq | solution.py:314
  130.0 2.4 compare_convert_fusion.select_ref
  132.4 23.1 %collective-permute-done.2 = bf16[512,768]{0,1:T(8,128)(2,1)} collective-permute-done((bf16[512,768]{0,1:T(8,128)(2,1)}, bf16[512,768]{0,1:T(8,128)(2,1)}, u32[]{:S(2)}, u32[]{:S(2)}) %collective-permute-start.2) | collective-permute-done | bytes 786464 | tf_op jit(solution)/shard_map/ppermute | solution.py:246
  155.5 3.7 %collective-permute-done = bf16[512,768]{0,1:T(8,128)(2,1)} collective-permute-done((bf16[512,768]{0,1:T(8,128)(2,1)}, bf16[512,768]{0,1:T(8,128)(2,1)}, u32[]{:S(2)}, u32[]{:S(2)}) %collective-permute-start) | collective-permute-done | bytes 786464 | tf_op jit(solution)/shard_map/ppermute | solution.py:246
  159.2 3.0 %add_convert_fusion = bf16[512,768]{0,1:T(8,128)(2,1)} fusion(bf16[512,768]{0,1:T(8,128)(2,1)} %collective-permute-done.2, bf16[512,768]{0,1:T(8,128)(2,1)} %collective-permute-done.1, bf16[512,768]{0,1:T(8,128)(2,1)} %collective-permute-done, s32[]{:T(128)S(6)} %select_n.50, bf16[2048,512]{0,1:T(8,128)(2,1)S(1)} %fusion.6, bf16[2048,256]{0,1:T(8,128)(2,1)S(1)} %fusion.7), kind=kLoop, calls=%fused_computation.47 | loop fusion | flops 4325376 | bytes 6291460 | tf_op jit(solution)/shard_map/convert_element_type | solution.py:303
  162.2 2.4 copy.29
  164.6 3.6 %all-to-all-start = ((bf16[16,32,768]{2,1,0:T(8,128)(2,1)}), bf16[16,32,768]{2,1,0:T(8,128)(2,1)S(1)}, u32[]{:S(2)}, u32[]{:S(2)}) async-start(bf16[16,32,768]{2,1,0:T(8,128)(2,1)} %bitcast.2), calls=%async_computation | async-start | bytes 1572864 | tf_op jit(solution)/shard_map/all_to_all | solution.py:305
  168.3 1.3 convolution_convert_fusion.5.own_ref
  169.6 5.2 %convolution_convert_fusion.1.own_ref = bf16[1536,1024]{1,0:T(8,128)(2,1)} fusion(bf16[1536,256]{0,1:T(8,128)(2,1)} %copy-done.14, bf16[1536,256]{0,1:T(8,128)(2,1)} %copy-done.16, s32[]{:T(128)S(6)} %select_n.54, bf16[2048,256]{1,0:T(8,128)(2,1)} %bitcast.58, bf16[2048,256]{1,0:T(8,128)(2,1)} %bitcast.62), kind=kOutput, calls=%fused_computation.12 | convolution fusion | flops 1617428480 | bytes 6815748 | tf_op jit(solution)/shard_map/dot_general | solution.py:18
  175.7 7.0 %payload.1.payload_ref = bf16[64,200,128]{2,1,0:T(8,128)(2,1)} custom-call(bf16[1536,1024]{1,0:T(8,128)(2,1)} %convolution_convert_fusion.1.own_ref, bf16[1536,1024]{1,0:T(8,128)(2,1)} %collective-permute-done.5.peer_ref), custom_call_target="tpu_custom_call" | custom-call | tf_op jit(solution)/shard_map/payload/pallas_call | solution.py:116
  183.9 2.0 totals.1
  185.9 8.7 %all-to-all-start.2 = ((bf16[64,200,128]{2,1,0:T(8,128)(2,1)}), bf16[64,200,128]{2,1,0:T(8,128)(2,1)}, u32[]{:S(2)}, u32[]{:S(2)}) async-start(bf16[64,200,128]{2,1,0:T(8,128)(2,1)} %get-tuple-element.22), calls=%async_computation.2 | async-start | bytes 6553600 | tf_op jit(solution)/shard_map/all_to_all | solution.py:26
  194.6 7.9 %broadcast_select_fusion.1 = (bf16[1536,1024]{1,0:T(8,128)(2,1)}, bf16[1536,1024]{1,0:T(8,128)(2,1)S(1)}, bf16[1536,1024]{1,0:T(8,128)(2,1)}, bf16[1536,1024]{1,0:T(8,128)(2,1)S(1)}) fusion(pred[]{:T(512)S(6)} %eq.47, bf16[1536,2048]{1,0:T(8,128)(2,1)} %collective-permute-done.3, bf16[1536,2048]{1,0:T(8,128)(2,1)} %bitcast.7), kind=kLoop, calls=%fused_computation.19 | loop fusion | flops 6291456 | bytes 25165824 | tf_op jit(solution)/shard_map/jit(_where)/select_n | solution.py:345
  202.5 1.8 multiply_reduce_fusion.2
  204.3 4.4 %multiply_reduce_fusion.1 = (f32[2048]{0:T(1024)S(1)}, f32[2048,256]{0,1:T(8,128)}) fusion(bf16[1536,256]{0,1:T(8,128)(2,1)S(1)} %copy-done.15, bf16[1536,1024]{1,0:T(8,128)(2,1)S(1)} %get-tuple-element.63, bf16[1536,1024]{1,0:T(8,128)(2,1)S(1)} %get-tuple-element.65), kind=kOutput, calls=%fused_computation.38 | convolution fusion | flops 1624242176 | bytes 9183232 | tf_op jit(solution)/shard_map/dot_general | solution.py:18
  209.8 6.8 %multiply_reduce_fusion = (f32[256]{0:T(256)}, f32[256,2048]{1,0:T(8,128)}) fusion(bf16[1536,256]{0,1:T(8,128)(2,1)} %get-tuple-element.69, bf16[1536,1024]{1,0:T(8,128)(2,1)} %get-tuple-element.64, bf16[1536,1024]{1,0:T(8,128)(2,1)} %get-tuple-element.62), kind=kOutput, calls=%fused_computation.37 | convolution fusion | flops 1624243968 | bytes 9176064 | tf_op jit(solution)/shard_map/dot_general | solution.py:18
  216.6 1.8 copy.31
  218.4 2.9 %copy.32 = f32[1,2048,256]{2,1,0:T(8,128)} copy(f32[1,2048,256]{1,2,0:T(8,128)} %bitcast.50) | data formatting | bytes 4194304
  222.4 16.2 %all-to-all-done.2.rows_ref.notes_ref = bf16[64,200,128]{2,1,0:T(8,128)(2,1)} async-done(((bf16[64,200,128]{2,1,0:T(8,128)(2,1)}), bf16[64,200,128]{2,1,0:T(8,128)(2,1)}, u32[]{:S(2)}, u32[]{:S(2)}) %all-to-all-start.2) | async-done | bytes 3276832 | tf_op jit(solution)/shard_map/all_to_all | solution.py:26
  238.6 6.7 %final.1 = (bf16[256,1024]{1,0:T(8,128)(2,1)}, f32[4,256]{1,0:T(4,128)}, f32[1,256]{1,0:T(1,128)}) custom-call(bf16[64,200,128]{2,1,0:T(8,128)(2,1)} %all-to-all-done.2.rows_ref.notes_ref, bf16[64,200,128]{2,1,0:T(8,128)(2,1)} %all-to-all-done.2.rows_ref.notes_ref, bf16[256,1536]{1,0:T(8,128)(2,1)} %compare_convert_fusion.select_ref, ...), custom_call_target="tpu_custom_call" | custom-call | tf_op jit(solution)/shard_map/final/pallas_call | solution.py:217
  (69 shorter events, 11.2 us)
Async XLA Ops:
  0.6 95.7 %copy-start = (bf16[1,256,2048]{2,1,0:T(8,128)(2,1)S(1)}, bf16[1,256,2048]{2,1,0:T(8,128)(2,1)}, u32[]{:S(2)}) copy-start(bf16[1,256,2048]{2,1,0:T(8,128)(2,1)} %param.16) | copy-start | bytes 3145732
  6.4 86.8 %copy-start.2 = (bf16[256,2048]{1,0:T(8,128)(2,1)S(1)}, bf16[256,2048]{1,0:T(8,128)(2,1)}, u32[]{:S(2)}) copy-start(bf16[256,2048]{1,0:T(8,128)(2,1)} %cot_ref.1) | copy-start | bytes 3145732
  93.2 1.9 copy-start.3
  93.2 10.5 %collective-permute-start.3 = (bf16[1536,2048]{1,0:T(8,128)(2,1)}, bf16[1536,2048]{1,0:T(8,128)(2,1)}, u32[]{:S(2)}, u32[]{:S(2)}) collective-permute-start(bf16[1536,2048]{1,0:T(8,128)(2,1)} %bitcast.7), channel_id=1, source_target_pairs={{0,1},{1,0},{2,3},{3,2},{4,5},{5,4},{6,7},{7,6},{8,9},{9,8},{10,11... | collective-permute-start | bytes 18874376 | tf_op jit(solution)/shard_map/ppermute | solution.py:22
  93.2 1.9 copy-start.7
  93.2 2.4 copy-start.9
  96.3 3.1 %copy-start.12 = (bf16[1,2048,256]{2,1,0:T(8,128)(2,1)S(1)}, bf16[1,2048,256]{2,1,0:T(8,128)(2,1)}, u32[]{:S(2)}) copy-start(bf16[1,2048,256]{2,1,0:T(8,128)(2,1)} %param.14) | copy-start | bytes 3145732
  96.3 3.1 %copy-start.13 = (bf16[1,2048,256]{2,1,0:T(8,128)(2,1)S(1)}, bf16[1,2048,256]{2,1,0:T(8,128)(2,1)}, u32[]{:S(2)}) copy-start(bf16[1,2048,256]{2,1,0:T(8,128)(2,1)} %param.15) | copy-start | bytes 3145732
  112.1 3.5 %copy-start.14 = (bf16[1536,256]{0,1:T(8,128)(2,1)}, bf16[1536,256]{0,1:T(8,128)(2,1)S(1)}, u32[]{:S(2)}) copy-start(bf16[1536,256]{0,1:T(8,128)(2,1)S(1)} %get-tuple-element.67) | copy-start | bytes 2359300
  112.1 3.5 %copy-start.16 = (bf16[1536,256]{0,1:T(8,128)(2,1)}, bf16[1536,256]{0,1:T(8,128)(2,1)S(1)}, u32[]{:S(2)}) copy-start(bf16[1536,256]{0,1:T(8,128)(2,1)S(1)} %get-tuple-element.66) | copy-start | bytes 2359300
  115.6 1.2 copy-start.4
  115.6 60.1 %collective-permute-start.5 = (bf16[1536,1024]{1,0:T(8,128)(2,1)}, bf16[1536,1024]{1,0:T(8,128)(2,1)}, u32[]{:S(2)}, u32[]{:S(2)}) collective-permute-start(bf16[1536,1024]{1,0:T(8,128)(2,1)} %convolution_convert_fusion), channel_id=1, source_target_pairs={{0,1},{1,0},{2,3},{3,2},{4,5},{5,4},{6,7},{7,6},{8,9},{9,8},{10,11... | collective-permute-start | bytes 9437192 | tf_op jit(solution)/shard_map/ppermute | solution.py:22
  119.0 36.5 %collective-permute-start.2 = (bf16[512,768]{0,1:T(8,128)(2,1)}, bf16[512,768]{0,1:T(8,128)(2,1)}, u32[]{:S(2)}, u32[]{:S(2)}) collective-permute-start(bf16[512,768]{0,1:T(8,128)(2,1)} %get-tuple-element.72), channel_id=1, source_target_pairs={{0,96},{2,98},{4,100},{6,102},{8,104},{10,106},{12,108},{14,110},{... | collective-permute-start | bytes 2359304 | tf_op jit(solution)/shard_map/ppermute | solution.py:246
  121.2 34.3 %collective-permute-start.1 = (bf16[512,768]{0,1:T(8,128)(2,1)}, bf16[512,768]{0,1:T(8,128)(2,1)}, u32[]{:S(2)}, u32[]{:S(2)}) collective-permute-start(bf16[512,768]{0,1:T(8,128)(2,1)} %get-tuple-element.71), channel_id=1, source_target_pairs={{0,64},{2,66},{4,68},{6,70},{8,72},{10,74},{12,76},{14,78},{16,80}... | collective-permute-start | bytes 2359304 | tf_op jit(solution)/shard_map/ppermute | solution.py:246
  121.8 37.3 %collective-permute-start = (bf16[512,768]{0,1:T(8,128)(2,1)}, bf16[512,768]{0,1:T(8,128)(2,1)}, u32[]{:S(2)}, u32[]{:S(2)}) collective-permute-start(bf16[512,768]{0,1:T(8,128)(2,1)} %get-tuple-element.70), channel_id=1, source_target_pairs={{0,32},{2,34},{4,36},{6,38},{8,40},{10,42},{12,44},{14,46},{16,48}... | collective-permute-start | bytes 2359304 | tf_op jit(solution)/shard_map/ppermute | solution.py:246
  122.9 2.7 %copy-start.10 = (f32[64,256]{1,0:T(8,128)S(1)}, f32[64,256]{1,0:T(8,128)}, u32[]{:S(2)}) copy-start(f32[64,256]{1,0:T(8,128)} %get-tuple-element.23.place_ref) | copy-start | bytes 196612
  123.0 1.3 copy-start.5
  125.6 96.8 %collective-permute-start.6 = (bf16[256,1024]{1,0:T(8,128)(2,1)}, bf16[256,1024]{1,0:T(8,128)(2,1)}, u32[]{:S(2)}, u32[]{:S(2)}) collective-permute-start(bf16[256,1024]{1,0:T(8,128)(2,1)} %convolution_convert_fusion.4), channel_id=1, source_target_pairs={{0,1},{1,0},{2,3},{3,2},{4,5},{5,4},{6,7},{7,6},{8,9},{9,8},{10,11... | collective-permute-start | bytes 1572872 | tf_op jit(solution)/shard_map/ppermute | solution.py:22
  162.2 6.1 %copy-start.6 = (bf16[2048,512]{1,0:T(8,128)(2,1)S(1)}, bf16[2048,512]{1,0:T(8,128)(2,1)}, u32[]{:S(2)}) copy-start(bf16[2048,512]{1,0:T(8,128)(2,1)} %copy-done.5) | copy-start | bytes 6291460
  164.6 18.4 %all-to-all-start = ((bf16[16,32,768]{2,1,0:T(8,128)(2,1)}), bf16[16,32,768]{2,1,0:T(8,128)(2,1)S(1)}, u32[]{:S(2)}, u32[]{:S(2)}) async-start(bf16[16,32,768]{2,1,0:T(8,128)(2,1)} %bitcast.2), calls=%async_computation | async-start | bytes 1572864 | tf_op jit(solution)/shard_map/all_to_all | solution.py:305
  169.6 5.2 %collective-permute-start.4 = (f32[1536]{0:T(1024)S(1)}, f32[1536]{0:T(1024)S(1)}, u32[]{:S(2)}, u32[]{:S(2)}) collective-permute-start(f32[1536]{0:T(1024)S(1)} %get-tuple-element.68), channel_id=1, source_target_pairs={{0,1},{1,0},{2,3},{3,2},{4,5},{5,4},{6,7},{7,6},{8,9},{9,8},{10,11... | collective-permute-start | bytes 18440 | tf_op jit(solution)/shard_map/ppermute | solution.py:22
  183.0 0.9 copy-start.8
  185.9 52.7 %all-to-all-start.2 = ((bf16[64,200,128]{2,1,0:T(8,128)(2,1)}), bf16[64,200,128]{2,1,0:T(8,128)(2,1)}, u32[]{:S(2)}, u32[]{:S(2)}) async-start(bf16[64,200,128]{2,1,0:T(8,128)(2,1)} %get-tuple-element.22), calls=%async_computation.2 | async-start | bytes 6553600 | tf_op jit(solution)/shard_map/all_to_all | solution.py:26
  194.6 7.9 %copy-start.17 = (bf16[1536,256]{0,1:T(8,128)(2,1)S(1)}, bf16[1536,256]{0,1:T(8,128)(2,1)}, u32[]{:S(2)}) copy-start(bf16[1536,256]{0,1:T(8,128)(2,1)} %copy-done.16) | copy-start | bytes 2359300
  202.5 1.8 copy-start.15
  204.3 4.4 %copy-start.11 = (f32[32,768]{1,0:T(8,128)S(1)}, f32[32,768]{1,0:T(8,128)}, u32[]{:S(2)}) copy-start(f32[32,768]{1,0:T(8,128)} %get-tuple-element.26) | copy-start | bytes 294916
  209.5 11.7 %collective-permute-start.7 = (f32[4160]{0:T(1024)S(1)}, f32[4160]{0:T(1024)S(1)}, u32[]{:S(2)}, u32[]{:S(2)}) collective-permute-start(f32[4160]{0:T(1024)S(1)} %concatenate.33), channel_id=1, source_target_pairs={{0,1},{1,0},{2,3},{3,2},{4,5},{5,4},{6,7},{7,6},{8,9},{9,8},{10,11... | collective-permute-start | bytes 49928 | tf_op jit(solution)/shard_map/ppermute | solution.py:22
  238.6 6.7 %copy-start.1 = (bf16[1,256,2048]{2,1,0:T(8,128)(2,1)S(1)}, bf16[1,256,2048]{2,1,0:T(8,128)(2,1)}, u32[]{:S(2)}) copy-start(bf16[1,256,2048]{2,1,0:T(8,128)(2,1)} %param.16) | copy-start | bytes 3145732

commit v3 on v2

--- a/solution.py
+++ b/solution.py
@@ -181,7 +181,7 @@
     )(got, notes, payload)
 
 
-def final_kernel(rows_ref, notes_ref, select_ref, own_ref, peer_ref, place_ref, ids_ref, gates_ref, tok_ref, gate_ref, down_ref):
+def final_kernel(rows_ref, notes_ref, select_ref, own_ref, peer_ref, place_ref, ids_ref, gates_ref, tok_ref, gate_ref, down_ref, gate_at):
     experts, lines, lanes = rows_ref.shape
     cap = lines // 2
     left = rows_ref[:, :cap, :].reshape(experts * cap, lanes)
@@ -196,7 +196,8 @@
         whole = jnp.sum(notes, axis=0)
         down_ref[...] = jnp.concatenate([whole[0:1] + whole[2:3], whole[1:2] + whole[3:4]], axis=1)
         row = lax.broadcasted_iota(jnp.int32, notes.shape, 1)
-        gate = jnp.sum(jnp.where((row == 4) | (row == 5), notes, 0.0), axis=1)
+        gate_at[...] = jnp.sum(jnp.where((row == 4) | (row == 5), notes, 0.0), axis=1)
+        gate = gate_at[...]
         place = place_ref[...]
         at = jnp.zeros(place.shape, F32)
         for r in range(cap):
@@ -237,13 +238,48 @@
             jax.ShapeDtypeStruct(gates_t.shape, F32),
             jax.ShapeDtypeStruct((1, 2 * lanes), F32),
         ],
+        scratch_shapes=[pltpu.VMEM((experts, lanes), F32)],
         name="final",
     )(payload, payload, select_t, s_own, s_peer, place, ids_t, gates_t)
 
 
+def positions(size):
+    return [(i // SIDE**2 % SIDE, i // SIDE % SIDE, i % SIDE) for i in range(size)]
+
+
 def next_along(x, by):
-    size = lax.axis_size("ep")
-    return lax.ppermute(x, "ep", [(i, (i + by * (size // SIDE)) % size) for i in range(size)])
+    pairs = []
+    for z, y, x_at in positions(lax.axis_size("ep")):
+        here = (z * SIDE + y) * SIDE + x_at
+        pairs.append((2 * here, 2 * ((((z + by) % SIDE) * SIDE + y) * SIDE + x_at)))
+        pairs.append((2 * here + 1, 2 * ((z * SIDE + (y + by) % SIDE) * SIDE + x_at) + 1))
+    return lax.ppermute(x, ("ep", "tp"), pairs)
+
+
+def plane_groups(size):
+    at = positions(size)
+    by_z = [[2 * i for i in range(size) if at[i][0] == c] for c in range(SIDE)]
+    by_y = [[2 * i + 1 for i in range(size) if at[i][1] == c] for c in range(SIDE)]
+    return by_z + by_y
+
+
+def stage_kernel(a_ref, b_ref, c_ref, d_ref, out_ref):
+    pair = a_ref[...].astype(F32) + b_ref[...].astype(F32)
+    out_ref[...] = (pair + (c_ref[...].astype(F32) + d_ref[...].astype(F32))).astype(BF16)
+
+
+def stage_total(pieces):
+    rows, cols = pieces[0].shape
+    steps = 4
+    spec = pl.BlockSpec((rows // steps, cols), lambda i: (i, 0))
+    return pl.pallas_call(
+        stage_kernel,
+        grid=(steps,),
+        in_specs=[spec] * len(pieces),
+        out_specs=spec,
+        out_shape=jax.ShapeDtypeStruct((rows, cols), BF16),
+        name="stage_total",
+    )(*pieces)
 
 
 def silu_parts(pre):
@@ -291,18 +327,28 @@
     s_own = input_rows(s_d, s_both, own, half)
     shared = jnp.concatenate([mm(tokens, s_d, ROWS), mm(cotangent, s_hidden, ROWS)], axis=1).astype(BF16)
     plane = experts // SIDE
-    z = lax.div(lax.axis_index("ep"), plane)
-    part = width // SIDE
-    pieces = [
-        lax.dynamic_slice_in_dim(shared, lax.rem(z + by, SIDE) * part, part, 0) for by in range(SIDE)
-    ]
+    block = width // SIDE**2
+    ep = lax.axis_index("ep")
+    z, y = lax.div(ep, plane), lax.rem(lax.div(ep, SIDE), SIDE)
+    main = jnp.where(tp == 0, z, y)
+    step, stride = jnp.where(tp == 0, SIDE, 1), jnp.where(tp == 0, 1, SIDE)
+    pieces = []
+    for by in range(SIDE):
+        first = lax.rem(main + by, SIDE) * step
+        pieces.append(
+            jnp.concatenate(
+                [
+                    lax.dynamic_slice_in_dim(shared, (first + j * stride) * block, block, 0)
+                    for j in range(SIDE)
+                ],
+                axis=0,
+            )
+        )
     arrived = [next_along(pieces[by], by) for by in range(1, SIDE)]
-    terms = pieces[0].astype(F32)
-    for piece in arrived:
-        terms = terms + piece.astype(F32)
-    terms = terms.astype(BF16).reshape(plane, width // experts, 3 * hid)
-    groups = [list(range(i, i + plane)) for i in range(0, experts, plane)]
-    shared_got = lax.all_to_all(terms, "ep", 0, 0, tiled=True, axis_index_groups=groups)
+    terms = stage_total(pieces[:1] + arrived).reshape(plane, width // experts, 3 * hid)
+    shared_got = lax.all_to_all(
+        terms, ("ep", "tp"), 0, 0, tiled=True, axis_index_groups=plane_groups(experts)
+    )
     s_peer = swap(s_other)
     w_gu = jnp.concatenate([w_g, w_u], axis=1)
     w_gu_own = lax.dynamic_slice_in_dim(w_gu, own, half, 0)

time: 246 us -> 232 us (0.943)
  waiting for transfers between devices: 43.8 us -> 26.8 us
  local copies, waits for them, and re-layouts: 15.9 us -> 8.9 us
  starting transfers between devices: 16.5 us -> 20.1 us
  matrix products: 43.7 us -> 46.9 us
    ppermute x3, waiting for transfers between devices: 26.8 us -> 11.3 us  [next_along(): return lax.ppermute(x, ('ep', 'tp'), pairs)]
    concatenate x0 -> x4, other arithmetic: none -> 4.95 us  [layer(): jnp.concatenate([lax.dynamic_slice_in_dim(shared, (first + j * stride) *...]
    pallas_call x0 -> x1, Pallas kernels: none -> 3.93 us  [stage_total(): pl.pallas_call(stage_kernel, grid=(steps,), in_specs=[spec] * len(pieces)...]
    eq x4, local copies, waits for them, and re-layouts: 4.36 us -> 0.66 us  [layer(): pick = place.T[:, :, None] == slot[:cap].astype(F32)[None, None, :]]
    dot_general x16, matrix products: 43.7 us -> 46.9 us  [mm(): return lax.dot_general(a, b, contract, preferred_element_type=F32)]
    convert_element_type x1 -> x0, other arithmetic: 2.99 us -> none  [layer(): terms = terms.astype(BF16).reshape(plane, width // experts, 3 * hid)]
    unnamed x39 -> x53, local copies, waits for them, and re-layouts: 7.64 us -> 6.81 us
  transfers between devices with their start and end apart: 10 -> 10, of which waited for: 5 -> 3; matrix products, arithmetic and copies ran while one was open for 25% -> 25% of each run, Pallas kernels for 4% -> 6%
where the time goes in v3:
time: 232 us; the launch traced here: 231 us
  blocking collectives  86.8 us (37%)
  matrix products  46.9 us (20%)
  waiting for transfers between devices  26.8 us (12%)
  Pallas kernels  23.9 us (10%)
  starting transfers between devices  20.1 us (9%)
  other arithmetic  16.3 us (7%)
  local copies, waits for them, and re-layouts  8.9 us (4%)
    all_to_all x1, blocking collectives, to_each(): return lax.all_to_all(x, 'ep', 0, 0, tiled=True)  86.8 us
    dot_general x16, matrix products, mm(): return lax.dot_general(a, b, contract, preferred_element_type=F32)  46.9 us
    all_to_all x1, waiting for transfers between devices, to_each(): return lax.all_to_all(x, 'ep', 0, 0, tiled=True)  15.5 us
    ppermute x3, waiting for transfers between devices, next_along(): return lax.ppermute(x, ('ep', 'tp'), pairs)  11.3 us
    all_to_all x1, starting transfers between devices, to_each(): return lax.all_to_all(x, 'ep', 0, 0, tiled=True)  10.4 us
    pallas_call x1, Pallas kernels, payload_of(): pl.pallas_call(payload_kernel, grid=(steps,), in_specs=[pl.BlockSpec((slo...  6.96 us
    select_n x1, other arithmetic, layer(): jnp.where(low, got[:, half:], peer[:, half:])  6.88 us
    unnamed x53, local copies, waits for them, and re-layouts  6.81 us
  transfers between devices with their start and end apart: 10, of which 3 were waited for; matrix products, arithmetic and copies ran while one was open for 25% of the time, Pallas kernels for 6%

profile of v3, /device:TPU:0, one launch (start us, length us, event | category | flops | bytes accessed | tf_op | source)
XLA Modules:
  0.0 231.0 jit_solution(2158593994755008581)
XLA Ops:
  0.7 5.8 %routing.1 = (bf16[1536,2048]{1,0:T(8,128)(2,1)}, f32[64,256]{1,0:T(8,128)}) custom-call(s32[1]{0:T(128)} %bitcast.3.tp_ref, s32[4,256]{1,0:T(4,128)} %bitcast.53, f32[4,256]{1,0:T(4,128)} %bitcast.55, bf16[256,2048]{1,0:T(8,128)(2,1)} %tok_ref.1, bf16[256,2048]{1,0:T(8,128)(2,1)} %cot_ref.1), custom_call_target="tpu_custom_call" | custom-call | tf_op jit(solution)/shard_map/routing/pallas_call | solution.py:75
  6.4 86.8 %all_to_all.15 = bf16[64,24,2048]{2,1,0:T(8,128)(2,1)} all-to-all(bf16[64,24,2048]{2,1,0:T(8,128)(2,1)} %bitcast.47), channel_id=1, replica_groups=mesh['ep'=64,'tp'=2] {'ep'}, dimensions={0} | all-to-all | bytes 12582912 | tf_op jit(solution)/shard_map/all_to_all | solution.py:26
  93.2 1.8 fusion.61
  95.0 1.8 fusion.62
  98.3 3.0 %fusion.9 = f32[1536,256]{0,1:T(8,128)S(1)} fusion(bf16[1536,2048]{1,0:T(8,128)(2,1)} %bitcast.7, bf16[1,256,2048]{2,1,0:T(8,128)(2,1)S(1)} %copy-done, s32[]{:T(128)S(6)} %select_n.116), kind=kOutput, calls=%fused_computation.52 | convolution fusion | flops 805306368 | bytes 5242884 | tf_op jit(solution)/shard_map/dot_general | solution.py:18
  101.4 3.8 %fusion.12 = f32[1536,512]{0,1:T(8,128)S(1)} fusion(bf16[1536,2048]{1,0:T(8,128)(2,1)} %bitcast.7, s32[]{:T(128)S(6)} %select_n.116, bf16[2048,256]{1,0:T(8,128)(2,1)S(1)} %bitcast.60, bf16[2048,256]{1,0:T(8,128)(2,1)S(1)} %bitcast.64), kind=kOutput, calls=%fused_computation.55 | convolution fusion | flops 1612709888 | bytes 8388612 | tf_op jit(solution)/shard_map/dot_general | solution.py:18
  105.2 3.8 %convolution_add_fusion = f32[1536,512]{0,1:T(8,128)S(1)} fusion(f32[1536,512]{0,1:T(8,128)S(1)} %fusion.12, bf16[1536,2048]{1,0:T(8,128)(2,1)} %collective-permute-done.3, s32[]{:T(128)S(6)} %select_n.117, bf16[2048,256]{1,0:T(8,128)(2,1)S(1)} %bitcast.61, bf16[2048,256]{1,0:T(8,128)(2,1)S(1)} %bitcast.65), kind=kOutput, calls=%fused_computation.41 | convolution fusion | flops 1613496320 | bytes 11534340 | tf_op jit(solution)/shard_map/dot_general | solution.py:18
  109.1 4.6 %multiply_convert_fusion.1 = (bf16[1536,256]{0,1:T(8,128)(2,1)S(1)}, bf16[1536,256]{0,1:T(8,128)(2,1)S(1)}, f32[1536]{0:T(1024)S(1)}, bf16[1536,256]{0,1:T(8,128)(2,1)}) fusion(f32[1536,512]{0,1:T(8,128)S(1)} %convolution_add_fusion, f32[1536,256]{0,1:T(8,128)S(1)} %fusion.9, bf16[1,256,2048]{2,1,0:T(8,128)(2,1)S(1)} %copy-done, s32[]{:T(128)S(6)} %select_n.117, ...), kind=kOutput, calls=%fused_computation.66 | convolution fusion | flops 812775936 | bytes 10754052 | tf_op jit(solution)/shard_map/dot_general | solution.py:18
  113.6 3.5 %convolution_convert_fusion = bf16[1536,1024]{1,0:T(8,128)(2,1)} fusion(bf16[1536,256]{0,1:T(8,128)(2,1)S(1)} %get-tuple-element.67, bf16[1536,256]{0,1:T(8,128)(2,1)S(1)} %get-tuple-element.66, s32[]{:T(128)S(6)} %select_n.117, bf16[2048,256]{1,0:T(8,128)(2,1)S(1)} %bitcast.62, bf16[2048,256]{1,0:T(8,128)(2,1)S(1)} %bitcast.66), kind=kOutput, calls=%fused_computation.39 | convolution fusion | flops 1617428480 | bytes 6815748 | tf_op jit(solution)/shard_map/dot_general | solution.py:18
  118.3 1.0 fusion.37
  123.8 2.9 %collective-permute-start.1 = (bf16[512,768]{1,0:T(8,128)(2,1)}, bf16[512,768]{1,0:T(8,128)(2,1)}, u32[]{:S(2)}, u32[]{:S(2)}) collective-permute-start(bf16[512,768]{1,0:T(8,128)(2,1)} %pad_maximum_fusion.8), channel_id=1, source_target_pairs={{0,64},{1,17},{2,66},{3,19},{4,68},{5,21},{6,70},{7,23},{8,72},{9,... | collective-permute-start | bytes 2359304 | tf_op jit(solution)/shard_map/ppermute | solution.py:256
  127.6 1.4 collective-permute-start.2
  129.2 1.5 convolution_convert_fusion.4
  131.3 2.2 pad_maximum_fusion.6.a_ref
  133.5 1.1 compare_convert_fusion.select_ref
  134.6 8.8 %collective-permute-done.1.c_ref = bf16[512,768]{1,0:T(8,128)(2,1)} collective-permute-done((bf16[512,768]{1,0:T(8,128)(2,1)}, bf16[512,768]{1,0:T(8,128)(2,1)}, u32[]{:S(2)}, u32[]{:S(2)}) %collective-permute-start.1) | collective-permute-done | bytes 786464 | tf_op jit(solution)/shard_map/ppermute | solution.py:256
  143.4 2.5 %collective-permute-done.2.d_ref = bf16[512,768]{1,0:T(8,128)(2,1)} collective-permute-done((bf16[512,768]{1,0:T(8,128)(2,1)}, bf16[512,768]{1,0:T(8,128)(2,1)}, u32[]{:S(2)}, u32[]{:S(2)}) %collective-permute-start.2) | collective-permute-done | bytes 786464 | tf_op jit(solution)/shard_map/ppermute | solution.py:256
  145.9 3.9 %stage_total.1 = bf16[512,768]{1,0:T(8,128)(2,1)} custom-call(bf16[512,768]{1,0:T(8,128)(2,1)} %pad_maximum_fusion.6.a_ref, bf16[512,768]{1,0:T(8,128)(2,1)} %collective-permute-done.b_ref, bf16[512,768]{1,0:T(8,128)(2,1)} %collective-permute-done.1.c_ref, bf16[512,768]{1,0:T(8,128)(2,1)} %collective-permute-done.2.d_ref), custom_call_target="tpu_custom_call" | custom-call | tf_op jit(solution)/shard_map/stage_total/pallas_call | solution.py:275
  149.8 3.8 %all-to-all-start = ((bf16[16,32,768]{2,1,0:T(8,128)(2,1)}), bf16[16,32,768]{2,1,0:T(8,128)(2,1)S(1)}, u32[]{:S(2)}, u32[]{:S(2)}) async-start(bf16[16,32,768]{2,1,0:T(8,128)(2,1)} %bitcast.49), calls=%async_computation | async-start | bytes 1572864 | tf_op jit(solution)/shard_map/all_to_all | solution.py:349
  153.6 1.3 convolution_convert_fusion.5.own_ref
  154.9 5.2 %convolution_convert_fusion.1.own_ref = bf16[1536,1024]{1,0:T(8,128)(2,1)} fusion(bf16[1536,256]{0,1:T(8,128)(2,1)} %copy-done.21, bf16[1536,256]{0,1:T(8,128)(2,1)} %copy-done.23, s32[]{:T(128)S(6)} %select_n.116, bf16[2048,256]{1,0:T(8,128)(2,1)} %bitcast.59, bf16[2048,256]{1,0:T(8,128)(2,1)} %bitcast.63), kind=kOutput, calls=%fused_computation.40 | convolution fusion | flops 1617428480 | bytes 6815748 | tf_op jit(solution)/shard_map/dot_general | solution.py:18
  161.1 7.0 %payload.1.payload_ref = bf16[64,200,128]{2,1,0:T(8,128)(2,1)} custom-call(bf16[1536,1024]{1,0:T(8,128)(2,1)} %convolution_convert_fusion.1.own_ref, bf16[1536,1024]{1,0:T(8,128)(2,1)} %collective-permute-done.5.peer_ref), custom_call_target="tpu_custom_call" | custom-call | tf_op jit(solution)/shard_map/payload/pallas_call | solution.py:116
  168.9 2.0 totals.1
  170.9 10.4 %all-to-all-start.2 = ((bf16[64,200,128]{2,1,0:T(8,128)(2,1)}), bf16[64,200,128]{2,1,0:T(8,128)(2,1)}, u32[]{:S(2)}, u32[]{:S(2)}) async-start(bf16[64,200,128]{2,1,0:T(8,128)(2,1)} %get-tuple-element.22), calls=%async_computation.2 | async-start | bytes 6553600 | tf_op jit(solution)/shard_map/all_to_all | solution.py:26
  181.3 6.9 %broadcast_select_fusion.1 = (bf16[1536,1024]{1,0:T(8,128)(2,1)S(1)}, bf16[1536,1024]{1,0:T(8,128)(2,1)S(1)}, bf16[1536,1024]{1,0:T(8,128)(2,1)}, bf16[1536,1024]{1,0:T(8,128)(2,1)S(1)}) fusion(pred[]{:T(512)S(6)} %eq.42, bf16[1536,2048]{1,0:T(8,128)(2,1)} %collective-permute-done.3, bf16[1536,2048]{1,0:T(8,128)(2,1)} %bitcast.7), kind=kLoop, calls=%fused_computation.43 | loop fusion | flops 6291456 | bytes 25165824 | tf_op jit(solution)/shard_map/jit(_where)/select_n | solution.py:391
  188.2 4.3 %multiply_reduce_fusion.2 = (f32[2048]{0:T(1024)S(1)}, f32[2048,256]{0,1:T(8,128)}) fusion(bf16[1536,256]{0,1:T(8,128)(2,1)S(1)} %copy-done.24, bf16[1536,1024]{1,0:T(8,128)(2,1)S(1)} %get-tuple-element.63, bf16[1536,1024]{1,0:T(8,128)(2,1)S(1)} %get-tuple-element.65), kind=kOutput, calls=%fused_computation.63 | convolution fusion | flops 1624242176 | bytes 9183232 | tf_op jit(solution)/shard_map/dot_general | solution.py:18
  192.6 4.4 %multiply_reduce_fusion.1 = (f32[2048]{0:T(1024)S(1)}, f32[2048,256]{0,1:T(8,128)}) fusion(bf16[1536,256]{0,1:T(8,128)(2,1)S(1)} %copy-done.22, bf16[1536,1024]{1,0:T(8,128)(2,1)S(1)} %get-tuple-element.63, bf16[1536,1024]{1,0:T(8,128)(2,1)S(1)} %get-tuple-element.65), kind=kOutput, calls=%fused_computation.62 | convolution fusion | flops 1624242176 | bytes 9183232 | tf_op jit(solution)/shard_map/dot_general | solution.py:18
  198.2 5.8 %multiply_reduce_fusion = (f32[256]{0:T(256)}, f32[256,2048]{1,0:T(8,128)}) fusion(bf16[1536,256]{0,1:T(8,128)(2,1)} %get-tuple-element.69, bf16[1536,1024]{1,0:T(8,128)(2,1)} %get-tuple-element.64, bf16[1536,1024]{1,0:T(8,128)(2,1)S(1)} %get-tuple-element.62), kind=kOutput, calls=%fused_computation.61 | convolution fusion | flops 1624243968 | bytes 9176064 | tf_op jit(solution)/shard_map/dot_general | solution.py:18
  204.0 3.0 %copy.33 = f32[1,2048,256]{2,1,0:T(8,128)} copy(f32[1,2048,256]{1,2,0:T(8,128)} %bitcast.50) | data formatting | bytes 4194304
  207.1 1.8 copy.34
  210.1 15.5 %all-to-all-done.2.rows_ref.notes_ref = bf16[64,200,128]{2,1,0:T(8,128)(2,1)} async-done(((bf16[64,200,128]{2,1,0:T(8,128)(2,1)}), bf16[64,200,128]{2,1,0:T(8,128)(2,1)}, u32[]{:S(2)}, u32[]{:S(2)}) %all-to-all-start.2) | async-done | bytes 3276832 | tf_op jit(solution)/shard_map/all_to_all | solution.py:26
  225.6 5.2 %final.1 = (bf16[256,1024]{1,0:T(8,128)(2,1)}, f32[4,256]{1,0:T(4,128)}, f32[1,256]{1,0:T(1,128)}) custom-call(bf16[64,200,128]{2,1,0:T(8,128)(2,1)} %all-to-all-done.2.rows_ref.notes_ref, bf16[64,200,128]{2,1,0:T(8,128)(2,1)} %all-to-all-done.2.rows_ref.notes_ref, bf16[256,1536]{1,0:T(8,128)(2,1)} %compare_convert_fusion.select_ref, ...), custom_call_target="tpu_custom_call" | custom-call | tf_op jit(solution)/shard_map/final/pallas_call | solution.py:218
  (88 shorter events, 13.0 us)
Async XLA Ops:
  0.6 97.7 %copy-start = (bf16[1,256,2048]{2,1,0:T(8,128)(2,1)S(1)}, bf16[1,256,2048]{2,1,0:T(8,128)(2,1)}, u32[]{:S(2)}) copy-start(bf16[1,256,2048]{2,1,0:T(8,128)(2,1)} %param.16) | copy-start | bytes 3145732
  6.4 86.8 %copy-start.4 = (bf16[256,2048]{1,0:T(8,128)(2,1)S(1)}, bf16[256,2048]{1,0:T(8,128)(2,1)}, u32[]{:S(2)}) copy-start(bf16[256,2048]{1,0:T(8,128)(2,1)} %cot_ref.1) | copy-start | bytes 3145732
  6.4 88.6 %copy-start.2 = (bf16[256,2048]{1,0:T(8,128)(2,1)S(1)}, bf16[256,2048]{1,0:T(8,128)(2,1)}, u32[]{:S(2)}) copy-start(bf16[256,2048]{1,0:T(8,128)(2,1)} %tok_ref.1) | copy-start | bytes 3145732
  93.2 12.0 %collective-permute-start.3 = (bf16[1536,2048]{1,0:T(8,128)(2,1)}, bf16[1536,2048]{1,0:T(8,128)(2,1)}, u32[]{:S(2)}, u32[]{:S(2)}) collective-permute-start(bf16[1536,2048]{1,0:T(8,128)(2,1)} %bitcast.7), channel_id=1, source_target_pairs={{0,1},{1,0},{2,3},{3,2},{4,5},{5,4},{6,7},{7,6},{8,9},{9,8},{10,11... | collective-permute-start | bytes 18874376 | tf_op jit(solution)/shard_map/ppermute | solution.py:22
  93.2 3.7 %copy-start.11 = (bf16[2048,256]{1,0:T(8,128)(2,1)S(1)}, bf16[2048,256]{1,0:T(8,128)(2,1)}, u32[]{:S(2)}) copy-start(bf16[2048,256]{1,0:T(8,128)(2,1)} %param.17) | copy-start | bytes 3145732
  95.0 2.5 %copy-start.3 = (bf16[256,2048]{1,0:T(8,128)(2,1)S(1)}, bf16[256,2048]{1,0:T(8,128)(2,1)}, u32[]{:S(2)}) copy-start(bf16[256,2048]{1,0:T(8,128)(2,1)} %tok_ref.1) | copy-start | bytes 3145732
  98.3 3.1 %copy-start.19 = (bf16[1,2048,256]{2,1,0:T(8,128)(2,1)S(1)}, bf16[1,2048,256]{2,1,0:T(8,128)(2,1)}, u32[]{:S(2)}) copy-start(bf16[1,2048,256]{2,1,0:T(8,128)(2,1)} %param.14) | copy-start | bytes 3145732
  98.3 3.1 %copy-start.20 = (bf16[1,2048,256]{2,1,0:T(8,128)(2,1)S(1)}, bf16[1,2048,256]{2,1,0:T(8,128)(2,1)}, u32[]{:S(2)}) copy-start(bf16[1,2048,256]{2,1,0:T(8,128)(2,1)} %param.15) | copy-start | bytes 3145732
  113.6 3.5 %copy-start.21 = (bf16[1536,256]{0,1:T(8,128)(2,1)}, bf16[1536,256]{0,1:T(8,128)(2,1)S(1)}, u32[]{:S(2)}) copy-start(bf16[1536,256]{0,1:T(8,128)(2,1)S(1)} %get-tuple-element.67) | copy-start | bytes 2359300
  113.6 3.5 %copy-start.23 = (bf16[1536,256]{0,1:T(8,128)(2,1)}, bf16[1536,256]{0,1:T(8,128)(2,1)S(1)}, u32[]{:S(2)}) copy-start(bf16[1536,256]{0,1:T(8,128)(2,1)S(1)} %get-tuple-element.66) | copy-start | bytes 2359300
  113.6 4.0 %copy-start.5 = (bf16[256,2048]{1,0:T(8,128)(2,1)S(1)}, bf16[256,2048]{1,0:T(8,128)(2,1)}, u32[]{:S(2)}) copy-start(bf16[256,2048]{1,0:T(8,128)(2,1)} %cot_ref.1) | copy-start | bytes 3145732
  117.1 43.9 %collective-permute-start.5 = (bf16[1536,1024]{1,0:T(8,128)(2,1)}, bf16[1536,1024]{1,0:T(8,128)(2,1)}, u32[]{:S(2)}, u32[]{:S(2)}) collective-permute-start(bf16[1536,1024]{1,0:T(8,128)(2,1)} %convolution_convert_fusion), channel_id=1, source_target_pairs={{0,1},{1,0},{2,3},{3,2},{4,5},{5,4},{6,7},{7,6},{8,9},{9,8},{10,11... | collective-permute-start | bytes 9437192 | tf_op jit(solution)/shard_map/ppermute | solution.py:22
  121.1 13.5 %collective-permute-start = (bf16[512,768]{1,0:T(8,128)(2,1)}, bf16[512,768]{1,0:T(8,128)(2,1)}, u32[]{:S(2)}, u32[]{:S(2)}) collective-permute-start(bf16[512,768]{1,0:T(8,128)(2,1)} %pad_maximum_fusion.7), channel_id=1, source_target_pairs={{0,32},{1,9},{2,34},{3,11},{4,36},{5,13},{6,38},{7,15},{8,40},{9,1... | collective-permute-start | bytes 2359304 | tf_op jit(solution)/shard_map/ppermute | solution.py:256
  121.8 4.9 %copy-start.13 = (bf16[128,768]{1,0:T(8,128)(2,1)S(1)}, bf16[128,768]{1,0:T(8,128)(2,1)}, u32[]{:S(2)}) copy-start(bf16[128,768]{1,0:T(8,128)(2,1)} %get-tuple-element.70) | copy-start | bytes 589828
  121.8 4.9 %copy-start.14 = (bf16[128,768]{1,0:T(8,128)(2,1)S(1)}, bf16[128,768]{1,0:T(8,128)(2,1)}, u32[]{:S(2)}) copy-start(bf16[128,768]{1,0:T(8,128)(2,1)} %get-tuple-element.76) | copy-start | bytes 589828
  121.8 7.2 %copy-start.12 = (bf16[2048,256]{1,0:T(8,128)(2,1)S(1)}, bf16[2048,256]{1,0:T(8,128)(2,1)}, u32[]{:S(2)}) copy-start(bf16[2048,256]{1,0:T(8,128)(2,1)} %param.17) | copy-start | bytes 3145732
  121.9 7.2 %copy-start.8 = (bf16[2048,256]{1,0:T(8,128)(2,1)S(1)}, bf16[2048,256]{1,0:T(8,128)(2,1)}, u32[]{:S(2)}) copy-start(bf16[2048,256]{1,0:T(8,128)(2,1)} %param.18) | copy-start | bytes 3145732
  123.8 19.6 %collective-permute-start.1 = (bf16[512,768]{1,0:T(8,128)(2,1)}, bf16[512,768]{1,0:T(8,128)(2,1)}, u32[]{:S(2)}, u32[]{:S(2)}) collective-permute-start(bf16[512,768]{1,0:T(8,128)(2,1)} %pad_maximum_fusion.8), channel_id=1, source_target_pairs={{0,64},{1,17},{2,66},{3,19},{4,68},{5,21},{6,70},{7,23},{8,72},{9,... | collective-permute-start | bytes 2359304 | tf_op jit(solution)/shard_map/ppermute | solution.py:256
  127.6 3.0 %copy-start.17 = (f32[64,256]{1,0:T(8,128)S(1)}, f32[64,256]{1,0:T(8,128)}, u32[]{:S(2)}) copy-start(f32[64,256]{1,0:T(8,128)} %get-tuple-element.23.place_ref) | copy-start | bytes 196612
  127.6 18.3 %collective-permute-start.2 = (bf16[512,768]{1,0:T(8,128)(2,1)}, bf16[512,768]{1,0:T(8,128)(2,1)}, u32[]{:S(2)}, u32[]{:S(2)}) collective-permute-start(bf16[512,768]{1,0:T(8,128)(2,1)} %pad_maximum_fusion.9), channel_id=1, source_target_pairs={{0,96},{1,25},{2,98},{3,27},{4,100},{5,29},{6,102},{7,31},{8,104},... | collective-permute-start | bytes 2359304 | tf_op jit(solution)/shard_map/ppermute | solution.py:256
  129.1 1.5 copy-start.6
  130.6 79.5 %collective-permute-start.6 = (bf16[256,1024]{1,0:T(8,128)(2,1)}, bf16[256,1024]{1,0:T(8,128)(2,1)}, u32[]{:S(2)}, u32[]{:S(2)}) collective-permute-start(bf16[256,1024]{1,0:T(8,128)(2,1)} %convolution_convert_fusion.4), channel_id=1, source_target_pairs={{0,1},{1,0},{2,3},{3,2},{4,5},{5,4},{6,7},{7,6},{8,9},{9,8},{10,11... | collective-permute-start | bytes 1572872 | tf_op jit(solution)/shard_map/ppermute | solution.py:22
  134.6 19.0 %copy-start.7 = (bf16[2048,512]{1,0:T(8,128)(2,1)S(1)}, bf16[2048,512]{1,0:T(8,128)(2,1)}, u32[]{:S(2)}) copy-start(bf16[2048,512]{1,0:T(8,128)(2,1)} %copy-done.6) | copy-start | bytes 6291460
  149.8 18.2 %all-to-all-start = ((bf16[16,32,768]{2,1,0:T(8,128)(2,1)}), bf16[16,32,768]{2,1,0:T(8,128)(2,1)S(1)}, u32[]{:S(2)}, u32[]{:S(2)}) async-start(bf16[16,32,768]{2,1,0:T(8,128)(2,1)} %bitcast.49), calls=%async_computation | async-start | bytes 1572864 | tf_op jit(solution)/shard_map/all_to_all | solution.py:349
  154.9 5.2 %collective-permute-start.4 = (f32[1536]{0:T(1024)S(1)}, f32[1536]{0:T(1024)S(1)}, u32[]{:S(2)}, u32[]{:S(2)}) collective-permute-start(f32[1536]{0:T(1024)S(1)} %get-tuple-element.68), channel_id=1, source_target_pairs={{0,1},{1,0},{2,3},{3,2},{4,5},{5,4},{6,7},{7,6},{8,9},{9,8},{10,11... | collective-permute-start | bytes 18440 | tf_op jit(solution)/shard_map/ppermute | solution.py:22
  170.9 54.7 %all-to-all-start.2 = ((bf16[64,200,128]{2,1,0:T(8,128)(2,1)}), bf16[64,200,128]{2,1,0:T(8,128)(2,1)}, u32[]{:S(2)}, u32[]{:S(2)}) async-start(bf16[64,200,128]{2,1,0:T(8,128)(2,1)} %get-tuple-element.22), calls=%async_computation.2 | async-start | bytes 6553600 | tf_op jit(solution)/shard_map/all_to_all | solution.py:26
  181.3 6.9 %copy-start.24 = (bf16[1536,256]{0,1:T(8,128)(2,1)S(1)}, bf16[1536,256]{0,1:T(8,128)(2,1)}, u32[]{:S(2)}) copy-start(bf16[1536,256]{0,1:T(8,128)(2,1)} %copy-done.23) | copy-start | bytes 2359300
  188.2 4.3 %copy-start.22 = (bf16[1536,256]{0,1:T(8,128)(2,1)S(1)}, bf16[1536,256]{0,1:T(8,128)(2,1)}, u32[]{:S(2)}) copy-start(bf16[1536,256]{0,1:T(8,128)(2,1)} %copy-done.21) | copy-start | bytes 2359300
  192.6 4.4 %copy-start.18 = (f32[32,768]{1,0:T(8,128)S(1)}, f32[32,768]{1,0:T(8,128)}, u32[]{:S(2)}) copy-start(f32[32,768]{1,0:T(8,128)} %get-tuple-element.26) | copy-start | bytes 294916
  197.8 11.1 %collective-permute-start.7 = (f32[4160]{0:T(1024)S(1)}, f32[4160]{0:T(1024)S(1)}, u32[]{:S(2)}, u32[]{:S(2)}) collective-permute-start(f32[4160]{0:T(1024)S(1)} %concatenate.49), channel_id=1, source_target_pairs={{0,1},{1,0},{2,3},{3,2},{4,5},{5,4},{6,7},{7,6},{8,9},{9,8},{10,11... | collective-permute-start | bytes 49928 | tf_op jit(solution)/shard_map/ppermute | solution.py:22
  204.0 3.0 %copy-start.10 = (f32[2048,256]{0,1:T(8,128)S(1)}, f32[2048,256]{0,1:T(8,128)}, u32[]{:S(2)}) copy-start(f32[2048,256]{0,1:T(8,128)} %get-tuple-element.101) | copy-start | bytes 6291460
  209.5 21.3 %copy-start.1 = (bf16[1,256,2048]{2,1,0:T(8,128)(2,1)S(1)}, bf16[1,256,2048]{2,1,0:T(8,128)(2,1)}, u32[]{:S(2)}) copy-start(bf16[1,256,2048]{2,1,0:T(8,128)(2,1)} %param.16) | copy-start | bytes 3145732
  (3 other events, 2.8 us)

commit v4 on v3

--- a/solution.py
+++ b/solution.py
@@ -12,6 +12,7 @@
 COLS = (((1,), (1,)), ((), ()))
 PLAIN = (((1,), (0,)), ((), ()))
 SIDE = 4
+GRANT = 24 * 1024 * 1024
 
 
 def mm(a, b, contract=PLAIN):
@@ -97,30 +98,35 @@
     )(tp.reshape(1), ids_t, gates_t, tokens, cotangent)
 
 
-def payload_kernel(own_ref, peer_ref, out_ref):
+def payload_kernel(d_ref, w_ref, peer_ref, out_ref):
     block, lines, lanes = out_ref.shape
-    cap = own_ref.shape[0] // block
+    cap = peer_ref.shape[0] // block
+    own = mm(d_ref[...], w_ref[...], COLS).astype(BF16).astype(F32)
+    both = (own + peer_ref[...].astype(F32)).astype(BF16)
     for e in range(block):
         at = slice(e * cap, (e + 1) * cap)
         for c in range(lines // cap):
-            cols = slice(c * lanes, (c + 1) * lanes)
-            both = own_ref[at, cols].astype(F32) + peer_ref[at, cols].astype(F32)
-            out_ref[e, c * cap : (c + 1) * cap, :] = both.astype(BF16)
-
-
-def payload_of(own, peer, experts, extra):
-    slots, half = own.shape
-    steps = 8
+            out_ref[e, c * cap : (c + 1) * cap, :] = both[at, c * lanes : (c + 1) * lanes]
+
+
+def payload_of(d_both, w_own, peer, experts, extra):
+    slots, half = peer.shape
+    steps = 4
     cap = slots // experts
     lines = cap * half // 128
     return pl.pallas_call(
         payload_kernel,
         grid=(steps,),
-        in_specs=[pl.BlockSpec((slots // steps, half), lambda i: (i, 0))] * 2,
+        in_specs=[
+            pl.BlockSpec((slots // steps, d_both.shape[1]), lambda i: (i, 0)),
+            pl.BlockSpec(w_own.shape, lambda i: (0, 0)),
+            pl.BlockSpec((slots // steps, half), lambda i: (i, 0)),
+        ],
         out_specs=pl.BlockSpec((experts // steps, lines, 128), lambda i: (i, 0, 0)),
         out_shape=jax.ShapeDtypeStruct((experts, lines + extra, 128), BF16),
+        compiler_params=pltpu.CompilerParams(vmem_limit_bytes=GRANT),
         name="payload",
-    )(own, peer)
+    )(d_both, w_own, peer)
 
 
 def total_kernel(got_ref, notes_ref, payload_ref, sums_ref, out_ref, acc):
@@ -177,16 +183,17 @@
         ],
         input_output_aliases={2: 1},
         scratch_shapes=[pltpu.VMEM((rows, cols), F32)],
+        compiler_params=pltpu.CompilerParams(vmem_limit_bytes=GRANT),
         name="totals",
     )(got, notes, payload)
 
 
 def final_kernel(rows_ref, notes_ref, select_ref, own_ref, peer_ref, place_ref, ids_ref, gates_ref, tok_ref, gate_ref, down_ref, gate_at):
     experts, lines, lanes = rows_ref.shape
-    cap = lines // 2
-    left = rows_ref[:, :cap, :].reshape(experts * cap, lanes)
-    right = rows_ref[:, cap:, :].reshape(experts * cap, lanes)
-    back = jnp.concatenate([left, right], axis=1)
+    tiles = own_ref.shape[1] // lanes
+    cap = lines // tiles
+    columns = [rows_ref[:, c * cap : (c + 1) * cap, :].reshape(experts * cap, lanes) for c in range(tiles)]
+    back = jnp.concatenate(columns, axis=1)
     routed = mm(select_ref[...], back)
     tok_ref[...] = (routed + (own_ref[...].astype(F32) + peer_ref[...].astype(F32))).astype(BF16)
 
@@ -213,23 +220,25 @@
     tok_rows, half = s_own.shape
     slots = select_t.shape[1]
     cap = slots // experts
-    steps = half // (2 * lanes)
+    steps = 2
+    cols = half // steps
+    tiles = cols // lanes
     extra = lines - cap * half // lanes
     return pl.pallas_call(
         final_kernel,
         grid=(steps,),
         in_specs=[
-            pl.BlockSpec((experts, 2 * cap, lanes), lambda i: (0, i, 0)),
+            pl.BlockSpec((experts, tiles * cap, lanes), lambda i: (0, i, 0)),
             pl.BlockSpec((experts, extra, lanes), lambda i: (0, lines // extra - 1, 0)),
             pl.BlockSpec((tok_rows, slots), lambda i: (0, 0)),
-            pl.BlockSpec((tok_rows, 2 * lanes), lambda i: (0, i)),
-            pl.BlockSpec((tok_rows, 2 * lanes), lambda i: (0, i)),
+            pl.BlockSpec((tok_rows, cols), lambda i: (0, i)),
+            pl.BlockSpec((tok_rows, cols), lambda i: (0, i)),
             pl.BlockSpec(place.shape, lambda i: (0, 0)),
             pl.BlockSpec(ids_t.shape, lambda i: (0, 0)),
             pl.BlockSpec(gates_t.shape, lambda i: (0, 0)),
         ],
         out_specs=[
-            pl.BlockSpec((tok_rows, 2 * lanes), lambda i: (0, i)),
+            pl.BlockSpec((tok_rows, cols), lambda i: (0, i)),
             pl.BlockSpec(gates_t.shape, lambda i: (0, 0)),
             pl.BlockSpec((1, 2 * lanes), lambda i: (0, 0)),
         ],
@@ -239,6 +248,7 @@
             jax.ShapeDtypeStruct((1, 2 * lanes), F32),
         ],
         scratch_shapes=[pltpu.VMEM((experts, lanes), F32)],
+        compiler_params=pltpu.CompilerParams(vmem_limit_bytes=GRANT),
         name="final",
     )(payload, payload, select_t, s_own, s_peer, place, ids_t, gates_t)
 
@@ -270,7 +280,7 @@
 
 def stage_total(pieces):
     rows, cols = pieces[0].shape
-    steps = 4
+    steps = 2
     spec = pl.BlockSpec((rows // steps, cols), lambda i: (i, 0))
     return pl.pallas_call(
         stage_kernel,
@@ -278,6 +288,7 @@
         in_specs=[spec] * len(pieces),
         out_specs=spec,
         out_shape=jax.ShapeDtypeStruct((rows, cols), BF16),
+        compiler_params=pltpu.CompilerParams(vmem_limit_bytes=GRANT),
         name="stage_total",
     )(*pieces)
 
@@ -368,11 +379,10 @@
     gate_part = jnp.sum(hidden.astype(F32) * hidden_cot, axis=1)
     d_both = jnp.concatenate([hidden_cot * up_pre * slope, hidden_cot * active], axis=1).astype(BF16)
     rows_other = mm(d_both, w_gu_other, COLS).astype(BF16)
-    rows_own = mm(d_both, w_gu_own, COLS).astype(BF16)
     from_peer = swap(rows_other)
     gate_peer = swap(gate_part)
     extra = 8
-    payload = payload_of(rows_own, from_peer, experts, extra)
+    payload = payload_of(d_both, w_gu_own, from_peer, experts, extra)
     gate_sum = jnp.pad((gate_part + gate_peer).reshape(experts, 1, cap), ((0, 0), (0, 0), (0, 128 - cap)))
     high = lax.reduce_precision(gate_sum, 8, 7)
     line = jnp.arange(extra)[None, :, None]

time: 232 us -> 231 us (level)
  other arithmetic: 16.3 us -> 24 us
  Pallas kernels: 23.9 us -> 19 us
  matrix products: 46.9 us -> 42.7 us
  local copies, waits for them, and re-layouts: 8.9 us -> 13 us
  starting transfers between devices: 20.1 us -> 17.7 us
    ppermute x3, waiting for transfers between devices: 11.3 us -> 6.25 us  [next_along(): return lax.ppermute(x, ('ep', 'tp'), pairs)]
    dot_general x16 -> x15, matrix products: 46.9 us -> 42.7 us  [mm(): return lax.dot_general(a, b, contract, preferred_element_type=F32)]
    eq x4, local copies, waits for them, and re-layouts: 0.66 us -> 4.36 us  [layer(): pick = place.T[:, :, None] == slot[:cap].astype(F32)[None, None, :]]
    concatenate x3, other arithmetic: 1.86 us -> 5.53 us  [layer(): jnp.concatenate([mm(tokens, s_d, ROWS), mm(cotangent, s_hidden, ROWS)], a...]
    all_to_all x1, starting transfers between devices: 10.4 us -> 7.45 us  [to_each(): return lax.all_to_all(x, 'ep', 0, 0, tiled=True)]
    all_to_all x1, waiting for transfers between devices: 0.01 us -> 2.85 us  [layer(): lax.all_to_all(terms, ('ep', 'tp'), 0, 0, tiled=True, axis_index_groups=p...]
    concatenate x0 -> x2, other arithmetic: none -> 2.75 us  [the longest x1 1.48 us: layer(): jnp.concatenate([hidden_cot * up_pre * slope, hidden_cot * active], axis=1)]
    unnamed x53 -> x49, local copies, waits for them, and re-layouts: 6.81 us -> 7.19 us
  transfers between devices with their start and end apart: 10 -> 10, of which waited for: 3 -> 4; matrix products, arithmetic and copies ran while one was open for 25% -> 29% of each run, Pallas kernels for 6% -> 4%
where the time goes in v4:
time: 231 us; the launch traced here: 230 us
  blocking collectives  86.7 us (38%)
  matrix products  42.7 us (18%)
  waiting for transfers between devices  25.3 us (11%)
  other arithmetic  24 us (10%)
  Pallas kernels  19 us (8%)
  starting transfers between devices  17.7 us (8%)
  local copies, waits for them, and re-layouts  13 us (6%)
    all_to_all x1, blocking collectives, to_each(): return lax.all_to_all(x, 'ep', 0, 0, tiled=True)  86.7 us
    dot_general x15, matrix products, mm(): return lax.dot_general(a, b, contract, preferred_element_type=F32)  42.7 us
    all_to_all x1, waiting for transfers between devices, to_each(): return lax.all_to_all(x, 'ep', 0, 0, tiled=True)  16.2 us
    select_n x1, other arithmetic, layer(): jnp.where(low, got[:, half:], peer[:, half:])  7.91 us
    all_to_all x1, starting transfers between devices, to_each(): return lax.all_to_all(x, 'ep', 0, 0, tiled=True)  7.45 us
    unnamed x49, local copies, waits for them, and re-layouts  7.19 us
    ppermute x3, waiting for transfers between devices, next_along(): return lax.ppermute(x, ('ep', 'tp'), pairs)  6.25 us
    pallas_call x1, Pallas kernels, routing(): pl.pallas_call(routing_kernel, grid_spec=pltpu.PrefetchScalarGridSpec(num...  5.76 us
  transfers between devices with their start and end apart: 10, of which 4 were waited for; matrix products, arithmetic and copies ran while one was open for 29% of the time, Pallas kernels for 4%

profile of v4, /device:TPU:0, one launch (start us, length us, event | category | flops | bytes accessed | tf_op | source)
XLA Modules:
  0.0 229.6 jit_solution(11448151031151153155)
XLA Ops:
  0.7 5.8 %routing.1 = (bf16[1536,2048]{1,0:T(8,128)(2,1)}, f32[64,256]{1,0:T(8,128)}) custom-call(s32[1]{0:T(128)} %bitcast.3.tp_ref, s32[4,256]{1,0:T(4,128)} %bitcast.49, f32[4,256]{1,0:T(4,128)} %bitcast.51, bf16[256,2048]{1,0:T(8,128)(2,1)} %tok_ref.1, bf16[256,2048]{1,0:T(8,128)(2,1)} %cot_ref.1), custom_call_target="tpu_custom_call" | custom-call | tf_op jit(solution)/shard_map/routing/pallas_call | solution.py:76
  6.4 86.7 %all_to_all.15 = bf16[64,24,2048]{2,1,0:T(8,128)(2,1)} all-to-all(bf16[64,24,2048]{2,1,0:T(8,128)(2,1)} %bitcast.53), channel_id=1, replica_groups=mesh['ep'=64,'tp'=2] {'ep'}, dimensions={0} | all-to-all | bytes 12582912 | tf_op jit(solution)/shard_map/all_to_all | solution.py:27
  94.4 2.2 fusion.57
  96.6 2.1 fusion.58
  99.3 2.1 fusion.6
  101.4 2.9 %fusion.9 = f32[1536,256]{1,0:T(8,128)S(1)} fusion(bf16[1536,2048]{1,0:T(8,128)(2,1)} %bitcast.7, bf16[1,256,2048]{2,1,0:T(8,128)(2,1)S(1)} %copy-done, s32[]{:T(128)S(6)} %select_n.116), kind=kOutput, calls=%fused_computation.51 | convolution fusion | flops 805306368 | bytes 5242884 | tf_op jit(solution)/shard_map/dot_general | solution.py:19
  104.3 3.8 %fusion.12 = f32[1536,512]{1,0:T(8,128)S(1)} fusion(bf16[1024,512]{1,0:T(8,128)(2,1)S(1)} %fusion.16.w_ref, bf16[1536,2048]{1,0:T(8,128)(2,1)} %bitcast.7), kind=kOutput, calls=%fused_computation.54 | convolution fusion | flops 1610612736 | bytes 7340032 | tf_op jit(solution)/shard_map/dot_general | solution.py:19
  108.2 3.7 %convolution_add_fusion = f32[1536,512]{1,0:T(8,128)S(1)} fusion(f32[1536,512]{1,0:T(8,128)S(1)} %fusion.12, bf16[1536,2048]{1,0:T(8,128)(2,1)} %collective-permute-done.3, s32[]{:T(128)S(6)} %select_n.117, bf16[2048,256]{1,0:T(8,128)(2,1)S(1)} %bitcast.58, bf16[2048,256]{1,0:T(8,128)(2,1)S(1)} %bitcast.61), kind=kOutput, calls=%fused_computation.40 | convolution fusion | flops 1613496320 | bytes 11534340 | tf_op jit(solution)/shard_map/dot_general | solution.py:19
  111.9 4.4 %multiply_convert_fusion.1 = (bf16[1536,256]{1,0:T(8,128)(2,1)S(1)}, bf16[1536,256]{1,0:T(8,128)(2,1)S(1)}, f32[1536]{0:T(1024)S(1)}, bf16[1536,256]{1,0:T(8,128)(2,1)}) fusion(f32[1536,512]{1,0:T(8,128)S(1)} %convolution_add_fusion, f32[1536,256]{1,0:T(8,128)S(1)} %fusion.9, bf16[1,256,2048]{2,1,0:T(8,128)(2,1)S(1)} %copy-done, s32[]{:T(128)S(6)} %select_n.117, ...), kind=kOutput, calls=%fused_computation.65 | convolution fusion | flops 812775936 | bytes 10754052 | tf_op jit(solution)/shard_map/dot_general | solution.py:19
  116.3 3.5 %convolution_convert_fusion = bf16[1536,1024]{1,0:T(8,128)(2,1)} fusion(s32[]{:T(128)S(6)} %select_n.117, bf16[2048,256]{1,0:T(8,128)(2,1)S(1)} %bitcast.59, bf16[2048,256]{1,0:T(8,128)(2,1)S(1)} %bitcast.62, bf16[1536,256]{1,0:T(8,128)(2,1)S(1)} %get-tuple-element.67, bf16[1536,256]{1,0:T(8,128)(2,1)S(1)} %get-tuple-element.66), kind=kOutput, calls=%fused_computation.39 | convolution fusion | flops 1617428480 | bytes 6815748 | tf_op jit(solution)/shard_map/dot_general | solution.py:19
  121.0 2.3 fusion.37
  123.3 2.0 fusion.38
  129.2 2.9 %collective-permute-start.1 = (bf16[512,768]{1,0:T(8,128)(2,1)}, bf16[512,768]{1,0:T(8,128)(2,1)S(1)}, u32[]{:S(2)}, u32[]{:S(2)}) collective-permute-start(bf16[512,768]{1,0:T(8,128)(2,1)} %pad_maximum_fusion.6), channel_id=1, source_target_pairs={{0,64},{1,17},{2,66},{3,19},{4,68},{5,21},{6,70},{7,23},{8,72},{9,... | collective-permute-start | bytes 2359304 | tf_op jit(solution)/shard_map/ppermute | solution.py:266
  132.1 1.9 pad_maximum_fusion.7
  139.4 3.0 %copy.40 = f32[256,1536]{1,0:T(8,128)} copy(f32[256,1536]{0,1:T(8,128)} %bitcast.54) | data formatting | bytes 3145728 | tf_op jit(solution)/shard_map/eq | solution.py:371
  145.1 3.4 %collective-permute-done.1.c_ref = bf16[512,768]{1,0:T(8,128)(2,1)S(1)} collective-permute-done((bf16[512,768]{1,0:T(8,128)(2,1)}, bf16[512,768]{1,0:T(8,128)(2,1)S(1)}, u32[]{:S(2)}, u32[]{:S(2)}) %collective-permute-start.1) | collective-permute-done | bytes 786464 | tf_op jit(solution)/shard_map/ppermute | solution.py:266
  148.4 2.9 %collective-permute-done.2.d_ref = bf16[512,768]{1,0:T(8,128)(2,1)} collective-permute-done((bf16[512,768]{1,0:T(8,128)(2,1)}, bf16[512,768]{1,0:T(8,128)(2,1)}, u32[]{:S(2)}, u32[]{:S(2)}) %collective-permute-start.2) | collective-permute-done | bytes 786464 | tf_op jit(solution)/shard_map/ppermute | solution.py:266
  151.3 2.1 stage_total.1
  153.5 4.3 %all-to-all-start = ((bf16[16,32,768]{2,1,0:T(8,128)(2,1)}), bf16[16,32,768]{2,1,0:T(8,128)(2,1)}, u32[]{:S(2)}, u32[]{:S(2)}) async-start(bf16[16,32,768]{2,1,0:T(8,128)(2,1)} %bitcast.2), calls=%async_computation | async-start | bytes 1572864 | tf_op jit(solution)/shard_map/all_to_all | solution.py:360
  157.8 2.7 %convolution_convert_fusion.4.own_ref = bf16[256,1024]{1,0:T(8,128)(2,1)} fusion(bf16[2048,512]{1,0:T(8,128)(2,1)} %copy-done.10, s32[]{:T(128)S(6)} %select_n.116, bf16[256,256]{0,1:T(8,128)(2,1)} %copy-done.13, bf16[256,256]{0,1:T(8,128)(2,1)} %copy-done.12), kind=kOutput, calls=%fused_computation.72 | convolution fusion | flops 269221888 | bytes 1835012 | tf_op jit(solution)/shard_map/dot_general | solution.py:19
  162.8 5.4 %payload.1.payload_ref = bf16[64,200,128]{2,1,0:T(8,128)(2,1)} custom-call(bf16[1536,512]{1,0:T(8,128)(2,1)S(1)} %pad_maximum_fusion.3.d_ref, bf16[1024,512]{1,0:T(8,128)(2,1)S(1)} %fusion.16.w_ref, bf16[1536,1024]{1,0:T(8,128)(2,1)} %collective-permute-done.5.peer_ref), custom_call_target="tpu_custom_call" | custom-call | tf_op jit(solution)/shard_map/payload/pallas_call | solution.py:117
  168.2 2.8 %all-to-all-done.got_ref = bf16[16,32,768]{2,1,0:T(8,128)(2,1)} async-done(((bf16[16,32,768]{2,1,0:T(8,128)(2,1)}), bf16[16,32,768]{2,1,0:T(8,128)(2,1)}, u32[]{:S(2)}, u32[]{:S(2)}) %all-to-all-start) | async-done | bytes 786464 | tf_op jit(solution)/shard_map/all_to_all | solution.py:360
  172.0 1.9 totals.1
  173.9 7.4 %all-to-all-start.2 = ((bf16[64,200,128]{2,1,0:T(8,128)(2,1)}), bf16[64,200,128]{2,1,0:T(8,128)(2,1)}, u32[]{:S(2)}, u32[]{:S(2)}) async-start(bf16[64,200,128]{2,1,0:T(8,128)(2,1)} %get-tuple-element.22), calls=%async_computation.2 | async-start | bytes 6553600 | tf_op jit(solution)/shard_map/all_to_all | solution.py:27
  181.4 7.9 %broadcast_select_fusion.1 = (bf16[1536,1024]{1,0:T(8,128)(2,1)}, bf16[1536,1024]{1,0:T(8,128)(2,1)S(1)}, bf16[1536,1024]{1,0:T(8,128)(2,1)}, bf16[1536,1024]{1,0:T(8,128)(2,1)S(1)}) fusion(pred[]{:T(512)S(6)} %eq.42, bf16[1536,2048]{1,0:T(8,128)(2,1)} %collective-permute-done.3, bf16[1536,2048]{1,0:T(8,128)(2,1)} %bitcast.7), kind=kLoop, calls=%fused_computation.42 | loop fusion | flops 6291456 | bytes 25165824 | tf_op jit(solution)/shard_map/jit(_where)/select_n | solution.py:401
  189.3 1.9 multiply_reduce_fusion.2
  191.2 4.2 %multiply_reduce_fusion.1 = (f32[2048]{0:T(1024)S(1)}, f32[2048,256]{0,1:T(8,128)}) fusion(bf16[1536,256]{1,0:T(8,128)(2,1)S(1)} %copy-done.20, bf16[1536,1024]{1,0:T(8,128)(2,1)S(1)} %get-tuple-element.63, bf16[1536,1024]{1,0:T(8,128)(2,1)S(1)} %get-tuple-element.65), kind=kOutput, calls=%fused_computation.61 | convolution fusion | flops 1624242176 | bytes 9183232 | tf_op jit(solution)/shard_map/dot_general | solution.py:19
  196.7 6.8 %multiply_reduce_fusion = (f32[256]{0:T(256)}, f32[256,2048]{1,0:T(8,128)}) fusion(bf16[1536,256]{1,0:T(8,128)(2,1)} %get-tuple-element.69, bf16[1536,1024]{1,0:T(8,128)(2,1)} %get-tuple-element.64, bf16[1536,1024]{1,0:T(8,128)(2,1)} %get-tuple-element.62), kind=kOutput, calls=%fused_computation.60 | convolution fusion | flops 1624243968 | bytes 9176064 | tf_op jit(solution)/shard_map/dot_general | solution.py:19
  203.5 1.8 copy.41
  205.3 2.9 %copy.42 = f32[1,2048,256]{2,1,0:T(8,128)} copy(f32[1,2048,256]{1,2,0:T(8,128)} %bitcast.56) | data formatting | bytes 4194304
  209.4 16.2 %all-to-all-done.2.rows_ref.notes_ref = bf16[64,200,128]{2,1,0:T(8,128)(2,1)} async-done(((bf16[64,200,128]{2,1,0:T(8,128)(2,1)}), bf16[64,200,128]{2,1,0:T(8,128)(2,1)}, u32[]{:S(2)}, u32[]{:S(2)}) %all-to-all-start.2) | async-done | bytes 3276832 | tf_op jit(solution)/shard_map/all_to_all | solution.py:27
  225.6 3.8 %final.1 = (bf16[256,1024]{1,0:T(8,128)(2,1)}, f32[4,256]{1,0:T(4,128)}, f32[1,256]{1,0:T(1,128)}) custom-call(bf16[64,200,128]{2,1,0:T(8,128)(2,1)} %all-to-all-done.2.rows_ref.notes_ref, bf16[64,200,128]{2,1,0:T(8,128)(2,1)} %all-to-all-done.2.rows_ref.notes_ref, bf16[256,1536]{1,0:T(8,128)(2,1)S(1)} %compare_convert_fusion.select_ref, ...), custom_call_target="tpu_custom_call" | custom-call | tf_op jit(solution)/shard_map/final/pallas_call | solution.py:227
  (85 shorter events, 20.8 us)
Async XLA Ops:
  0.6 100.8 %copy-start = (bf16[1,256,2048]{2,1,0:T(8,128)(2,1)S(1)}, bf16[1,256,2048]{2,1,0:T(8,128)(2,1)}, u32[]{:S(2)}) copy-start(bf16[1,256,2048]{2,1,0:T(8,128)(2,1)} %param.16) | copy-start | bytes 3145732
  93.1 15.1 %collective-permute-start.3 = (bf16[1536,2048]{1,0:T(8,128)(2,1)}, bf16[1536,2048]{1,0:T(8,128)(2,1)}, u32[]{:S(2)}, u32[]{:S(2)}) collective-permute-start(bf16[1536,2048]{1,0:T(8,128)(2,1)} %bitcast.7), channel_id=1, source_target_pairs={{0,1},{1,0},{2,3},{3,2},{4,5},{5,4},{6,7},{7,6},{8,9},{9,8},{10,11... | collective-permute-start | bytes 18874376 | tf_op jit(solution)/shard_map/ppermute | solution.py:23
  94.4 4.3 %copy-start.8 = (bf16[256,2048]{1,0:T(8,128)(2,1)S(1)}, bf16[256,2048]{1,0:T(8,128)(2,1)}, u32[]{:S(2)}) copy-start(bf16[256,2048]{1,0:T(8,128)(2,1)} %tok_ref.1) | copy-start | bytes 3145732
  94.4 4.3 %copy-start.16 = (bf16[2048,256]{1,0:T(8,128)(2,1)S(1)}, bf16[2048,256]{1,0:T(8,128)(2,1)}, u32[]{:S(2)}) copy-start(bf16[2048,256]{1,0:T(8,128)(2,1)} %param.17) | copy-start | bytes 3145732
  99.3 36.2 %copy-start.12 = (bf16[256,256]{0,1:T(8,128)(2,1)}, bf16[256,256]{0,1:T(8,128)(2,1)S(1)}, u32[]{:S(2)}) copy-start(bf16[256,256]{0,1:T(8,128)(2,1)S(1)} %get-tuple-element.86) | copy-start | bytes 393220
  99.3 36.2 %copy-start.13 = (bf16[256,256]{0,1:T(8,128)(2,1)}, bf16[256,256]{0,1:T(8,128)(2,1)S(1)}, u32[]{:S(2)}) copy-start(bf16[256,256]{0,1:T(8,128)(2,1)S(1)} %get-tuple-element.87) | copy-start | bytes 393220
  104.3 3.9 %copy-start.14 = (bf16[1,2048,256]{2,1,0:T(8,128)(2,1)S(1)}, bf16[1,2048,256]{2,1,0:T(8,128)(2,1)}, u32[]{:S(2)}) copy-start(bf16[1,2048,256]{2,1,0:T(8,128)(2,1)} %param.14) | copy-start | bytes 3145732
  104.3 3.9 %copy-start.15 = (bf16[1,2048,256]{2,1,0:T(8,128)(2,1)S(1)}, bf16[1,2048,256]{2,1,0:T(8,128)(2,1)}, u32[]{:S(2)}) copy-start(bf16[1,2048,256]{2,1,0:T(8,128)(2,1)} %param.15) | copy-start | bytes 3145732
  116.3 3.5 %copy-start.19 = (bf16[1536,256]{1,0:T(8,128)(2,1)}, bf16[1536,256]{1,0:T(8,128)(2,1)S(1)}, u32[]{:S(2)}) copy-start(bf16[1536,256]{1,0:T(8,128)(2,1)S(1)} %get-tuple-element.67) | copy-start | bytes 2359300
  116.3 3.5 %copy-start.21 = (bf16[1536,256]{1,0:T(8,128)(2,1)}, bf16[1536,256]{1,0:T(8,128)(2,1)S(1)}, u32[]{:S(2)}) copy-start(bf16[1536,256]{1,0:T(8,128)(2,1)S(1)} %get-tuple-element.66) | copy-start | bytes 2359300
  116.3 4.0 %copy-start.9 = (bf16[256,2048]{1,0:T(8,128)(2,1)S(1)}, bf16[256,2048]{1,0:T(8,128)(2,1)}, u32[]{:S(2)}) copy-start(bf16[256,2048]{1,0:T(8,128)(2,1)} %cot_ref.1) | copy-start | bytes 3145732
  119.8 43.0 %collective-permute-start.5 = (bf16[1536,1024]{1,0:T(8,128)(2,1)}, bf16[1536,1024]{1,0:T(8,128)(2,1)}, u32[]{:S(2)}, u32[]{:S(2)}) collective-permute-start(bf16[1536,1024]{1,0:T(8,128)(2,1)} %convolution_convert_fusion), channel_id=1, source_target_pairs={{0,1},{1,0},{2,3},{3,2},{4,5},{5,4},{6,7},{7,6},{8,9},{9,8},{10,11... | collective-permute-start | bytes 9437192 | tf_op jit(solution)/shard_map/ppermute | solution.py:23
  120.9 4.4 %copy-start.7 = (bf16[2048,256]{1,0:T(8,128)(2,1)}, bf16[2048,256]{1,0:T(8,128)(2,1)S(1)}, u32[]{:S(2)}) copy-start(bf16[2048,256]{1,0:T(8,128)(2,1)S(1)} %fusion.7) | copy-start | bytes 3145732
  126.2 18.8 %collective-permute-start = (bf16[512,768]{1,0:T(8,128)(2,1)}, bf16[512,768]{1,0:T(8,128)(2,1)S(1)}, u32[]{:S(2)}, u32[]{:S(2)}) collective-permute-start(bf16[512,768]{1,0:T(8,128)(2,1)} %pad_maximum_fusion.5), channel_id=1, source_target_pairs={{0,32},{1,9},{2,34},{3,11},{4,36},{5,13},{6,38},{7,15},{8,40},{9,1... | collective-permute-start | bytes 2359304 | tf_op jit(solution)/shard_map/ppermute | solution.py:266
  126.9 8.4 %copy-start.17 = (bf16[2048,256]{1,0:T(8,128)(2,1)S(1)}, bf16[2048,256]{1,0:T(8,128)(2,1)}, u32[]{:S(2)}) copy-start(bf16[2048,256]{1,0:T(8,128)(2,1)} %param.17) | copy-start | bytes 3145732
  128.2 7.2 %copy-start.11 = (bf16[2048,256]{1,0:T(8,128)(2,1)S(1)}, bf16[2048,256]{1,0:T(8,128)(2,1)}, u32[]{:S(2)}) copy-start(bf16[2048,256]{1,0:T(8,128)(2,1)} %param.18) | copy-start | bytes 3145732
  129.2 19.2 %collective-permute-start.1 = (bf16[512,768]{1,0:T(8,128)(2,1)}, bf16[512,768]{1,0:T(8,128)(2,1)S(1)}, u32[]{:S(2)}, u32[]{:S(2)}) collective-permute-start(bf16[512,768]{1,0:T(8,128)(2,1)} %pad_maximum_fusion.6), channel_id=1, source_target_pairs={{0,64},{1,17},{2,66},{3,19},{4,68},{5,21},{6,70},{7,23},{8,72},{9,... | collective-permute-start | bytes 2359304 | tf_op jit(solution)/shard_map/ppermute | solution.py:266
  134.0 4.2 %copy-start.4 = (f32[64,256]{1,0:T(8,128)S(1)}, f32[64,256]{1,0:T(8,128)}, u32[]{:S(2)}) copy-start(f32[64,256]{1,0:T(8,128)} %get-tuple-element.23.place_ref) | copy-start | bytes 196612
  134.0 17.4 %collective-permute-start.2 = (bf16[512,768]{1,0:T(8,128)(2,1)}, bf16[512,768]{1,0:T(8,128)(2,1)}, u32[]{:S(2)}, u32[]{:S(2)}) collective-permute-start(bf16[512,768]{1,0:T(8,128)(2,1)} %pad_maximum_fusion.7), channel_id=1, source_target_pairs={{0,96},{1,25},{2,98},{3,27},{4,100},{5,29},{6,102},{7,31},{8,104},... | collective-permute-start | bytes 2359304 | tf_op jit(solution)/shard_map/ppermute | solution.py:266
  135.5 1.3 copy-start.10
  138.1 4.4 %copy-start.18 = (bf16[128,768]{1,0:T(8,128)(2,1)S(1)}, bf16[128,768]{1,0:T(8,128)(2,1)}, u32[]{:S(2)}) copy-start(bf16[128,768]{1,0:T(8,128)(2,1)} %get-tuple-element.73) | copy-start | bytes 589828
  138.1 71.3 %collective-permute-start.6 = (bf16[256,1024]{1,0:T(8,128)(2,1)}, bf16[256,1024]{1,0:T(8,128)(2,1)}, u32[]{:S(2)}, u32[]{:S(2)}) collective-permute-start(bf16[256,1024]{1,0:T(8,128)(2,1)} %convolution_convert_fusion.3), channel_id=1, source_target_pairs={{0,1},{1,0},{2,3},{3,2},{4,5},{5,4},{6,7},{7,6},{8,9},{9,8},{10,11... | collective-permute-start | bytes 1572872 | tf_op jit(solution)/shard_map/ppermute | solution.py:23
  153.5 17.6 %all-to-all-start = ((bf16[16,32,768]{2,1,0:T(8,128)(2,1)}), bf16[16,32,768]{2,1,0:T(8,128)(2,1)}, u32[]{:S(2)}, u32[]{:S(2)}) async-start(bf16[16,32,768]{2,1,0:T(8,128)(2,1)} %bitcast.2), calls=%async_computation | async-start | bytes 1572864 | tf_op jit(solution)/shard_map/all_to_all | solution.py:360
  160.4 1.5 collective-permute-start.4
  173.9 51.7 %all-to-all-start.2 = ((bf16[64,200,128]{2,1,0:T(8,128)(2,1)}), bf16[64,200,128]{2,1,0:T(8,128)(2,1)}, u32[]{:S(2)}, u32[]{:S(2)}) async-start(bf16[64,200,128]{2,1,0:T(8,128)(2,1)} %get-tuple-element.22), calls=%async_computation.2 | async-start | bytes 6553600 | tf_op jit(solution)/shard_map/all_to_all | solution.py:27
  181.4 7.9 %copy-start.22 = (bf16[1536,256]{1,0:T(8,128)(2,1)S(1)}, bf16[1536,256]{1,0:T(8,128)(2,1)}, u32[]{:S(2)}) copy-start(bf16[1536,256]{1,0:T(8,128)(2,1)} %copy-done.21) | copy-start | bytes 2359300
  189.3 1.9 copy-start.20
  196.2 12.0 %collective-permute-start.7 = (f32[4160]{0:T(1024)S(1)}, f32[4160]{0:T(1024)S(1)}, u32[]{:S(2)}, u32[]{:S(2)}) collective-permute-start(f32[4160]{0:T(1024)S(1)} %concatenate.49), channel_id=1, source_target_pairs={{0,1},{1,0},{2,3},{3,2},{4,5},{5,4},{6,7},{7,6},{8,9},{9,8},{10,11... | collective-permute-start | bytes 49928 | tf_op jit(solution)/shard_map/ppermute | solution.py:23
  205.3 20.3 %copy-start.2 = (bf16[256,1024]{1,0:T(8,128)(2,1)S(1)}, bf16[256,1024]{1,0:T(8,128)(2,1)}, u32[]{:S(2)}) copy-start(bf16[256,1024]{1,0:T(8,128)(2,1)} %convolution_convert_fusion.4.own_ref) | copy-start | bytes 1572868
  205.3 20.3 %copy-start.5 = (s32[256,4]{0,1:T(4,128)S(1)}, s32[256,4]{0,1:T(4,128)}, u32[]{:S(2)}) copy-start(s32[256,4]{0,1:T(4,128)} %param.11) | copy-start | bytes 12292
  205.3 20.3 %copy-start.6 = (f32[256,4]{0,1:T(4,128)S(1)}, f32[256,4]{0,1:T(4,128)}, u32[]{:S(2)}) copy-start(f32[256,4]{0,1:T(4,128)} %param.12) | copy-start | bytes 12292
  208.8 20.6 %copy-start.1 = (bf16[1,256,2048]{2,1,0:T(8,128)(2,1)S(1)}, bf16[1,256,2048]{2,1,0:T(8,128)(2,1)}, u32[]{:S(2)}) copy-start(bf16[1,256,2048]{2,1,0:T(8,128)(2,1)} %param.16) | copy-start | bytes 3145732
  (1 other events, 1.0 us)

commit v5 on v4

--- a/solution.py
+++ b/solution.py
@@ -12,6 +12,7 @@
 COLS = (((1,), (1,)), ((), ()))
 PLAIN = (((1,), (0,)), ((), ()))
 SIDE = 4
+TURN = 53
 GRANT = 24 * 1024 * 1024
 
 
@@ -23,8 +24,14 @@
     return lax.ppermute(x, "tp", [(0, 1), (1, 0)])
 
 
+def turn_of(e, size):
+    return (TURN * e) & (size - 1)
+
+
 def to_each(x):
-    return lax.all_to_all(x, "ep", 0, 0, tiled=True)
+    size = x.shape[0]
+    order = sorted(range(size), key=lambda e: turn_of(e, size))
+    return lax.all_to_all(x, "ep", 0, 0, tiled=True, axis_index_groups=[order])
 
 
 def routing_kernel(tp_ref, ids_ref, gates_ref, tok_ref, cot_ref, sent_ref, place_ref, place_at, gate_at):
@@ -42,7 +49,7 @@
         hit = jnp.zeros((experts, tok_rows), F32)
         gate_of = jnp.zeros((experts, tok_rows), F32)
         for k in range(ids_ref.shape[0]):
-            name = ids_ref[k : k + 1, :] == e
+            name = turn_of(ids_ref[k : k + 1, :], experts) == e
             hit = jnp.where(name, 1.0, hit)
             gate_of = jnp.where(name, gates_ref[k : k + 1, :], gate_of)
         earlier = lax.broadcasted_iota(jnp.int32, (tok_rows, tok_rows), 0)
@@ -211,7 +218,7 @@
             at = jnp.where(place == r, gate[:, r : r + 1], at)
         e = lax.broadcasted_iota(jnp.int32, place.shape, 0)
         for k in range(ids_ref.shape[0]):
-            mine = jnp.sum(jnp.where(ids_ref[k : k + 1, :] == e, at, 0.0), axis=0, keepdims=True)
+            mine = jnp.sum(jnp.where(turn_of(ids_ref[k : k + 1, :], experts) == e, at, 0.0), axis=0, keepdims=True)
             gate_ref[k : k + 1, :] = mine / gates_ref[k : k + 1, :]
 
 

time: 231 us -> 229 us (level)
  no operation moved by 1% of the time
where the time goes in v5:
time: 229 us; the launch traced here: 227 us
  blocking collectives  85.8 us (37%)
  matrix products  42.7 us (19%)
  waiting for transfers between devices  24.4 us (11%)
  other arithmetic  24 us (10%)
  Pallas kernels  19 us (8%)
  starting transfers between devices  17.1 us (7%)
  local copies, waits for them, and re-layouts  13 us (6%)
    all_to_all x1, blocking collectives, to_each(): return lax.all_to_all(x, 'ep', 0, 0, tiled=True, axis_index_groups=[order])  85.8 us
    dot_general x15, matrix products, mm(): return lax.dot_general(a, b, contract, preferred_element_type=F32)  42.7 us
    all_to_all x1, waiting for transfers between devices, to_each(): return lax.all_to_all(x, 'ep', 0, 0, tiled=True, axis_index_groups=[order])  14.3 us
    select_n x1, other arithmetic, layer(): jnp.where(low, got[:, half:], peer[:, half:])  7.91 us
    all_to_all x1, starting transfers between devices, to_each(): return lax.all_to_all(x, 'ep', 0, 0, tiled=True, axis_index_groups=[order])  7.69 us
    ppermute x3, waiting for transfers between devices, next_along(): return lax.ppermute(x, ('ep', 'tp'), pairs)  7.36 us
    unnamed x49, local copies, waits for them, and re-layouts  7.19 us
    pallas_call x1, Pallas kernels, routing(): pl.pallas_call(routing_kernel, grid_spec=pltpu.PrefetchScalarGridSpec(num...  5.76 us
  transfers between devices with their start and end apart: 10, of which 4 were waited for; matrix products, arithmetic and copies ran while one was open for 29% of the time, Pallas kernels for 4%

profile of v5, /device:TPU:0, one launch (start us, length us, event | category | flops | bytes accessed | tf_op | source)
XLA Modules:
  0.0 227.2 jit_solution(5843413109162455314)
XLA Ops:
  0.7 5.8 %routing.1 = (bf16[1536,2048]{1,0:T(8,128)(2,1)}, f32[64,256]{1,0:T(8,128)}) custom-call(s32[1]{0:T(128)} %bitcast.3.tp_ref, s32[4,256]{1,0:T(4,128)} %bitcast.49, f32[4,256]{1,0:T(4,128)} %bitcast.51, bf16[256,2048]{1,0:T(8,128)(2,1)} %tok_ref.1, bf16[256,2048]{1,0:T(8,128)(2,1)} %cot_ref.1), custom_call_target="tpu_custom_call" | custom-call | tf_op jit(solution)/shard_map/routing/pallas_call | solution.py:83
  6.4 85.8 %all_to_all.15 = bf16[64,24,2048]{2,1,0:T(8,128)(2,1)} all-to-all(bf16[64,24,2048]{2,1,0:T(8,128)(2,1)} %bitcast.53), channel_id=1, replica_groups={{0,58,116,46,104,34,92,22,80,10,68,126,56,114,44,102,32,90,20,78,8,66,1..., dimensions={0} | all-to-all | bytes 12582912 | tf_op jit(solution)/shard_map/all_to_all | solution.py:34
  93.5 2.2 fusion.57
  95.7 2.1 fusion.58
  98.4 2.1 fusion.6
  100.5 2.9 %fusion.9 = f32[1536,256]{1,0:T(8,128)S(1)} fusion(bf16[1536,2048]{1,0:T(8,128)(2,1)} %bitcast.7, bf16[1,256,2048]{2,1,0:T(8,128)(2,1)S(1)} %copy-done, s32[]{:T(128)S(6)} %select_n.116), kind=kOutput, calls=%fused_computation.51 | convolution fusion | flops 805306368 | bytes 5242884 | tf_op jit(solution)/shard_map/dot_general | solution.py:20
  103.5 3.8 %fusion.12 = f32[1536,512]{1,0:T(8,128)S(1)} fusion(bf16[1024,512]{1,0:T(8,128)(2,1)S(1)} %fusion.16.w_ref, bf16[1536,2048]{1,0:T(8,128)(2,1)} %bitcast.7), kind=kOutput, calls=%fused_computation.54 | convolution fusion | flops 1610612736 | bytes 7340032 | tf_op jit(solution)/shard_map/dot_general | solution.py:20
  107.3 3.7 %convolution_add_fusion = f32[1536,512]{1,0:T(8,128)S(1)} fusion(f32[1536,512]{1,0:T(8,128)S(1)} %fusion.12, bf16[1536,2048]{1,0:T(8,128)(2,1)} %collective-permute-done.3, s32[]{:T(128)S(6)} %select_n.117, bf16[2048,256]{1,0:T(8,128)(2,1)S(1)} %bitcast.58, bf16[2048,256]{1,0:T(8,128)(2,1)S(1)} %bitcast.61), kind=kOutput, calls=%fused_computation.40 | convolution fusion | flops 1613496320 | bytes 11534340 | tf_op jit(solution)/shard_map/dot_general | solution.py:20
  111.1 4.4 %multiply_convert_fusion.1 = (bf16[1536,256]{1,0:T(8,128)(2,1)S(1)}, bf16[1536,256]{1,0:T(8,128)(2,1)S(1)}, f32[1536]{0:T(1024)S(1)}, bf16[1536,256]{1,0:T(8,128)(2,1)}) fusion(f32[1536,512]{1,0:T(8,128)S(1)} %convolution_add_fusion, f32[1536,256]{1,0:T(8,128)S(1)} %fusion.9, bf16[1,256,2048]{2,1,0:T(8,128)(2,1)S(1)} %copy-done, s32[]{:T(128)S(6)} %select_n.117, ...), kind=kOutput, calls=%fused_computation.65 | convolution fusion | flops 812775936 | bytes 10754052 | tf_op jit(solution)/shard_map/dot_general | solution.py:20
  115.5 3.5 %convolution_convert_fusion = bf16[1536,1024]{1,0:T(8,128)(2,1)} fusion(s32[]{:T(128)S(6)} %select_n.117, bf16[2048,256]{1,0:T(8,128)(2,1)S(1)} %bitcast.59, bf16[2048,256]{1,0:T(8,128)(2,1)S(1)} %bitcast.62, bf16[1536,256]{1,0:T(8,128)(2,1)S(1)} %get-tuple-element.67, bf16[1536,256]{1,0:T(8,128)(2,1)S(1)} %get-tuple-element.66), kind=kOutput, calls=%fused_computation.39 | convolution fusion | flops 1617428480 | bytes 6815748 | tf_op jit(solution)/shard_map/dot_general | solution.py:20
  120.2 2.3 %fusion.37 = (bf16[128,768]{1,0:T(8,128)(2,1)S(1)}, bf16[128,768]{1,0:T(8,128)(2,1)S(1)}, bf16[128,768]{1,0:T(8,128)(2,1)S(1)}, bf16[128,768]{1,0:T(8,128)(2,1)}...) fusion(s32[]{:T(128)S(6)} %select_n.112, bf16[2048,512]{1,0:T(8,128)(2,1)} %fusion.6, ...), kind=kLoop, calls=%fused_computation.105 | loop fusion | flops 2359296 | bytes 4325400 | tf_op jit(solution)/shard_map/concatenate | solution.py:346
  122.5 2.0 fusion.38
  128.0 2.4 %collective-permute-start.1 = (bf16[512,768]{1,0:T(8,128)(2,1)}, bf16[512,768]{1,0:T(8,128)(2,1)S(1)}, u32[]{:S(2)}, u32[]{:S(2)}) collective-permute-start(bf16[512,768]{1,0:T(8,128)(2,1)} %pad_maximum_fusion.6), channel_id=1, source_target_pairs={{0,64},{1,17},{2,66},{3,19},{4,68},{5,21},{6,70},{7,23},{8,72},{9,... | collective-permute-start | bytes 2359304 | tf_op jit(solution)/shard_map/ppermute | solution.py:273
  130.4 1.9 pad_maximum_fusion.7
  137.4 3.0 %copy.40 = f32[256,1536]{1,0:T(8,128)} copy(f32[256,1536]{0,1:T(8,128)} %bitcast.54) | data formatting | bytes 3145728 | tf_op jit(solution)/shard_map/eq | solution.py:378
  143.1 4.1 %collective-permute-done.b_ref = bf16[512,768]{1,0:T(8,128)(2,1)S(1)} collective-permute-done((bf16[512,768]{1,0:T(8,128)(2,1)}, bf16[512,768]{1,0:T(8,128)(2,1)S(1)}, u32[]{:S(2)}, u32[]{:S(2)}) %collective-permute-start) | collective-permute-done | bytes 786464 | tf_op jit(solution)/shard_map/ppermute | solution.py:273
  147.2 3.3 %collective-permute-done.2.d_ref = bf16[512,768]{1,0:T(8,128)(2,1)} collective-permute-done((bf16[512,768]{1,0:T(8,128)(2,1)}, bf16[512,768]{1,0:T(8,128)(2,1)}, u32[]{:S(2)}, u32[]{:S(2)}) %collective-permute-start.2) | collective-permute-done | bytes 786464 | tf_op jit(solution)/shard_map/ppermute | solution.py:273
  150.5 2.1 stage_total.1
  152.6 4.6 %all-to-all-start = ((bf16[16,32,768]{2,1,0:T(8,128)(2,1)}), bf16[16,32,768]{2,1,0:T(8,128)(2,1)}, u32[]{:S(2)}, u32[]{:S(2)}) async-start(bf16[16,32,768]{2,1,0:T(8,128)(2,1)} %bitcast.2), calls=%async_computation | async-start | bytes 1572864 | tf_op jit(solution)/shard_map/all_to_all | solution.py:367
  157.2 2.7 %convolution_convert_fusion.4.own_ref = bf16[256,1024]{1,0:T(8,128)(2,1)} fusion(bf16[2048,512]{1,0:T(8,128)(2,1)} %copy-done.10, s32[]{:T(128)S(6)} %select_n.116, bf16[256,256]{0,1:T(8,128)(2,1)} %copy-done.13, bf16[256,256]{0,1:T(8,128)(2,1)} %copy-done.12), kind=kOutput, calls=%fused_computation.72 | convolution fusion | flops 269221888 | bytes 1835012 | tf_op jit(solution)/shard_map/dot_general | solution.py:20
  162.3 5.4 %payload.1.payload_ref = bf16[64,200,128]{2,1,0:T(8,128)(2,1)} custom-call(bf16[1536,512]{1,0:T(8,128)(2,1)S(1)} %pad_maximum_fusion.3.d_ref, bf16[1024,512]{1,0:T(8,128)(2,1)S(1)} %fusion.16.w_ref, bf16[1536,1024]{1,0:T(8,128)(2,1)} %collective-permute-done.5.peer_ref), custom_call_target="tpu_custom_call" | custom-call | tf_op jit(solution)/shard_map/payload/pallas_call | solution.py:124
  167.6 2.7 %all-to-all-done.got_ref = bf16[16,32,768]{2,1,0:T(8,128)(2,1)} async-done(((bf16[16,32,768]{2,1,0:T(8,128)(2,1)}), bf16[16,32,768]{2,1,0:T(8,128)(2,1)}, u32[]{:S(2)}, u32[]{:S(2)}) %all-to-all-start) | async-done | bytes 786464 | tf_op jit(solution)/shard_map/all_to_all | solution.py:367
  171.2 1.9 totals.1
  173.2 7.7 %all-to-all-start.2 = ((bf16[64,200,128]{2,1,0:T(8,128)(2,1)}), bf16[64,200,128]{2,1,0:T(8,128)(2,1)}, u32[]{:S(2)}, u32[]{:S(2)}) async-start(bf16[64,200,128]{2,1,0:T(8,128)(2,1)} %get-tuple-element.22), calls=%async_computation.2 | async-start | bytes 6553600 | tf_op jit(solution)/shard_map/all_to_all | solution.py:34
  180.9 7.9 %broadcast_select_fusion.1 = (bf16[1536,1024]{1,0:T(8,128)(2,1)}, bf16[1536,1024]{1,0:T(8,128)(2,1)S(1)}, bf16[1536,1024]{1,0:T(8,128)(2,1)}, bf16[1536,1024]{1,0:T(8,128)(2,1)S(1)}) fusion(pred[]{:T(512)S(6)} %eq.42, bf16[1536,2048]{1,0:T(8,128)(2,1)} %collective-permute-done.3, bf16[1536,2048]{1,0:T(8,128)(2,1)} %bitcast.7), kind=kLoop, calls=%fused_computation.42 | loop fusion | flops 6291456 | bytes 25165824 | tf_op jit(solution)/shard_map/jit(_where)/select_n | solution.py:408
  188.8 1.9 multiply_reduce_fusion.2
  190.7 4.2 %multiply_reduce_fusion.1 = (f32[2048]{0:T(1024)S(1)}, f32[2048,256]{0,1:T(8,128)}) fusion(bf16[1536,256]{1,0:T(8,128)(2,1)S(1)} %copy-done.20, bf16[1536,1024]{1,0:T(8,128)(2,1)S(1)} %get-tuple-element.63, bf16[1536,1024]{1,0:T(8,128)(2,1)S(1)} %get-tuple-element.65), kind=kOutput, calls=%fused_computation.61 | convolution fusion | flops 1624242176 | bytes 9183232 | tf_op jit(solution)/shard_map/dot_general | solution.py:20
  196.2 6.8 %multiply_reduce_fusion = (f32[256]{0:T(256)}, f32[256,2048]{1,0:T(8,128)}) fusion(bf16[1536,256]{1,0:T(8,128)(2,1)} %get-tuple-element.69, bf16[1536,1024]{1,0:T(8,128)(2,1)} %get-tuple-element.64, bf16[1536,1024]{1,0:T(8,128)(2,1)} %get-tuple-element.62), kind=kOutput, calls=%fused_computation.60 | convolution fusion | flops 1624243968 | bytes 9176064 | tf_op jit(solution)/shard_map/dot_general | solution.py:20
  203.0 1.8 copy.41
  204.8 2.9 %copy.42 = f32[1,2048,256]{2,1,0:T(8,128)} copy(f32[1,2048,256]{1,2,0:T(8,128)} %bitcast.56) | data formatting | bytes 4194304
  208.9 14.3 %all-to-all-done.2.rows_ref.notes_ref = bf16[64,200,128]{2,1,0:T(8,128)(2,1)} async-done(((bf16[64,200,128]{2,1,0:T(8,128)(2,1)}), bf16[64,200,128]{2,1,0:T(8,128)(2,1)}, u32[]{:S(2)}, u32[]{:S(2)}) %all-to-all-start.2) | async-done | bytes 3276832 | tf_op jit(solution)/shard_map/all_to_all | solution.py:34
  223.2 3.8 %final.1 = (bf16[256,1024]{1,0:T(8,128)(2,1)}, f32[4,256]{1,0:T(4,128)}, f32[1,256]{1,0:T(1,128)}) custom-call(bf16[64,200,128]{2,1,0:T(8,128)(2,1)} %all-to-all-done.2.rows_ref.notes_ref, bf16[64,200,128]{2,1,0:T(8,128)(2,1)} %all-to-all-done.2.rows_ref.notes_ref, bf16[256,1536]{1,0:T(8,128)(2,1)S(1)} %compare_convert_fusion.select_ref, ...), custom_call_target="tpu_custom_call" | custom-call | tf_op jit(solution)/shard_map/final/pallas_call | solution.py:234
  (85 shorter events, 20.2 us)
Async XLA Ops:
  0.6 99.9 %copy-start = (bf16[1,256,2048]{2,1,0:T(8,128)(2,1)S(1)}, bf16[1,256,2048]{2,1,0:T(8,128)(2,1)}, u32[]{:S(2)}) copy-start(bf16[1,256,2048]{2,1,0:T(8,128)(2,1)} %param.16) | copy-start | bytes 3145732
  92.2 15.1 %collective-permute-start.3 = (bf16[1536,2048]{1,0:T(8,128)(2,1)}, bf16[1536,2048]{1,0:T(8,128)(2,1)}, u32[]{:S(2)}, u32[]{:S(2)}) collective-permute-start(bf16[1536,2048]{1,0:T(8,128)(2,1)} %bitcast.7), channel_id=1, source_target_pairs={{0,1},{1,0},{2,3},{3,2},{4,5},{5,4},{6,7},{7,6},{8,9},{9,8},{10,11... | collective-permute-start | bytes 18874376 | tf_op jit(solution)/shard_map/ppermute | solution.py:24
  93.5 4.3 %copy-start.8 = (bf16[256,2048]{1,0:T(8,128)(2,1)S(1)}, bf16[256,2048]{1,0:T(8,128)(2,1)}, u32[]{:S(2)}) copy-start(bf16[256,2048]{1,0:T(8,128)(2,1)} %tok_ref.1) | copy-start | bytes 3145732
  93.5 4.3 %copy-start.16 = (bf16[2048,256]{1,0:T(8,128)(2,1)S(1)}, bf16[2048,256]{1,0:T(8,128)(2,1)}, u32[]{:S(2)}) copy-start(bf16[2048,256]{1,0:T(8,128)(2,1)} %param.17) | copy-start | bytes 3145732
  98.4 35.1 %copy-start.12 = (bf16[256,256]{0,1:T(8,128)(2,1)}, bf16[256,256]{0,1:T(8,128)(2,1)S(1)}, u32[]{:S(2)}) copy-start(bf16[256,256]{0,1:T(8,128)(2,1)S(1)} %get-tuple-element.86) | copy-start | bytes 393220
  98.4 35.1 %copy-start.13 = (bf16[256,256]{0,1:T(8,128)(2,1)}, bf16[256,256]{0,1:T(8,128)(2,1)S(1)}, u32[]{:S(2)}) copy-start(bf16[256,256]{0,1:T(8,128)(2,1)S(1)} %get-tuple-element.87) | copy-start | bytes 393220
  103.4 3.9 %copy-start.14 = (bf16[1,2048,256]{2,1,0:T(8,128)(2,1)S(1)}, bf16[1,2048,256]{2,1,0:T(8,128)(2,1)}, u32[]{:S(2)}) copy-start(bf16[1,2048,256]{2,1,0:T(8,128)(2,1)} %param.14) | copy-start | bytes 3145732
  103.5 3.9 %copy-start.15 = (bf16[1,2048,256]{2,1,0:T(8,128)(2,1)S(1)}, bf16[1,2048,256]{2,1,0:T(8,128)(2,1)}, u32[]{:S(2)}) copy-start(bf16[1,2048,256]{2,1,0:T(8,128)(2,1)} %param.15) | copy-start | bytes 3145732
  115.5 3.5 %copy-start.19 = (bf16[1536,256]{1,0:T(8,128)(2,1)}, bf16[1536,256]{1,0:T(8,128)(2,1)S(1)}, u32[]{:S(2)}) copy-start(bf16[1536,256]{1,0:T(8,128)(2,1)S(1)} %get-tuple-element.67) | copy-start | bytes 2359300
  115.5 3.5 %copy-start.21 = (bf16[1536,256]{1,0:T(8,128)(2,1)}, bf16[1536,256]{1,0:T(8,128)(2,1)S(1)}, u32[]{:S(2)}) copy-start(bf16[1536,256]{1,0:T(8,128)(2,1)S(1)} %get-tuple-element.66) | copy-start | bytes 2359300
  115.5 4.0 %copy-start.9 = (bf16[256,2048]{1,0:T(8,128)(2,1)S(1)}, bf16[256,2048]{1,0:T(8,128)(2,1)}, u32[]{:S(2)}) copy-start(bf16[256,2048]{1,0:T(8,128)(2,1)} %cot_ref.1) | copy-start | bytes 3145732
  119.0 43.3 %collective-permute-start.5 = (bf16[1536,1024]{1,0:T(8,128)(2,1)}, bf16[1536,1024]{1,0:T(8,128)(2,1)}, u32[]{:S(2)}, u32[]{:S(2)}) collective-permute-start(bf16[1536,1024]{1,0:T(8,128)(2,1)} %convolution_convert_fusion), channel_id=1, source_target_pairs={{0,1},{1,0},{2,3},{3,2},{4,5},{5,4},{6,7},{7,6},{8,9},{9,8},{10,11... | collective-permute-start | bytes 9437192 | tf_op jit(solution)/shard_map/ppermute | solution.py:24
  120.0 4.4 %copy-start.7 = (bf16[2048,256]{1,0:T(8,128)(2,1)}, bf16[2048,256]{1,0:T(8,128)(2,1)S(1)}, u32[]{:S(2)}) copy-start(bf16[2048,256]{1,0:T(8,128)(2,1)S(1)} %fusion.7) | copy-start | bytes 3145732
  125.4 21.8 %collective-permute-start = (bf16[512,768]{1,0:T(8,128)(2,1)}, bf16[512,768]{1,0:T(8,128)(2,1)S(1)}, u32[]{:S(2)}, u32[]{:S(2)}) collective-permute-start(bf16[512,768]{1,0:T(8,128)(2,1)} %pad_maximum_fusion.5), channel_id=1, source_target_pairs={{0,32},{1,9},{2,34},{3,11},{4,36},{5,13},{6,38},{7,15},{8,40},{9,1... | collective-permute-start | bytes 2359304 | tf_op jit(solution)/shard_map/ppermute | solution.py:273
  125.8 7.6 %copy-start.17 = (bf16[2048,256]{1,0:T(8,128)(2,1)S(1)}, bf16[2048,256]{1,0:T(8,128)(2,1)}, u32[]{:S(2)}) copy-start(bf16[2048,256]{1,0:T(8,128)(2,1)} %param.17) | copy-start | bytes 3145732
  127.1 6.4 %copy-start.11 = (bf16[2048,256]{1,0:T(8,128)(2,1)S(1)}, bf16[2048,256]{1,0:T(8,128)(2,1)}, u32[]{:S(2)}) copy-start(bf16[2048,256]{1,0:T(8,128)(2,1)} %param.18) | copy-start | bytes 3145732
  128.0 19.2 %collective-permute-start.1 = (bf16[512,768]{1,0:T(8,128)(2,1)}, bf16[512,768]{1,0:T(8,128)(2,1)S(1)}, u32[]{:S(2)}, u32[]{:S(2)}) collective-permute-start(bf16[512,768]{1,0:T(8,128)(2,1)} %pad_maximum_fusion.6), channel_id=1, source_target_pairs={{0,64},{1,17},{2,66},{3,19},{4,68},{5,21},{6,70},{7,23},{8,72},{9,... | collective-permute-start | bytes 2359304 | tf_op jit(solution)/shard_map/ppermute | solution.py:273
  132.3 3.9 %copy-start.4 = (f32[64,256]{1,0:T(8,128)S(1)}, f32[64,256]{1,0:T(8,128)}, u32[]{:S(2)}) copy-start(f32[64,256]{1,0:T(8,128)} %get-tuple-element.23.place_ref) | copy-start | bytes 196612
  132.3 18.2 %collective-permute-start.2 = (bf16[512,768]{1,0:T(8,128)(2,1)}, bf16[512,768]{1,0:T(8,128)(2,1)}, u32[]{:S(2)}, u32[]{:S(2)}) collective-permute-start(bf16[512,768]{1,0:T(8,128)(2,1)} %pad_maximum_fusion.7), channel_id=1, source_target_pairs={{0,96},{1,25},{2,98},{3,27},{4,100},{5,29},{6,102},{7,31},{8,104},... | collective-permute-start | bytes 2359304 | tf_op jit(solution)/shard_map/ppermute | solution.py:273
  133.6 1.3 copy-start.10
  136.2 4.4 %copy-start.18 = (bf16[128,768]{1,0:T(8,128)(2,1)S(1)}, bf16[128,768]{1,0:T(8,128)(2,1)}, u32[]{:S(2)}) copy-start(bf16[128,768]{1,0:T(8,128)(2,1)} %get-tuple-element.73) | copy-start | bytes 589828
  136.2 72.8 %collective-permute-start.6 = (bf16[256,1024]{1,0:T(8,128)(2,1)}, bf16[256,1024]{1,0:T(8,128)(2,1)}, u32[]{:S(2)}, u32[]{:S(2)}) collective-permute-start(bf16[256,1024]{1,0:T(8,128)(2,1)} %convolution_convert_fusion.3), channel_id=1, source_target_pairs={{0,1},{1,0},{2,3},{3,2},{4,5},{5,4},{6,7},{7,6},{8,9},{9,8},{10,11... | collective-permute-start | bytes 1572872 | tf_op jit(solution)/shard_map/ppermute | solution.py:24
  152.6 17.7 %all-to-all-start = ((bf16[16,32,768]{2,1,0:T(8,128)(2,1)}), bf16[16,32,768]{2,1,0:T(8,128)(2,1)}, u32[]{:S(2)}, u32[]{:S(2)}) async-start(bf16[16,32,768]{2,1,0:T(8,128)(2,1)} %bitcast.2), calls=%async_computation | async-start | bytes 1572864 | tf_op jit(solution)/shard_map/all_to_all | solution.py:367
  159.8 1.5 collective-permute-start.4
  173.2 50.1 %all-to-all-start.2 = ((bf16[64,200,128]{2,1,0:T(8,128)(2,1)}), bf16[64,200,128]{2,1,0:T(8,128)(2,1)}, u32[]{:S(2)}, u32[]{:S(2)}) async-start(bf16[64,200,128]{2,1,0:T(8,128)(2,1)} %get-tuple-element.22), calls=%async_computation.2 | async-start | bytes 6553600 | tf_op jit(solution)/shard_map/all_to_all | solution.py:34
  180.9 7.9 %copy-start.22 = (bf16[1536,256]{1,0:T(8,128)(2,1)S(1)}, bf16[1536,256]{1,0:T(8,128)(2,1)}, u32[]{:S(2)}) copy-start(bf16[1536,256]{1,0:T(8,128)(2,1)} %copy-done.21) | copy-start | bytes 2359300
  188.8 1.9 copy-start.20
  195.7 12.0 %collective-permute-start.7 = (f32[4160]{0:T(1024)S(1)}, f32[4160]{0:T(1024)S(1)}, u32[]{:S(2)}, u32[]{:S(2)}) collective-permute-start(f32[4160]{0:T(1024)S(1)} %concatenate.49), channel_id=1, source_target_pairs={{0,1},{1,0},{2,3},{3,2},{4,5},{5,4},{6,7},{7,6},{8,9},{9,8},{10,11... | collective-permute-start | bytes 49928 | tf_op jit(solution)/shard_map/ppermute | solution.py:24
  204.8 18.5 %copy-start.2 = (bf16[256,1024]{1,0:T(8,128)(2,1)S(1)}, bf16[256,1024]{1,0:T(8,128)(2,1)}, u32[]{:S(2)}) copy-start(bf16[256,1024]{1,0:T(8,128)(2,1)} %convolution_convert_fusion.4.own_ref) | copy-start | bytes 1572868
  204.8 18.5 %copy-start.5 = (s32[256,4]{0,1:T(4,128)S(1)}, s32[256,4]{0,1:T(4,128)}, u32[]{:S(2)}) copy-start(s32[256,4]{0,1:T(4,128)} %param.11) | copy-start | bytes 12292
  204.8 18.5 %copy-start.6 = (f32[256,4]{0,1:T(4,128)S(1)}, f32[256,4]{0,1:T(4,128)}, u32[]{:S(2)}) copy-start(f32[256,4]{0,1:T(4,128)} %param.12) | copy-start | bytes 12292
  208.3 18.7 %copy-start.1 = (bf16[1,256,2048]{2,1,0:T(8,128)(2,1)S(1)}, bf16[1,256,2048]{2,1,0:T(8,128)(2,1)}, u32[]{:S(2)}) copy-start(bf16[1,256,2048]{2,1,0:T(8,128)(2,1)} %param.16) | copy-start | bytes 3145732
  (1 other events, 1.0 us)

commit v6 on v5

--- a/solution.py
+++ b/solution.py
@@ -136,47 +136,33 @@
     )(d_both, w_own, peer)
 
 
-def total_kernel(got_ref, notes_ref, payload_ref, sums_ref, out_ref, acc):
-    step = pl.program_id(0)
-    part = jnp.sum(got_ref[...].astype(F32), axis=0)
-
-    @pl.when(step == 0)
-    def _():
-        acc[...] = part
-
-    @pl.when(step > 0)
-    def _():
-        acc[...] = acc[...] + part
-
-    @pl.when(step == pl.num_programs(0) - 1)
-    def _():
-        total = acc[...]
-        sums_ref[...] = total
-        down = total[:, 2 * (total.shape[1] // 3) :]
-        norms = jnp.sum(down * down, axis=0, keepdims=True)
-        high = norms.astype(BF16).astype(F32)
-        low = norms - high
-        lines = out_ref.shape[1:]
-        row = lax.broadcasted_iota(jnp.int32, lines, 0)
-        marks = jnp.zeros(lines, F32)
-        pieces = norms.shape[1] // lines[1]
-        for at, value in enumerate((high, low)):
-            for c in range(pieces):
-                line = value[:, c * lines[1] : (c + 1) * lines[1]]
-                marks = jnp.where(row == at * pieces + c, line, marks)
-        out_ref[...] = (notes_ref[...] + marks[None]).astype(BF16)
+def total_kernel(got_ref, notes_ref, payload_ref, down_ref, out_ref):
+    down = jnp.sum(got_ref[...].astype(F32), axis=0)
+    down_ref[...] = down
+    norms = jnp.sum(down * down, axis=0, keepdims=True)
+    high = norms.astype(BF16).astype(F32)
+    low = norms - high
+    lines = out_ref.shape[1:]
+    row = lax.broadcasted_iota(jnp.int32, lines, 0)
+    marks = jnp.zeros(lines, F32)
+    pieces = norms.shape[1] // lines[1]
+    for at, value in enumerate((high, low)):
+        for c in range(pieces):
+            line = value[:, c * lines[1] : (c + 1) * lines[1]]
+            marks = jnp.where(row == at * pieces + c, line, marks)
+    out_ref[...] = (notes_ref[...] + marks[None]).astype(BF16)
 
 
 def totals(got, notes, payload):
     size, rows, cols = got.shape
-    steps = 2
+    cols = cols // 3
     experts, extra, lanes = notes.shape
     last = payload.shape[1] // extra - 1
     return pl.pallas_call(
         total_kernel,
-        grid=(steps,),
+        grid=(1,),
         in_specs=[
-            pl.BlockSpec((size // steps, rows, cols), lambda i: (i, 0, 0)),
+            pl.BlockSpec((size, rows, cols), lambda i: (0, 0, 2)),
             pl.BlockSpec((experts, extra, lanes), lambda i: (0, 0, 0)),
             pl.BlockSpec(memory_space=pl.ANY),
         ],
@@ -189,7 +175,6 @@
             jax.ShapeDtypeStruct(payload.shape, BF16),
         ],
         input_output_aliases={2: 1},
-        scratch_shapes=[pltpu.VMEM((rows, cols), F32)],
         compiler_params=pltpu.CompilerParams(vmem_limit_bytes=GRANT),
         name="totals",
     )(got, notes, payload)
@@ -394,10 +379,11 @@
     high = lax.reduce_precision(gate_sum, 8, 7)
     line = jnp.arange(extra)[None, :, None]
     notes = jnp.where(line == 4, high, jnp.where(line == 5, gate_sum - high, 0.0))
-    shared_sum, payload = totals(shared_got, notes, payload)
+    down_sum, payload = totals(shared_got, notes, payload)
     back = to_each(payload)
-    shared_g, shared_u = shared_sum[:, :hid], shared_sum[:, hid : 2 * hid]
-    shared_d = shared_sum[:, 2 * hid :].T
+    shared_sum = jnp.sum(shared_got[:, :, : 2 * hid].astype(F32), axis=0)
+    shared_g, shared_u = shared_sum[:, :hid], shared_sum[:, hid:]
+    shared_d = down_sum.T
 
     low = tp == 0
     inputs = jnp.concatenate(

time: 229 us -> 230 us (level)
  waiting for transfers between devices: 24.4 us -> 30.6 us
    all_to_all x1, waiting for transfers between devices: 2.68 us -> 8.14 us  [layer(): lax.all_to_all(terms, ('ep', 'tp'), 0, 0, tiled=True, axis_index_groups=p...]
    concatenate x3, other arithmetic: 5.53 us -> 3.19 us  [layer(): jnp.concatenate([mm(tokens, s_d, ROWS), mm(cotangent, s_hidden, ROWS)], a...]
    unnamed x49 -> x57, local copies, waits for them, and re-layouts: 7.19 us -> 7.54 us
  transfers between devices with their start and end apart: 10 -> 10, of which waited for: 4 -> 4; matrix products, arithmetic and copies ran while one was open for 29% -> 28% of each run, Pallas kernels for 4% -> 3%
where the time goes in v6:
time: 230 us; the launch traced here: 228 us
  blocking collectives  85.8 us (37%)
  matrix products  42.4 us (18%)
  waiting for transfers between devices  30.6 us (13%)
  other arithmetic  22.4 us (10%)
  Pallas kernels  16.8 us (7%)
  starting transfers between devices  15.5 us (7%)
  local copies, waits for them, and re-layouts  13.3 us (6%)
    all_to_all x1, blocking collectives, to_each(): return lax.all_to_all(x, 'ep', 0, 0, tiled=True, axis_index_groups=[order])  85.8 us
    dot_general x15, matrix products, mm(): return lax.dot_general(a, b, contract, preferred_element_type=F32)  42.4 us
    all_to_all x1, waiting for transfers between devices, to_each(): return lax.all_to_all(x, 'ep', 0, 0, tiled=True, axis_index_groups=[order])  13.9 us
    ppermute x3, waiting for transfers between devices, next_along(): return lax.ppermute(x, ('ep', 'tp'), pairs)  8.53 us
    all_to_all x1, waiting for transfers between devices, layer(): lax.all_to_all(terms, ('ep', 'tp'), 0, 0, tiled=True, axis_index_groups=p...  8.14 us
    unnamed x57, local copies, waits for them, and re-layouts  7.54 us
    select_n x1, other arithmetic, layer(): jnp.where(low, got[:, half:], peer[:, half:])  6.89 us
    all_to_all x1, starting transfers between devices, to_each(): return lax.all_to_all(x, 'ep', 0, 0, tiled=True, axis_index_groups=[order])  6.51 us
  transfers between devices with their start and end apart: 10, of which 4 were waited for; matrix products, arithmetic and copies ran while one was open for 28% of the time, Pallas kernels for 3%

profile of v6, /device:TPU:0, one launch (start us, length us, event | category | flops | bytes accessed | tf_op | source)
XLA Modules:
  0.0 228.0 jit_solution(9590338100693923771)
XLA Ops:
  0.7 5.8 %routing.1 = (bf16[1536,2048]{1,0:T(8,128)(2,1)}, f32[64,256]{1,0:T(8,128)}) custom-call(s32[1]{0:T(128)} %bitcast.3.tp_ref, s32[4,256]{1,0:T(4,128)} %bitcast.48, f32[4,256]{1,0:T(4,128)} %bitcast.50, bf16[256,2048]{1,0:T(8,128)(2,1)} %tok_ref.1, bf16[256,2048]{1,0:T(8,128)(2,1)} %cot_ref.1), custom_call_target="tpu_custom_call" | custom-call | tf_op jit(solution)/shard_map/routing/pallas_call | solution.py:83
  6.4 85.8 %all_to_all.15 = bf16[64,24,2048]{2,1,0:T(8,128)(2,1)} all-to-all(bf16[64,24,2048]{2,1,0:T(8,128)(2,1)} %bitcast.52), channel_id=1, replica_groups={{0,58,116,46,104,34,92,22,80,10,68,126,56,114,44,102,32,90,20,78,8,66,1..., dimensions={0} | all-to-all | bytes 12582912 | tf_op jit(solution)/shard_map/all_to_all | solution.py:34
  92.2 1.4 fusion.16.w_ref
  93.8 1.8 fusion.57
  95.6 2.2 fusion.58
  101.8 2.9 %fusion.9 = f32[1536,256]{1,0:T(8,128)S(1)} fusion(bf16[1536,2048]{1,0:T(8,128)(2,1)} %bitcast.7, bf16[1,256,2048]{2,1,0:T(8,128)(2,1)S(1)} %copy-done, s32[]{:T(128)S(6)} %select_n.116), kind=kOutput, calls=%fused_computation.51 | convolution fusion | flops 805306368 | bytes 5242884 | tf_op jit(solution)/shard_map/dot_general | solution.py:20
  104.7 3.8 %fusion.12 = f32[1536,512]{1,0:T(8,128)S(1)} fusion(bf16[1024,512]{1,0:T(8,128)(2,1)S(1)} %fusion.16.w_ref, bf16[1536,2048]{1,0:T(8,128)(2,1)} %bitcast.7), kind=kOutput, calls=%fused_computation.54 | convolution fusion | flops 1610612736 | bytes 7340032 | tf_op jit(solution)/shard_map/dot_general | solution.py:20
  108.6 3.7 %convolution_add_fusion = f32[1536,512]{1,0:T(8,128)S(1)} fusion(f32[1536,512]{1,0:T(8,128)S(1)} %fusion.12, bf16[1536,2048]{1,0:T(8,128)(2,1)} %collective-permute-done.3, s32[]{:T(128)S(6)} %select_n.117, bf16[2048,256]{1,0:T(8,128)(2,1)S(1)} %bitcast.57, bf16[2048,256]{1,0:T(8,128)(2,1)S(1)} %bitcast.60), kind=kOutput, calls=%fused_computation.40 | convolution fusion | flops 1613496320 | bytes 11534340 | tf_op jit(solution)/shard_map/dot_general | solution.py:20
  112.3 4.4 %multiply_convert_fusion.1 = (bf16[1536,256]{1,0:T(8,128)(2,1)S(1)}, bf16[1536,256]{1,0:T(8,128)(2,1)S(1)}, f32[1536]{0:T(1024)S(1)}, bf16[1536,256]{1,0:T(8,128)(2,1)}) fusion(f32[1536,512]{1,0:T(8,128)S(1)} %convolution_add_fusion, f32[1536,256]{1,0:T(8,128)S(1)} %fusion.9, bf16[1,256,2048]{2,1,0:T(8,128)(2,1)S(1)} %copy-done, s32[]{:T(128)S(6)} %select_n.117, ...), kind=kOutput, calls=%fused_computation.65 | convolution fusion | flops 812775936 | bytes 10754052 | tf_op jit(solution)/shard_map/dot_general | solution.py:20
  116.7 3.5 %convolution_convert_fusion = bf16[1536,1024]{1,0:T(8,128)(2,1)} fusion(s32[]{:T(128)S(6)} %select_n.117, bf16[2048,256]{1,0:T(8,128)(2,1)S(1)} %bitcast.58, bf16[2048,256]{1,0:T(8,128)(2,1)S(1)} %bitcast.61, bf16[1536,256]{1,0:T(8,128)(2,1)S(1)} %get-tuple-element.67, bf16[1536,256]{1,0:T(8,128)(2,1)S(1)} %get-tuple-element.66), kind=kOutput, calls=%fused_computation.39 | convolution fusion | flops 1617428480 | bytes 6815748 | tf_op jit(solution)/shard_map/dot_general | solution.py:20
  123.1 2.0 pad_maximum_fusion.6
  125.1 2.4 %collective-permute-start.1 = (bf16[512,768]{1,0:T(8,128)(2,1)}, bf16[512,768]{1,0:T(8,128)(2,1)S(1)}, u32[]{:S(2)}, u32[]{:S(2)}) collective-permute-start(bf16[512,768]{1,0:T(8,128)(2,1)} %pad_maximum_fusion.6), channel_id=1, source_target_pairs={{0,64},{1,17},{2,66},{3,19},{4,68},{5,21},{6,70},{7,23},{8,72},{9,... | collective-permute-start | bytes 2359304 | tf_op jit(solution)/shard_map/ppermute | solution.py:258
  127.5 1.9 pad_maximum_fusion.7
  130.7 1.3 copy-done.11
  134.5 3.0 %copy.40 = f32[256,1536]{1,0:T(8,128)} copy(f32[256,1536]{0,1:T(8,128)} %bitcast.53) | data formatting | bytes 3145728 | tf_op jit(solution)/shard_map/eq | solution.py:363
  138.9 4.4 %collective-permute-done.b_ref = bf16[512,768]{1,0:T(8,128)(2,1)S(1)} collective-permute-done((bf16[512,768]{1,0:T(8,128)(2,1)}, bf16[512,768]{1,0:T(8,128)(2,1)S(1)}, u32[]{:S(2)}, u32[]{:S(2)}) %collective-permute-start) | collective-permute-done | bytes 786464 | tf_op jit(solution)/shard_map/ppermute | solution.py:258
  143.3 4.1 %collective-permute-done.2.d_ref = bf16[512,768]{1,0:T(8,128)(2,1)S(1)} collective-permute-done((bf16[512,768]{1,0:T(8,128)(2,1)}, bf16[512,768]{1,0:T(8,128)(2,1)S(1)}, u32[]{:S(2)}, u32[]{:S(2)}) %collective-permute-start.2) | collective-permute-done | bytes 786464 | tf_op jit(solution)/shard_map/ppermute | solution.py:258
  148.6 4.5 %all-to-all-start = ((bf16[16,32,768]{2,1,0:T(8,128)(2,1)}), bf16[16,32,768]{2,1,0:T(8,128)(2,1)S(1)}, u32[]{:S(2)}, u32[]{:S(2)}) async-start(bf16[16,32,768]{2,1,0:T(8,128)(2,1)} %bitcast.2), calls=%async_computation | async-start | bytes 1572864 | tf_op jit(solution)/shard_map/all_to_all | solution.py:352
  153.1 2.7 %convolution_convert_fusion.4.own_ref = bf16[256,1024]{1,0:T(8,128)(2,1)} fusion(bf16[2048,512]{1,0:T(8,128)(2,1)} %copy-done.11, s32[]{:T(128)S(6)} %select_n.116, bf16[256,256]{0,1:T(8,128)(2,1)} %copy-done.15, bf16[256,256]{0,1:T(8,128)(2,1)} %copy-done.13), kind=kOutput, calls=%fused_computation.72 | convolution fusion | flops 269221888 | bytes 1835012 | tf_op jit(solution)/shard_map/dot_general | solution.py:20
  155.8 2.5 %compare_convert_fusion.select_ref = bf16[256,1536]{1,0:T(8,128)(2,1)} fusion(f32[256,1536]{1,0:T(8,128)} %copy.40, f32[1536]{0:T(1024)S(1)} %eq.48), kind=kLoop, calls=%fused_computation.70 | loop fusion | flops 786432 | bytes 2365440 | tf_op jit(solution)/shard_map/convert_element_type | solution.py:364
  158.3 8.1 %all-to-all-done.got_ref = bf16[16,32,768]{2,1,0:T(8,128)(2,1)S(1)} async-done(((bf16[16,32,768]{2,1,0:T(8,128)(2,1)}), bf16[16,32,768]{2,1,0:T(8,128)(2,1)S(1)}, u32[]{:S(2)}, u32[]{:S(2)}) %all-to-all-start) | async-done | bytes 786464 | tf_op jit(solution)/shard_map/all_to_all | solution.py:352
  167.3 1.5 pad_maximum_fusion.3.d_ref
  169.0 5.4 %payload.1.payload_ref = bf16[64,200,128]{2,1,0:T(8,128)(2,1)} custom-call(bf16[1536,512]{1,0:T(8,128)(2,1)S(1)} %pad_maximum_fusion.3.d_ref, bf16[1024,512]{1,0:T(8,128)(2,1)S(1)} %fusion.16.w_ref, bf16[1536,1024]{1,0:T(8,128)(2,1)} %collective-permute-done.5.peer_ref), custom_call_target="tpu_custom_call" | custom-call | tf_op jit(solution)/shard_map/payload/pallas_call | solution.py:124
  175.2 6.5 %all-to-all-start.2 = ((bf16[64,200,128]{2,1,0:T(8,128)(2,1)}), bf16[64,200,128]{2,1,0:T(8,128)(2,1)}, u32[]{:S(2)}, u32[]{:S(2)}) async-start(bf16[64,200,128]{2,1,0:T(8,128)(2,1)} %get-tuple-element.22), calls=%async_computation.2 | async-start | bytes 6553600 | tf_op jit(solution)/shard_map/all_to_all | solution.py:34
  181.7 6.9 %broadcast_select_fusion.1 = (bf16[1536,1024]{1,0:T(8,128)(2,1)S(1)}, bf16[1536,1024]{1,0:T(8,128)(2,1)S(1)}, bf16[1536,1024]{1,0:T(8,128)(2,1)}, bf16[1536,1024]{1,0:T(8,128)(2,1)S(1)}) fusion(pred[]{:T(512)S(6)} %eq.42, bf16[1536,2048]{1,0:T(8,128)(2,1)} %collective-permute-done.3, bf16[1536,2048]{1,0:T(8,128)(2,1)} %bitcast.7), kind=kLoop, calls=%fused_computation.42 | loop fusion | flops 6291456 | bytes 25165824 | tf_op jit(solution)/shard_map/jit(_where)/select_n | solution.py:394
  188.6 4.2 %multiply_reduce_fusion.2 = (f32[2048]{0:T(1024)S(1)}, f32[2048,256]{0,1:T(8,128)}) fusion(bf16[1536,256]{1,0:T(8,128)(2,1)S(1)} %copy-done.26, bf16[1536,1024]{1,0:T(8,128)(2,1)S(1)} %get-tuple-element.63, bf16[1536,1024]{1,0:T(8,128)(2,1)S(1)} %get-tuple-element.65), kind=kOutput, calls=%fused_computation.62 | convolution fusion | flops 1624242176 | bytes 9183232 | tf_op jit(solution)/shard_map/dot_general | solution.py:20
  192.8 4.2 %multiply_reduce_fusion.1 = (f32[2048]{0:T(1024)S(1)}, f32[2048,256]{0,1:T(8,128)}) fusion(bf16[1536,256]{1,0:T(8,128)(2,1)S(1)} %copy-done.24, bf16[1536,1024]{1,0:T(8,128)(2,1)S(1)} %get-tuple-element.63, bf16[1536,1024]{1,0:T(8,128)(2,1)S(1)} %get-tuple-element.65), kind=kOutput, calls=%fused_computation.61 | convolution fusion | flops 1624242176 | bytes 9183232 | tf_op jit(solution)/shard_map/dot_general | solution.py:20
  197.2 5.8 %multiply_reduce_fusion = (f32[256]{0:T(256)}, f32[256,2048]{1,0:T(8,128)}) fusion(bf16[1536,256]{1,0:T(8,128)(2,1)} %get-tuple-element.69, bf16[1536,1024]{1,0:T(8,128)(2,1)} %get-tuple-element.64, bf16[1536,1024]{1,0:T(8,128)(2,1)S(1)} %get-tuple-element.62), kind=kOutput, calls=%fused_computation.60 | convolution fusion | flops 1624243968 | bytes 9176064 | tf_op jit(solution)/shard_map/dot_general | solution.py:20
  203.1 2.9 %copy.41 = f32[1,2048,256]{2,1,0:T(8,128)} copy(f32[1,2048,256]{1,2,0:T(8,128)} %bitcast.54) | data formatting | bytes 4194304
  206.0 3.0 %copy.42 = f32[1,2048,256]{2,1,0:T(8,128)} copy(f32[1,2048,256]{1,2,0:T(8,128)} %bitcast.55) | data formatting | bytes 4194304
  210.2 13.9 %all-to-all-done.2.rows_ref.notes_ref = bf16[64,200,128]{2,1,0:T(8,128)(2,1)} async-done(((bf16[64,200,128]{2,1,0:T(8,128)(2,1)}), bf16[64,200,128]{2,1,0:T(8,128)(2,1)}, u32[]{:S(2)}, u32[]{:S(2)}) %all-to-all-start.2) | async-done | bytes 3276832 | tf_op jit(solution)/shard_map/all_to_all | solution.py:34
  224.1 3.8 %final.1 = (bf16[256,1024]{1,0:T(8,128)(2,1)}, f32[4,256]{1,0:T(4,128)}, f32[1,256]{1,0:T(1,128)}) custom-call(bf16[64,200,128]{2,1,0:T(8,128)(2,1)} %all-to-all-done.2.rows_ref.notes_ref, bf16[64,200,128]{2,1,0:T(8,128)(2,1)} %all-to-all-done.2.rows_ref.notes_ref, bf16[256,1536]{1,0:T(8,128)(2,1)S(1)} %copy-done.2, bf16[256,1024]{1,0:T(8,128)(2,1)S(1)} %copy-done.3, ...), custom_call_target="tpu_custom_call" | custom-call | tf_op jit(solution)/shard_map/final/pallas_call | solution.py:219
  (94 shorter events, 16.7 us)
Async XLA Ops:
  0.6 101.2 %copy-start = (bf16[1,256,2048]{2,1,0:T(8,128)(2,1)S(1)}, bf16[1,256,2048]{2,1,0:T(8,128)(2,1)}, u32[]{:S(2)}) copy-start(bf16[1,256,2048]{2,1,0:T(8,128)(2,1)} %param.16) | copy-start | bytes 3145732
  92.2 16.4 %collective-permute-start.3 = (bf16[1536,2048]{1,0:T(8,128)(2,1)}, bf16[1536,2048]{1,0:T(8,128)(2,1)}, u32[]{:S(2)}, u32[]{:S(2)}) collective-permute-start(bf16[1536,2048]{1,0:T(8,128)(2,1)} %bitcast.7), channel_id=1, source_target_pairs={{0,1},{1,0},{2,3},{3,2},{4,5},{5,4},{6,7},{7,6},{8,9},{9,8},{10,11... | collective-permute-start | bytes 18874376 | tf_op jit(solution)/shard_map/ppermute | solution.py:24
  93.8 4.0 %copy-start.10 = (bf16[256,2048]{1,0:T(8,128)(2,1)S(1)}, bf16[256,2048]{1,0:T(8,128)(2,1)}, u32[]{:S(2)}) copy-start(bf16[256,2048]{1,0:T(8,128)(2,1)} %tok_ref.1) | copy-start | bytes 3145732
  93.8 4.0 %copy-start.19 = (bf16[2048,256]{1,0:T(8,128)(2,1)S(1)}, bf16[2048,256]{1,0:T(8,128)(2,1)}, u32[]{:S(2)}) copy-start(bf16[2048,256]{1,0:T(8,128)(2,1)} %param.17) | copy-start | bytes 3145732
  99.8 8.8 %copy-start.7 = (bf16[2048,512]{1,0:T(8,128)(2,1)}, bf16[2048,512]{1,0:T(8,128)(2,1)S(1)}, u32[]{:S(2)}) copy-start(bf16[2048,512]{1,0:T(8,128)(2,1)S(1)} %fusion.6) | copy-start | bytes 6291460
  104.7 3.9 %copy-start.17 = (bf16[1,2048,256]{2,1,0:T(8,128)(2,1)S(1)}, bf16[1,2048,256]{2,1,0:T(8,128)(2,1)}, u32[]{:S(2)}) copy-start(bf16[1,2048,256]{2,1,0:T(8,128)(2,1)} %param.14) | copy-start | bytes 3145732
  104.7 3.9 %copy-start.18 = (bf16[1,2048,256]{2,1,0:T(8,128)(2,1)S(1)}, bf16[1,2048,256]{2,1,0:T(8,128)(2,1)}, u32[]{:S(2)}) copy-start(bf16[1,2048,256]{2,1,0:T(8,128)(2,1)} %param.15) | copy-start | bytes 3145732
  116.7 3.5 %copy-start.23 = (bf16[1536,256]{1,0:T(8,128)(2,1)}, bf16[1536,256]{1,0:T(8,128)(2,1)S(1)}, u32[]{:S(2)}) copy-start(bf16[1536,256]{1,0:T(8,128)(2,1)S(1)} %get-tuple-element.67) | copy-start | bytes 2359300
  116.7 3.5 %copy-start.25 = (bf16[1536,256]{1,0:T(8,128)(2,1)}, bf16[1536,256]{1,0:T(8,128)(2,1)S(1)}, u32[]{:S(2)}) copy-start(bf16[1536,256]{1,0:T(8,128)(2,1)S(1)} %get-tuple-element.66) | copy-start | bytes 2359300
  120.2 2.9 %copy-start.22 = (bf16[128,768]{1,0:T(8,128)(2,1)S(1)}, bf16[128,768]{1,0:T(8,128)(2,1)}, u32[]{:S(2)}) copy-start(bf16[128,768]{1,0:T(8,128)(2,1)} %get-tuple-element.80) | copy-start | bytes 589828
  120.2 48.8 %collective-permute-start.5 = (bf16[1536,1024]{1,0:T(8,128)(2,1)}, bf16[1536,1024]{1,0:T(8,128)(2,1)}, u32[]{:S(2)}, u32[]{:S(2)}) collective-permute-start(bf16[1536,1024]{1,0:T(8,128)(2,1)} %convolution_convert_fusion), channel_id=1, source_target_pairs={{0,1},{1,0},{2,3},{3,2},{4,5},{5,4},{6,7},{7,6},{8,9},{9,8},{10,11... | collective-permute-start | bytes 9437192 | tf_op jit(solution)/shard_map/ppermute | solution.py:24
  121.5 6.0 %copy-start.21 = (bf16[128,768]{1,0:T(8,128)(2,1)S(1)}, bf16[128,768]{1,0:T(8,128)(2,1)}, u32[]{:S(2)}) copy-start(bf16[128,768]{1,0:T(8,128)(2,1)} %get-tuple-element.70) | copy-start | bytes 589828
  121.5 21.8 %collective-permute-start = (bf16[512,768]{1,0:T(8,128)(2,1)}, bf16[512,768]{1,0:T(8,128)(2,1)S(1)}, u32[]{:S(2)}, u32[]{:S(2)}) collective-permute-start(bf16[512,768]{1,0:T(8,128)(2,1)} %pad_maximum_fusion.5), channel_id=1, source_target_pairs={{0,32},{1,9},{2,34},{3,11},{4,36},{5,13},{6,38},{7,15},{8,40},{9,1... | collective-permute-start | bytes 2359304 | tf_op jit(solution)/shard_map/ppermute | solution.py:258
  121.9 8.6 %copy-start.20 = (bf16[2048,256]{1,0:T(8,128)(2,1)S(1)}, bf16[2048,256]{1,0:T(8,128)(2,1)}, u32[]{:S(2)}) copy-start(bf16[2048,256]{1,0:T(8,128)(2,1)} %param.17) | copy-start | bytes 3145732
  123.1 7.5 %copy-start.12 = (bf16[2048,256]{1,0:T(8,128)(2,1)S(1)}, bf16[2048,256]{1,0:T(8,128)(2,1)}, u32[]{:S(2)}) copy-start(bf16[2048,256]{1,0:T(8,128)(2,1)} %param.18) | copy-start | bytes 3145732
  125.1 6.9 %copy-start.14 = (bf16[256,256]{0,1:T(8,128)(2,1)S(1)}, bf16[256,256]{0,1:T(8,128)(2,1)}, u32[]{:S(2)}) copy-start(bf16[256,256]{0,1:T(8,128)(2,1)} %copy-done.13) | copy-start | bytes 393220
  125.1 6.9 %copy-start.16 = (bf16[256,256]{0,1:T(8,128)(2,1)S(1)}, bf16[256,256]{0,1:T(8,128)(2,1)}, u32[]{:S(2)}) copy-start(bf16[256,256]{0,1:T(8,128)(2,1)} %copy-done.15) | copy-start | bytes 393220
  125.1 18.2 %collective-permute-start.1 = (bf16[512,768]{1,0:T(8,128)(2,1)}, bf16[512,768]{1,0:T(8,128)(2,1)S(1)}, u32[]{:S(2)}, u32[]{:S(2)}) collective-permute-start(bf16[512,768]{1,0:T(8,128)(2,1)} %pad_maximum_fusion.6), channel_id=1, source_target_pairs={{0,64},{1,17},{2,66},{3,19},{4,68},{5,21},{6,70},{7,23},{8,72},{9,... | collective-permute-start | bytes 2359304 | tf_op jit(solution)/shard_map/ppermute | solution.py:258
  129.4 3.9 %copy-start.4 = (f32[64,256]{1,0:T(8,128)S(1)}, f32[64,256]{1,0:T(8,128)}, u32[]{:S(2)}) copy-start(f32[64,256]{1,0:T(8,128)} %get-tuple-element.23.place_ref) | copy-start | bytes 196612
  129.4 18.1 %collective-permute-start.2 = (bf16[512,768]{1,0:T(8,128)(2,1)}, bf16[512,768]{1,0:T(8,128)(2,1)S(1)}, u32[]{:S(2)}, u32[]{:S(2)}) collective-permute-start(bf16[512,768]{1,0:T(8,128)(2,1)} %pad_maximum_fusion.7), channel_id=1, source_target_pairs={{0,96},{1,25},{2,98},{3,27},{4,100},{5,29},{6,102},{7,31},{8,104},... | collective-permute-start | bytes 2359304 | tf_op jit(solution)/shard_map/ppermute | solution.py:258
  133.3 76.9 %collective-permute-start.6 = (bf16[256,1024]{1,0:T(8,128)(2,1)}, bf16[256,1024]{1,0:T(8,128)(2,1)}, u32[]{:S(2)}, u32[]{:S(2)}) collective-permute-start(bf16[256,1024]{1,0:T(8,128)(2,1)} %convolution_convert_fusion.3), channel_id=1, source_target_pairs={{0,1},{1,0},{2,3},{3,2},{4,5},{5,4},{6,7},{7,6},{8,9},{9,8},{10,11... | collective-permute-start | bytes 1572872 | tf_op jit(solution)/shard_map/ppermute | solution.py:24
  148.6 17.8 %all-to-all-start = ((bf16[16,32,768]{2,1,0:T(8,128)(2,1)}), bf16[16,32,768]{2,1,0:T(8,128)(2,1)S(1)}, u32[]{:S(2)}, u32[]{:S(2)}) async-start(bf16[16,32,768]{2,1,0:T(8,128)(2,1)} %bitcast.2), calls=%async_computation | async-start | bytes 1572864 | tf_op jit(solution)/shard_map/all_to_all | solution.py:352
  167.2 1.6 collective-permute-start.4
  175.2 48.9 %all-to-all-start.2 = ((bf16[64,200,128]{2,1,0:T(8,128)(2,1)}), bf16[64,200,128]{2,1,0:T(8,128)(2,1)}, u32[]{:S(2)}, u32[]{:S(2)}) async-start(bf16[64,200,128]{2,1,0:T(8,128)(2,1)} %get-tuple-element.22), calls=%async_computation.2 | async-start | bytes 6553600 | tf_op jit(solution)/shard_map/all_to_all | solution.py:34
  181.7 6.9 %copy-start.26 = (bf16[1536,256]{1,0:T(8,128)(2,1)S(1)}, bf16[1536,256]{1,0:T(8,128)(2,1)}, u32[]{:S(2)}) copy-start(bf16[1536,256]{1,0:T(8,128)(2,1)} %copy-done.25) | copy-start | bytes 2359300
  188.6 4.2 %copy-start.24 = (bf16[1536,256]{1,0:T(8,128)(2,1)S(1)}, bf16[1536,256]{1,0:T(8,128)(2,1)}, u32[]{:S(2)}) copy-start(bf16[1536,256]{1,0:T(8,128)(2,1)} %copy-done.23) | copy-start | bytes 2359300
  197.0 11.9 %collective-permute-start.7 = (f32[4160]{0:T(1024)S(1)}, f32[4160]{0:T(1024)S(1)}, u32[]{:S(2)}, u32[]{:S(2)}) collective-permute-start(f32[4160]{0:T(1024)S(1)} %concatenate.49), channel_id=1, source_target_pairs={{0,1},{1,0},{2,3},{3,2},{4,5},{5,4},{6,7},{7,6},{8,9},{9,8},{10,11... | collective-permute-start | bytes 49928 | tf_op jit(solution)/shard_map/ppermute | solution.py:24
  205.9 18.1 %copy-start.2 = (bf16[256,1536]{1,0:T(8,128)(2,1)S(1)}, bf16[256,1536]{1,0:T(8,128)(2,1)}, u32[]{:S(2)}) copy-start(bf16[256,1536]{1,0:T(8,128)(2,1)} %compare_convert_fusion.select_ref) | copy-start | bytes 2359300
  205.9 18.1 %copy-start.3 = (bf16[256,1024]{1,0:T(8,128)(2,1)S(1)}, bf16[256,1024]{1,0:T(8,128)(2,1)}, u32[]{:S(2)}) copy-start(bf16[256,1024]{1,0:T(8,128)(2,1)} %convolution_convert_fusion.4.own_ref) | copy-start | bytes 1572868
  205.9 18.1 %copy-start.5 = (s32[256,4]{0,1:T(4,128)S(1)}, s32[256,4]{0,1:T(4,128)}, u32[]{:S(2)}) copy-start(s32[256,4]{0,1:T(4,128)} %param.11) | copy-start | bytes 12292
  206.0 18.1 %copy-start.6 = (f32[256,4]{0,1:T(4,128)S(1)}, f32[256,4]{0,1:T(4,128)}, u32[]{:S(2)}) copy-start(f32[256,4]{0,1:T(4,128)} %param.12) | copy-start | bytes 12292
  209.5 18.3 %copy-start.1 = (bf16[1,256,2048]{2,1,0:T(8,128)(2,1)S(1)}, bf16[1,256,2048]{2,1,0:T(8,128)(2,1)}, u32[]{:S(2)}) copy-start(bf16[1,256,2048]{2,1,0:T(8,128)(2,1)} %param.16) | copy-start | bytes 3145732
  (5 other events, 8.5 us)
